TPU v7x, 32 devices: a whole 2x2x4 slice. The times are simulated.
32 devices in a mesh: sp: 4 (over z), fs: 4 (over y, core), tp: 2 (over x).
Axes of the slice: x: 2, y: 2, z: 4, core: 2. Of those that a mesh axis runs over, the one named last changes fastest.
Arguments:
- tokens: bfloat16 [4, 768, 2048], P('fs', 'sp'), may hold values from -6 to 6
- decay_pace: float32 [4, 768], P('fs', 'sp'), may hold values from 0.5 to 2, as said below
- start_state: float32 [4, 16, 64, 64], P('fs', 'tp'), may hold values from -80 to 80
- norm_gain: float32 [2048], replicated, may hold values from 0.1 to 1.9
- conv_value: bfloat16 [2048, 512], P(('sp', 'fs'), 'tp'), may hold values from -0.125 to 0.125
- conv_admit: bfloat16 [2048, 512], P(('sp', 'fs'), 'tp'), may hold values from -0.125 to 0.125
- conv_gate: bfloat16 [2048, 512], P(('sp', 'fs'), 'tp'), may hold values from -0.125 to 0.125
- state_query: bfloat16 [2048, 1024], P(('sp', 'fs'), 'tp'), may hold values from -0.125 to 0.125
- state_key: bfloat16 [2048, 1024], P(('sp', 'fs'), 'tp'), may hold values from -0.125 to 0.125
- state_value: bfloat16 [2048, 1024], P(('sp', 'fs'), 'tp'), may hold values from -0.125 to 0.125
- state_decay: bfloat16 [2048, 1024], P(('sp', 'fs'), 'tp'), may hold values from -0.125 to 0.125
- state_gate: bfloat16 [2048, 1024], P(('sp', 'fs'), 'tp'), may hold values from -0.125 to 0.125
- conv_taps: float32 [31, 512], P(None, 'tp'), may hold values from -4 to 4
- conv_gain: float32 [512], P('tp'), may hold values from 0.1 to 1.9
- point_weight: bfloat16 [512, 512], replicated, may hold values from -0.25 to 0.25
- decay_base: float32 [1024], P('tp'), may hold values from -13 to -3
- correction: float32 [1024], P('tp'), may hold values from 0 to 0.9
- group_gain: float32 [1024], P('tp'), may hold values from 0.1 to 1.9
- output_conv: bfloat16 [512, 2048], P('tp', ('sp', 'fs')), may hold values from -0.25 to 0.25
- output_state: bfloat16 [1024, 2048], P('tp', ('sp', 'fs')), may hold values from -0.1875 to 0.1875
Outputs:
- mixed: bfloat16 [4, 768, 2048], P('fs', ('sp', 'tp'))
Inputs may be any that keep to these rules, and one draw needn't show every extreme that they name: `decay_pace`: constant over runs of positions, a quarter of 192 long.
All inputs are finite; a program needn't handle non-finite values.
Results may differ from a plain program's by a relative error of at most 0.017.
Values may be sent and summed in bfloat16 or wider, within the bound.
No kernel may reach another device: no remote copies, remote signals or barrier semaphores. Data moves between devices by JAX's collectives and lax.ppermute only.
A program may use at most 64 MiB of HBM per device.

v0:
```python
import jax
import jax.numpy as jnp
from jax import lax
from jax.sharding import PartitionSpec as P

NORM_FLOOR = 0.1
CHANNEL_FLOOR = 0.1
GROUP_FLOOR = 1.0


def passed_along(value, axis, steps):
    count = lax.axis_size(axis)
    leading, last = (max(0, -steps), min(count, count - steps))
    return lax.ppermute(value, axis, [(source, source + steps) for source in range(leading, last)])


def entering_2(value, axis, join, neutral):
    place = lax.axis_index(axis)
    gathered = jax.tree.map(
        lambda a, kind: lax.all_gather(a.astype(kind), axis),
        value,
        jax.tree.map(lambda a: jnp.bfloat16 if a.dtype == jnp.float32 else a.dtype, value),
    )
    state = jax.tree.map(lambda a, e: jnp.zeros_like(a) + jnp.asarray(e, a.dtype), value, neutral)

    def one(lap, state):
        return join(
            state,
            jax.tree.map(
                lambda a, own: lax.dynamic_index_in_dim(a, lap, 0, False).astype(own.dtype),
                gathered,
                value,
            ),
        )

    return lax.fori_loop(0, place, one, state)


def apply_map(matrix, right):
    return jnp.einsum("hbti,hbic->hbtc", matrix, right, precision=lax.Precision.HIGHEST)


def pair_terms(left, right, mask):
    return jnp.einsum("hbtc,hbic->hbti", left, right, precision=lax.Precision.HIGHEST) * mask


def compose(earlier, later):
    first = jnp.matmul(earlier[0], later[0], precision=lax.Precision.HIGHEST)
    second = jnp.matmul(earlier[1], later[0], precision=lax.Precision.HIGHEST) + later[1]
    return (first, second)


def block_terms(query, keys, values, unit, write, log_keep):
    size = query.shape[-1]
    span = query.shape[2]
    total_log = jnp.cumsum(log_keep, axis=2)
    before_log = total_log - log_keep
    last_log = total_log[:, :, span - 1 :, :]
    lead_remove = -unit * jnp.exp(before_log)
    lead_query = query * jnp.exp(total_log)
    back_write = write * jnp.exp(-total_log)
    back_key = keys * jnp.exp(-total_log)
    places = jnp.arange(span)
    strict = (places[:, None] > places[None, :]).astype(jnp.float32)
    weak = (places[:, None] >= places[None, :]).astype(jnp.float32)
    remove_write = pair_terms(lead_remove, back_write, strict)
    remove_key = pair_terms(lead_remove, back_key, strict)
    query_write = pair_terms(lead_query, back_write, weak)
    query_key = pair_terms(lead_query, back_key, weak)
    right_side = jnp.concatenate([apply_map(remove_key, values), lead_remove], axis=-1)
    system = jnp.eye(span, dtype=jnp.float32) - remove_write
    solved = jax.scipy.linalg.solve_triangular(system, right_side, lower=True, unit_diagonal=True)
    own_part = solved[..., :size]
    start_part = solved[..., size:]
    local_out = apply_map(query_write, own_part) + apply_map(query_key, values)
    start_map = lead_query + apply_map(query_write, start_part)
    tail_write = write * jnp.exp(last_log - total_log)
    tail_key = keys * jnp.exp(last_log - total_log)
    carry_map = jnp.einsum(
        "hbtk,hbtj->hbkj", start_part, tail_write, precision=lax.Precision.HIGHEST
    ) + jnp.eye(size, dtype=jnp.float32) * jnp.exp(last_log)
    carry_add = jnp.einsum(
        "hbtv,hbtj->hbvj", own_part, tail_write, precision=lax.Precision.HIGHEST
    ) + jnp.einsum("hbtv,hbtj->hbvj", values, tail_key, precision=lax.Precision.HIGHEST)
    return (local_out, start_map, carry_map, carry_add)


def body(
    tokens,
    decay_pace,
    start_state,
    norm_gain,
    conv_value,
    conv_admit,
    conv_gate,
    state_query,
    state_key,
    state_value,
    state_decay,
    state_gate,
    conv_taps,
    conv_gain,
    point_weight,
    decay_base,
    correction,
    group_gain,
    output_conv,
    output_state,
):
    width = tokens.shape[-1]
    rows = tokens.reshape(-1, width)
    length = rows.shape[0]
    floats = rows.astype(jnp.float32)
    inverse = lax.rsqrt(jnp.mean(floats * floats, axis=1, keepdims=True) + NORM_FLOOR)
    normed = (floats * inverse * norm_gain).astype(jnp.bfloat16)
    shards = (
        conv_value,
        conv_admit,
        conv_gate,
        state_query,
        state_key,
        state_value,
        state_decay,
        state_gate,
    )
    stacked = jnp.concatenate(shards, axis=1)
    projected = jnp.dot(
        normed,
        lax.all_gather(stacked, ("sp", "fs"), axis=0, tiled=True),
        preferred_element_type=jnp.float32,
    ).astype(jnp.bfloat16)
    pieces = []
    offset = 0
    for shard in shards:
        pieces.append(projected[:, offset : offset + shard.shape[1]].astype(jnp.float32))
        offset = offset + shard.shape[1]
    value, admit, gate_conv, query, keys, values, decay_in, gate_state = pieces
    channels = value.shape[1]
    kernel = conv_taps.shape[0]
    conv_input = (value * jax.nn.sigmoid(admit)).astype(jnp.bfloat16)
    earlier = passed_along(conv_input[length - (kernel - 1) :], "sp", 1)
    padded = jnp.concatenate([earlier, conv_input], axis=0).astype(jnp.float32)
    conv_sum = jnp.zeros((length, channels), jnp.float32)
    for place in range(kernel):
        conv_sum = conv_sum + conv_taps[place] * padded[place : place + length]
    local_point = lax.dynamic_slice_in_dim(
        point_weight, lax.axis_index("tp") * channels, channels, 1
    )
    whole_sum, whole_gain = (
        lax.all_gather(conv_sum.astype(jnp.bfloat16), "tp", axis=1, tiled=True).astype(
            conv_sum.dtype
        ),
        lax.all_gather(conv_gain.astype(jnp.bfloat16), "tp", axis=0, tiled=True).astype(
            conv_gain.dtype
        ),
    )
    mean = jnp.mean(whole_sum, axis=1, keepdims=True)
    spread = jnp.mean(whole_sum * whole_sum, axis=1, keepdims=True) - mean * mean
    shaped = jax.nn.silu(
        (whole_sum - mean) * lax.rsqrt(spread + CHANNEL_FLOOR) * whole_gain
    ).astype(jnp.bfloat16)
    pointwise = jnp.dot(shaped, local_point, preferred_element_type=jnp.float32)
    conv_out = (pointwise * jax.nn.silu(gate_conv)).astype(jnp.bfloat16)
    size = start_state.shape[-1]
    heads = query.shape[1] // size
    span = min(64, length)
    blocks = length // span
    log_keep = -jnp.exp(decay_base + jnp.tanh(decay_in)) * decay_pace.reshape(-1)[:, None]
    key_heads = keys.reshape(length, heads, size)
    unit = key_heads * lax.rsqrt(
        jnp.maximum(jnp.sum(key_heads * key_heads, axis=-1, keepdims=True), 1.0)
    )
    write = unit * correction.reshape(heads, size)

    def arrange(array):
        return array.reshape(blocks, span, heads, size).transpose(2, 0, 1, 3)

    local_out, start_map, carry_map, carry_add = block_terms(
        arrange(query),
        arrange(keys),
        arrange(values),
        arrange(unit),
        arrange(write),
        arrange(log_keep),
    )
    identity = (
        jnp.broadcast_to(jnp.eye(size, dtype=jnp.float32), (heads, size, size)),
        jnp.zeros((heads, size, size), jnp.float32),
    )

    def along(carried, block_pair):
        return (compose(carried, block_pair), carried)

    device_pair, prefixes = lax.scan(
        along, identity, (jnp.moveaxis(carry_map, 1, 0), jnp.moveaxis(carry_add, 1, 0))
    )
    prior_map, prior_add = entering_2(device_pair, "sp", compose, identity)
    begin = start_state.reshape(heads, size, size)
    entering = jnp.matmul(begin, prior_map, precision=lax.Precision.HIGHEST) + prior_add
    block_starts = (
        jnp.matmul(entering[None], prefixes[0], precision=lax.Precision.HIGHEST) + prefixes[1]
    )
    block_starts = jnp.moveaxis(block_starts, 0, 1)
    outputs = local_out + jnp.einsum(
        "hbtk,hbvk->hbtv", start_map, block_starts, precision=lax.Precision.HIGHEST
    )
    outputs = outputs.transpose(1, 2, 0, 3).reshape(length, heads, size)
    centered = outputs - jnp.mean(outputs, axis=-1, keepdims=True)
    variance = jnp.mean(centered * centered, axis=-1, keepdims=True)
    grouped = centered * lax.rsqrt(variance + GROUP_FLOOR) * group_gain.reshape(heads, size)
    state_out = (grouped.reshape(length, heads * size) * jax.nn.silu(gate_state)).astype(
        jnp.bfloat16
    )
    local_mix = jnp.concatenate([conv_out, state_out], axis=1)
    moved = lax.all_to_all(local_mix, "tp", split_axis=0, concat_axis=1, tiled=True)
    conv_rows, state_rows = (
        lax.all_gather(output_conv, "tp", axis=0, tiled=True),
        lax.all_gather(output_state, "tp", axis=0, tiled=True),
    )
    groups = lax.axis_size("tp")
    joined = jnp.concatenate(
        [conv_rows.reshape(groups, channels, -1), state_rows.reshape(groups, heads * size, -1)],
        axis=1,
    )
    joined = joined.reshape(groups * (channels + heads * size), -1)
    mixed = jnp.dot(
        moved,
        lax.all_gather(joined, ("sp", "fs"), axis=1, tiled=True),
        preferred_element_type=jnp.float32,
    )
    return mixed.astype(jnp.bfloat16).reshape(1, -1, width)


def solution(mesh):
    return jax.shard_map(
        body,
        mesh=mesh,
        in_specs=(
            P("fs", "sp", None),
            P("fs", "sp"),
            P("fs", "tp", None, None),
            P(),
            P(("sp", "fs"), "tp"),
            P(("sp", "fs"), "tp"),
            P(("sp", "fs"), "tp"),
            P(("sp", "fs"), "tp"),
            P(("sp", "fs"), "tp"),
            P(("sp", "fs"), "tp"),
            P(("sp", "fs"), "tp"),
            P(("sp", "fs"), "tp"),
            P(None, "tp"),
            P("tp"),
            P(),
            P("tp"),
            P("tp"),
            P("tp"),
            P("tp", ("sp", "fs")),
            P("tp", ("sp", "fs")),
        ),
        out_specs=P("fs", ("sp", "tp"), None),
        check_vma=False,
    )
```

profile of v0, /device:TPU:0, one launch (start us, length us, event | category | flops | bytes accessed | tf_op | source)
XLA Modules:
  0.0 373.3 jit_solution(13243552099346474829)
XLA Ops:
  6.5 0.9 constant_dynamic-update-slice_fusion.8
  7.5 0.8 constant_dynamic-update-slice_fusion.7
  8.3 0.8 constant_dynamic-update-slice_fusion.6
  9.1 0.9 constant_dynamic-update-slice_fusion.5
  10.1 0.9 constant_dynamic-update-slice_fusion.4
  11.0 0.9 constant_dynamic-update-slice_fusion.3
  11.9 0.9 constant_dynamic-update-slice_fusion.2
  12.8 1.0 constant_dynamic-update-slice_fusion.1
  13.8 0.9 copy-done.8
  14.9 5.9 %all_gather.37 = bf16[512,128]{1,0:T(8,128)(2,1)S(1)} all-gather(bf16[256,128]{1,0:T(8,128)(2,1)S(1)} %copy-done.24), channel_id=1, replica_groups=mesh['sp'=4,'fs'=4,'tp'=2] {'tp'}, dimensions={0}, use_global_device_ids=true | all-gather | bytes 196608 | tf_op jit(solution)/shard_map/all_gather | solution.py:217
  20.7 5.6 %all_gather.38 = bf16[1024,128]{1,0:T(8,128)(2,1)S(1)} all-gather(bf16[512,128]{1,0:T(8,128)(2,1)S(1)} %copy-done.20), channel_id=1, replica_groups=mesh['sp'=4,'fs'=4,'tp'=2] {'tp'}, dimensions={0}, use_global_device_ids=true | all-gather | bytes 393216 | tf_op jit(solution)/shard_map/all_gather | solution.py:218
  26.4 0.8 pad_maximum_fusion
  27.2 0.7 fusion.125
  29.5 4.2 %all-gather.2 = bf16[2,1,256]{2,1,0:T(2,128)(2,1)S(1)} all-gather(bf16[1,1,256]{2,1,0:T(2,128)(2,1)S(1)} %reshape.181), channel_id=1, replica_groups=mesh['sp'=4,'fs'=4,'tp'=2] {'tp'}, dimensions={0}, use_global_device_ids=true | all-gather | bytes 1536 | tf_op jit(solution)/shard_map/all_gather | solution.py:153
  34.5 0.7 copy.96
  35.2 89.4 %all-gather.6.cloned.1.call-done = bf16[2048,3328]{1,0:T(8,128)(2,1)} async-done(((bf16[128,3328]{1,0:T(8,128)(2,1)}), bf16[2048,3328]{1,0:T(8,128)(2,1)}) %all-gather.6.cloned.1.call-update) | async-done | bytes 13631504 | tf_op jit(solution)/shard_map/all_gather | solution.py:129
  124.5 7.8 %convolution_convert_fusion = bf16[192,3328]{1,0:T(8,128)(2,1)S(1)} fusion(bf16[2048,3328]{1,0:T(8,128)(2,1)} %all-gather.6.cloned.1.call-done, bf16[1,192,2048]{2,1,0:T(8,128)(2,1)S(1)} %copy-done.9, f32[2048]{0:T(1024)S(1)} %copy-done.62, f32[192]{0:T(256)S(1)} %add_rsqrt_fusion.2), kind=kOutput, calls=%fused_computation.27 | convolution fusion | flops 2619457536 | bytes 15704832 | tf_op jit(solution)/shard_map/dot_general | solution.py:127
  132.4 0.9 fusion.124
  133.9 2.8 collective-permute-start
  139.0 1.6 bitcast_multiply_fusion.3
  140.6 2.5 convolution_multiply_fusion.1
  143.2 2.6 fusion.30
  145.7 119.3 %custom-call.4 = f32[8,3,1,64,64]{3,4,2,1,0:T(8,128)} custom-call(f32[8,3,1,64,64]{4,3,2,1,0:T(8,128)} %fusion.30), custom_call_target="InvertDiagBlocksLowerTriangular" | custom-call | tf_op jit(solution)/shard_map/jit(_solve_triangular)/vmap(vmap())/triangular_solve | solution.py:72
  265.1 1.2 reshape.169
  266.3 0.8 copy.97
  267.1 0.7 copy.100
  267.8 1.7 fusion.68
  269.5 1.6 fusion.35
  271.2 1.7 fusion.49
  272.9 2.8 fusion.22
  275.8 1.7 fusion.26
  277.5 17.8 %while.30 = (s32[]{:T(128)}, f32[8,64,64]{1,2,0:T(8,128)S(1)}, f32[8,64,64]{1,2,0:T(8,128)S(1)}, f32[3,8,64,64]{2,3,1,0:T(8,128)}, f32[3,8,64,64]{3,2,1,0:T(8,12...) while((s32[]{:T(128)}, f32[8,64,64]{1,2,0:T(8,128)S(1)}, ...), condition=%wide.region_6.7_spmd.clone, body=%wide.region_5.6_spmd.clone.sunk | while | flops 50429952 | bytes 3541100 | solution.py:194
  277.6 1.0 constant_dynamic-slice_fusion.5
  278.7 1.6 fusion.164
  280.4 0.7 constant_dynamic-update-slice_fusion.10
  281.2 0.7 bitcast_dynamic-update-slice_fusion.2
  281.9 1.5 convolution_bitcast_fusion.10
  283.5 1.0 constant_dynamic-slice_fusion.5
  284.7 1.6 fusion.164
  286.4 0.7 constant_dynamic-update-slice_fusion.10
  287.1 0.7 bitcast_dynamic-update-slice_fusion.2
  287.8 1.5 convolution_bitcast_fusion.10
  289.5 1.0 constant_dynamic-slice_fusion.5
  290.6 1.6 fusion.164
  292.3 0.7 constant_dynamic-update-slice_fusion.10
  293.0 0.8 bitcast_dynamic-update-slice_fusion.2
  293.8 1.5 convolution_bitcast_fusion.10
  295.6 2.1 reshape.178
  297.7 16.0 %all-gather = bf16[32,64,64]{2,1,0:T(8,128)(2,1)S(1)} all-gather(bf16[8,64,64]{2,1,0:T(8,128)(2,1)S(1)} %copy.105), channel_id=2, replica_groups=mesh['sp'=4,'fs'=4,'tp'=2] {'sp'}, dimensions={0}, use_global_device_ids=true | all-gather | bytes 327680 | tf_op jit(solution)/shard_map/all_gather | solution.py:20
  313.7 15.8 %all-gather.1 = bf16[32,64,64]{2,1,0:T(8,128)(2,1)} all-gather(bf16[8,64,64]{2,1,0:T(8,128)(2,1)S(1)} %copy.106), channel_id=3, replica_groups=mesh['sp'=4,'fs'=4,'tp'=2] {'sp'}, dimensions={0}, use_global_device_ids=true | all-gather | bytes 327680 | tf_op jit(solution)/shard_map/all_gather | solution.py:20
  329.8 1.6 fusion.32
  331.4 1.9 convolution_multiply_fusion.3
  333.4 1.5 fusion.51
  334.9 1.9 fusion.24
  336.8 1.8 convolution_multiply_fusion
  338.7 0.8 convolution_add_fusion.3
  339.5 1.2 convolution_add_fusion.2
  340.7 1.4 fusion.127
  343.8 1.1 fusion.72
  344.9 0.7 maximum_convert_fusion
  346.5 5.3 %all_gather.31 = bf16[192,512]{1,0:T(8,128)(2,1)S(1)} all-gather(bf16[192,256]{1,0:T(8,128)(2,1)S(1)} %fusion.82), channel_id=1, replica_groups=mesh['sp'=4,'fs'=4,'tp'=2] {'tp'}, dimensions={1}, use_global_device_ids=true | all-gather | bytes 294912 | tf_op jit(solution)/shard_map/all_gather | solution.py:150
  352.0 1.2 fusion.33
  353.3 8.5 %all_to_all.19 = bf16[2,96,768]{2,1,0:T(8,128)(2,1)S(1)} all-to-all(bf16[2,96,768]{2,1,0:T(8,128)(2,1)S(1)} %bitcast.225), channel_id=1, replica_groups=mesh['sp'=4,'fs'=4,'tp'=2] {'tp'}, dimensions={0} | all-to-all | bytes 589824 | tf_op jit(solution)/shard_map/all_to_all | solution.py:215
  361.8 4.7 %fusion.18 = bf16[1,96,2048]{2,1,0:T(8,128)(2,1)} fusion(bf16[96,1536]{1,0:T(8,128)(2,1)S(1)} %bitcast.227, bf16[1536,2048]{1,0:T(8,128)(2,1)} %all-gather.8.cloned.1.call-done), kind=kOutput, calls=%fused_computation.29 | convolution fusion | flops 604176384 | bytes 6979584 | tf_op jit(solution)/shard_map/dot_general | solution.py:226
  (195 shorter events, 9.1 us)
Async XLA Ops:
  6.5 345.5 %copy-start = (bf16[512,512]{1,0:T(8,128)(2,1)S(1)}, bf16[512,512]{1,0:T(8,128)(2,1)}, u32[]{:S(2)}) copy-start(bf16[512,512]{1,0:T(8,128)(2,1)} %param.38) | copy-start | bytes 1572868
  6.5 8.3 %copy-start.24 = (bf16[256,128]{1,0:T(8,128)(2,1)S(1)}, bf16[256,128]{1,0:T(8,128)(2,1)}, u32[]{:S(2)}) copy-start(bf16[256,128]{1,0:T(8,128)(2,1)} %param.42) | copy-start | bytes 196612
  6.5 14.2 %copy-start.20 = (bf16[512,128]{1,0:T(8,128)(2,1)S(1)}, bf16[512,128]{1,0:T(8,128)(2,1)}, u32[]{:S(2)}) copy-start(bf16[512,128]{1,0:T(8,128)(2,1)} %param.43) | copy-start | bytes 393220
  6.5 118.0 %all-gather.6.cloned.1.call-start = ((), (), s32[]{:S(2)}) async-start(), calls=%async_computation.1 | async-start | bytes 14483456 | tf_op jit(solution)/shard_map/all_gather | solution.py:129
  11.9 15.3 %copy-start.25 = (f32[31,256]{1,0:T(8,128)S(1)}, f32[31,256]{1,0:T(8,128)}, u32[]{:S(2)}) copy-start(f32[31,256]{1,0:T(8,128)} %param.36) | copy-start | bytes 95236
  12.8 16.3 %copy-start.9 = (bf16[1,192,2048]{2,1,0:T(8,128)(2,1)S(1)}, bf16[1,192,2048]{2,1,0:T(8,128)(2,1)}, u32[]{:S(2)}) copy-start(bf16[1,192,2048]{2,1,0:T(8,128)(2,1)} %param.24) | copy-start | bytes 2359300
  14.8 14.7 %copy-start.63 = (f32[256]{0:T(256)S(1)}, f32[256]{0:T(256)}, u32[]{:S(2)}) copy-start(f32[256]{0:T(256)} %param.37) | copy-start | bytes 3076
  14.8 19.6 %copy-start.59 = (f32[512]{0:T(512)S(1)}, f32[512]{0:T(512)}, u32[]{:S(2)}) copy-start(f32[512]{0:T(512)} %param.40) | copy-start | bytes 6148
  14.8 109.7 %copy-start.62 = (f32[2048]{0:T(1024)S(1)}, f32[2048]{0:T(1024)}, u32[]{:S(2)}) copy-start(f32[2048]{0:T(1024)} %param.27) | copy-start | bytes 24580
  14.8 347.0 %all-gather.8.cloned.1.call-start = ((), (), s32[]{:S(2)}) async-start(), calls=%async_computation.2 | async-start | bytes 6684672 | tf_op jit(solution)/shard_map/all_gather | solution.py:228
  34.4 108.8 %copy-start.13 = (f32[64,64]{1,0:T(8,128)}, f32[64,64]{1,0:T(8,128)S(1)}, u32[]{:S(2)}) copy-start(f32[64,64]{1,0:T(8,128)S(1)} %get-tuple-element.207) | copy-start | bytes 49156
  34.5 108.7 %copy-start.21 = (f32[8,64]{1,0:T(8,128)}, f32[8,64]{1,0:T(8,128)S(1)}, u32[]{:S(2)}) copy-start(f32[8,64]{1,0:T(8,128)S(1)} %mul.623) | copy-start | bytes 6148
  132.3 4.5 %copy-start.7 = (bf16[192,3328]{1,0:T(8,128)(2,1)}, bf16[192,3328]{1,0:T(8,128)(2,1)S(1)}, u32[]{:S(2)}) copy-start(bf16[192,3328]{1,0:T(8,128)(2,1)S(1)} %convolution_convert_fusion) | copy-start | bytes 3833860
  132.3 4.3 %copy-start.57 = (f32[512]{0:T(512)S(1)}, f32[512]{0:T(512)}, u32[]{:S(2)}) copy-start(f32[512]{0:T(512)} %param.39) | copy-start | bytes 6148
  132.4 4.3 %copy-start.61 = (f32[1,192]{1,0:T(1,128)S(1)}, f32[1,192]{1,0:T(1,128)}, u32[]{:S(2)}) copy-start(f32[1,192]{1,0:T(1,128)} %param.25) | copy-start | bytes 2308
  132.4 4.6 %copy-start.15 = (bf16[192,256]{1,0:T(8,128)(2,1)}, bf16[192,256]{1,0:T(8,128)(2,1)S(1)}, u32[]{:S(2)}) copy-start(bf16[192,256]{1,0:T(8,128)(2,1)S(1)} %multiply_convert_fusion) | copy-start | bytes 294916
  133.9 211.0 %collective-permute-start = (bf16[30,256]{1,0:T(8,128)(2,1)}, bf16[30,256]{1,0:T(8,128)(2,1)}, u32[]{:S(2)}, u32[]{:S(2)}) collective-permute-start(bf16[30,256]{1,0:T(8,128)(2,1)} %slice.304), channel_id=1, source_target_pairs={{0,8},{8,16},{16,24},{1,9},{9,17},{17,25},{2,10},{10,18},{18,26},{... | collective-permute-start | bytes 46088 | tf_op jit(solution)/shard_map/ppermute | solution.py:14
  266.3 9.5 %copy-start.5 = (bf16[3,64,8,64]{3,2,1,0:T(8,128)(2,1)}, bf16[3,64,8,64]{3,2,1,0:T(8,128)(2,1)S(1)}, u32[]{:S(2)}) copy-start(bf16[3,64,8,64]{3,2,1,0:T(8,128)(2,1)S(1)} %reshape.169) | copy-start | bytes 589828
  266.3 3.2 copy-start.12
  269.5 1.6 copy-start.22
  271.2 1.8 copy-start.1
  271.2 1.8 copy-start.14
  275.8 1.8 copy-start.18
  295.4 34.1 %copy-start.19 = (f32[64,64]{0,1:T(8,128)S(1)}, f32[64,64]{0,1:T(8,128)}, u32[]{:S(2)}) copy-start(f32[64,64]{0,1:T(8,128)} %copy.96) | copy-start | bytes 49156
  329.5 1.9 copy-start.17
  329.5 1.9 copy-start.23
  329.8 1.6 copy-start.3
  331.4 1.9 copy-start.2
  333.4 1.5 copy-start.10
  333.4 1.5 copy-start.11
  336.8 1.9 copy-start.6
  343.3 1.7 copy-start.16
  343.3 2.4 copy-start.26
  343.3 2.4 copy-start.27
  343.3 2.4 copy-start.28
  343.3 2.4 copy-start.29
  343.4 2.4 copy-start.30
  343.4 2.4 copy-start.31
  343.4 2.4 copy-start.32
  343.4 2.4 copy-start.33
  343.4 2.4 copy-start.34
  343.4 2.4 copy-start.35
  343.4 2.4 copy-start.36
  343.4 2.4 copy-start.37
  343.4 2.4 copy-start.38
  343.4 2.4 copy-start.39
  343.5 2.4 copy-start.40
  343.5 2.4 copy-start.41
  343.5 2.4 copy-start.42
  343.5 2.4 copy-start.43
  343.5 2.4 copy-start.44
  343.5 2.4 copy-start.45
  343.5 2.4 copy-start.46
  343.5 2.4 copy-start.47
  343.5 2.4 copy-start.48
  343.5 2.4 copy-start.49
  343.6 2.4 copy-start.50
  343.6 2.4 copy-start.51
  343.6 2.4 copy-start.52
  343.6 2.4 copy-start.53
  343.6 2.4 copy-start.54
  343.6 2.4 copy-start.55
  343.6 2.4 copy-start.56
  346.0 6.0 %copy-start.60 = (f32[2,1,256]{2,1,0:T(1,128)S(1)}, f32[2,1,256]{2,1,0:T(1,128)}, u32[]{:S(2)}) copy-start(f32[2,1,256]{2,1,0:T(1,128)} %convert_element_type.135) | copy-start | bytes 6148
  (3 other events, 2.7 us)
Sparse Core Ops, SparseCore 0:
  14.9 109.5 all-gather.5
  126.7 65.0 all-gather.7
where the time goes:
time: 377 us; the launch traced here: 373 us
  other arithmetic  128 us (34%)
  waiting for transfers between devices  89.4 us (24%)
  blocking collectives  61.3 us (16%)
  matrix products  49.8 us (13%)
  local copies, waits for them, and re-layouts  27.3 us (7%)
  between operations  14.7 us (4%)
    another operation x3, other arithmetic, block_terms(): jax.scipy.linalg.solve_triangular(system, right_side, lower=True, unit_di...  119 us
    all_gather x1, waiting for transfers between devices, body(): lax.all_gather(stacked, ('sp', 'fs'), axis=0, tiled=True)  89.4 us
    all_gather x2, blocking collectives, entering_2(): lax.all_gather(a.astype(kind), axis)  31.8 us
    dot_general x4, matrix products, pair_terms(): jnp.einsum('hbtc,hbic->hbti', left, right, precision=lax.Precision.HIGHEST)  8.86 us
    all_to_all x1, blocking collectives, body(): lax.all_to_all(local_mix, 'tp', split_axis=0, concat_axis=1, tiled=True)  8.49 us
    unnamed x136, local copies, waits for them, and re-layouts  7.9 us
    dot_general x1, matrix products, body(): jnp.dot(normed, lax.all_gather(stacked, ('sp', 'fs'), axis=0, tiled=True)...  7.79 us
  transfers between devices with their start and end apart: 3, of which 1 were waited for; matrix products, arithmetic and copies ran while one was open for 51% of the time, Pallas kernels for 0%

commit v1 on v0

--- a/solution.py
+++ b/solution.py
@@ -1,11 +1,504 @@
+import functools
+
 import jax
 import jax.numpy as jnp
 from jax import lax
+from jax.experimental import pallas as pl
+from jax.experimental.pallas import tpu as pltpu
 from jax.sharding import PartitionSpec as P
 
 NORM_FLOOR = 0.1
 CHANNEL_FLOOR = 0.1
 GROUP_FLOOR = 1.0
+LANES = 128
+SPAN = 64
+BF = jnp.bfloat16
+F32 = jnp.float32
+ANY = pl.BlockSpec(memory_space=pl.ANY)
+VM = pl.BlockSpec(memory_space=pltpu.VMEM)
+SM = pl.BlockSpec(memory_space=pltpu.SMEM)
+
+
+def dot_nn(a, b):
+    return lax.dot_general(a, b, (((1,), (0,)), ((), ())), preferred_element_type=F32)
+
+
+def dot_nt(a, b):
+    return lax.dot_general(a, b, (((1,), (1,)), ((), ())), preferred_element_type=F32)
+
+
+def dot_tn(a, b):
+    return lax.dot_general(a, b, (((0,), (0,)), ((), ())), preferred_element_type=F32)
+
+
+def sigmoid(x):
+    return 1.0 / (1.0 + jnp.exp(-x))
+
+
+def iota(shape, dim):
+    return lax.broadcasted_iota(jnp.int32, shape, dim)
+
+
+def split_weights_kernel(place, *refs):
+    convs, states, outs = refs[:3], refs[3:8], refs[8:]
+    count = len(outs)
+    half = LANES // 2
+    for step, out in enumerate(outs):
+        target = lax.rem(place[0] + step, count)
+        for at, ref in enumerate(states):
+            out[:, at * LANES : (at + 1) * LANES] = ref[
+                :, pl.ds(pl.multiple_of(target * LANES, LANES), LANES)
+            ]
+        odd = lax.rem(target, 2) == 1
+        for at, ref in enumerate(convs):
+            pair = ref[:, pl.ds(pl.multiple_of((target // 2) * LANES, LANES), LANES)]
+            start = len(states) * LANES + at * half
+            out[:, start : start + half] = jnp.where(odd, pair[:, half:], pair[:, :half])
+
+
+def norm_kernel(place, tokens, gain, out_conv, out_state, normed, part, rows_out):
+    count = part.shape[0]
+    floats = tokens[...].astype(F32)
+    inverse = lax.rsqrt(jnp.mean(floats * floats, axis=1, keepdims=True) + NORM_FLOOR)
+    normed[...] = (floats * inverse * gain[...]).astype(BF)
+    part[...] = normed[pl.ds(pl.multiple_of(place[0] * count, 16), count), :]
+    split = out_conv.shape[0]
+    rows_out[:split, :] = out_conv[...]
+    rows_out[split:, :] = out_state[...]
+
+
+def assemble_kernel(*refs):
+    *sources, out, sem = refs
+    copies = [pltpu.make_async_copy(s, out.at[i], sem.at[i]) for i, s in enumerate(sources)]
+    for copy in copies:
+        copy.start()
+    for copy in copies:
+        copy.wait()
+
+
+def assemble(*arrays):
+    return pl.pallas_call(
+        assemble_kernel,
+        out_shape=jax.ShapeDtypeStruct((len(arrays),) + arrays[0].shape, arrays[0].dtype),
+        in_specs=[ANY] * len(arrays),
+        out_specs=ANY,
+        scratch_shapes=[pltpu.SemaphoreType.DMA((len(arrays),))],
+        name="assemble",
+    )(*arrays)
+
+
+def mixer_kernel(
+    place, pace, own, *refs, length, halves, blocks_order
+):
+    near = refs[: len(blocks_order)]
+    far = refs[len(blocks_order) : 2 * len(blocks_order)]
+    (
+        mine, sibling, start, base, correction, group_gain, taps, out,
+        x, w, proj, log_keep, conv_rows, y, sems,
+    ) = refs[2 * len(blocks_order) :]
+    z, f, t = place[0], place[1], place[2]
+    total_rows = x.shape[0]
+    count = total_rows // length
+    part = length // halves
+    jobs = []
+    slot = 0
+    for i in range(mine.shape[0]):
+        level, step = i // count, i % count
+        source = lax.rem(z - step + count, count)
+        for ref, flip in ((mine, 0), (sibling, 1)):
+            row = (source * count + (f ^ (2 * level) ^ flip)) * LANES
+            jobs.append(
+                (None, pltpu.make_async_copy(
+                    ref.at[i], w.at[pl.ds(pl.multiple_of(row, LANES), LANES), :], sems.at[slot]
+                ))
+            )
+            slot += 1
+    jobs.append(
+        (None, pltpu.make_async_copy(
+            own, x.at[pl.ds(pl.multiple_of(z * length, 64), length), :], sems.at[slot]
+        ))
+    )
+    slot += 1
+    for (offset, valid), a, b in zip(blocks_order, near, far):
+        position = offset(z)
+        for ref, half in ((a, t), (b, 1 - t)):
+            row = pl.multiple_of(position * length + half * part, 32)
+            jobs.append(
+                (valid(z), pltpu.make_async_copy(ref, x.at[pl.ds(row, part), :], sems.at[slot]))
+            )
+            slot += 1
+    for condition, copy in jobs:
+        if condition is None:
+            copy.start()
+        else:
+            pl.when(condition)(copy.start)
+    for condition, copy in jobs:
+        if condition is None:
+            copy.wait()
+        else:
+            pl.when(condition)(copy.wait)
+
+    half = LANES // 2
+    lane = iota((1, LANES), 1)
+    first = (lane < half).astype(F32)
+    second = 1.0 - first
+    ri, ci = iota((LANES, LANES), 0), iota((LANES, LANES), 1)
+    same = (ri // half) == (ci // half)
+    mean_mat = jnp.where(same, 1.0 / half, 0.0).astype(BF)
+    sum_mat = jnp.where(same, 1.0, 0.0).astype(BF)
+    strict = same & (ri > ci)
+    weak = same & (ri >= ci)
+    eye = jnp.where(ri == ci, 1.0, 0.0).astype(F32)
+
+    run = length // 4
+    column = pl.ds(pl.multiple_of(z * LANES, LANES), LANES)
+    base_row = base[:, column]
+    for block in range(count):
+        rows = slice(block * length, (block + 1) * length)
+        proj[rows, :] = dot_nn(x[rows, :], w[...]).astype(BF)
+        decay_in = proj[rows, 3 * LANES : 4 * LANES].astype(F32)
+        rate = -jnp.exp(base_row + jnp.tanh(decay_in))
+        for r in range(4):
+            log_keep[block * length + r * run : block * length + (r + 1) * run, :] = (
+                rate[r * run : (r + 1) * run, :] * pace[block * 4 + r]
+            )
+
+    left = 5 * LANES
+    pair = proj[:, left : left + LANES].astype(F32)
+    conv_in = (pair * pltpu.roll(sigmoid(pair), half, 1)).astype(BF).astype(F32)
+    middle = total_rows // 2
+    pad = conv_rows.shape[0] - middle
+    moved = pltpu.roll(conv_in[middle - pad :, :], half, 1)
+    conv_rows[:pad, :] = moved[:pad, :] * second
+    conv_rows[pad:, :] = conv_in[:middle, :] * first + moved[pad:, :] * second
+    kernel = taps.shape[0]
+    tap = taps[:, pl.ds(pl.multiple_of((z // 2) * LANES, LANES), LANES)]
+    turned = pltpu.roll(tap, half, 1)
+    odd = (lax.rem(z, 2) == 1).astype(F32)
+    tap = jnp.where((lane < half) == (odd < 0.5), tap, turned)
+    lead = pad - (kernel - 1)
+    strip = 96
+    for at in range(0, middle, strip):
+        total = jnp.zeros((strip, LANES), F32)
+        for j in range(kernel):
+            total = total + tap[j : j + 1, :] * conv_rows[at + lead + j : at + lead + j + strip, :]
+        total = total.astype(BF)
+        out[at : at + strip, LANES : LANES + half] = total[:, :half]
+        out[middle + at : middle + at + strip, LANES : LANES + half] = total[:, half:]
+    out[:, LANES + half : 2 * LANES] = proj[:, left + LANES : left + LANES + half]
+
+    chunks = total_rows // SPAN
+    corr_row = correction[:, column]
+    tri = jnp.where(iota((SPAN, SPAN), 0) >= iota((SPAN, SPAN), 1), 1.0, 0.0).astype(F32)
+
+    def stack(a):
+        return jnp.concatenate([a * first, a * second], axis=0).astype(BF)
+
+    sums = lax.dot_general(
+        tri,
+        jnp.concatenate([log_keep[c * SPAN : (c + 1) * SPAN, :] for c in range(chunks)], axis=1),
+        (((1,), (0,)), ((), ())),
+        precision=lax.Precision.HIGHEST,
+        preferred_element_type=F32,
+    )
+    levels = []
+    size = 1
+    while size < SPAN:
+        inside = (ri // (2 * size)) == (ci // (2 * size))
+        levels.append(inside & ((ri & size) != 0) & ((ci & size) == 0))
+        size *= 2
+
+    group = 6
+    carried = []
+    for at in range(0, chunks, group):
+        members = list(range(at, min(at + group, chunks)))
+        grams, tails, heads = [], [], []
+        for c in members:
+            rows = slice(c * SPAN, (c + 1) * SPAN)
+            total = sums[:, c * LANES : (c + 1) * LANES]
+            before = total - log_keep[rows, :]
+            last = total[SPAN - 1 : SPAN, :]
+            q = proj[rows, 0:LANES].astype(F32)
+            k = proj[rows, LANES : 2 * LANES].astype(F32)
+            v = proj[rows, 2 * LANES : 3 * LANES].astype(F32)
+            norm = dot_nn((k * k).astype(BF), sum_mat)
+            unit = k * lax.rsqrt(jnp.maximum(norm, 1.0))
+            write = unit * corr_row
+            back = jnp.exp(-total)
+            rest = jnp.exp(last - total)
+            lead_remove = stack(-unit * jnp.exp(before))
+            lead_query = stack(q * jnp.exp(total))
+            grams.append(
+                dot_nt(
+                    jnp.concatenate([lead_remove, lead_query], axis=0),
+                    jnp.concatenate([stack(write * back), stack(k * back)], axis=0),
+                )
+            )
+            tails.append((stack(write * rest), stack(k * rest), jnp.exp(last)))
+            heads.append((lead_remove, lead_query, stack(v)))
+        system = [jnp.where(strict, g[:LANES, :LANES], 0.0) for g in grams]
+        inverse = [eye + jnp.where(levels[0], a, 0.0) for a in system]
+        for level in levels[1:]:
+            low = [i.astype(BF) for i in inverse]
+            inner = [
+                dot_nn(i, jnp.where(level, a, 0.0).astype(BF)).astype(BF) for i, a in zip(low, system)
+            ]
+            inverse = [i + dot_nn(n, b) for i, n, b in zip(inverse, inner, low)]
+        direct = [
+            dot_nn(
+                jnp.concatenate(
+                    [
+                        jnp.where(strict, g[:LANES, LANES:], 0.0),
+                        jnp.where(weak, g[LANES:, LANES:], 0.0),
+                    ],
+                    axis=0,
+                ).astype(BF),
+                h[2],
+            )
+            for g, h in zip(grams, heads)
+        ]
+        solved = [
+            dot_nn(i.astype(BF), jnp.concatenate([d[:LANES].astype(BF), h[0]], axis=1)).astype(BF)
+            for i, d, h in zip(inverse, direct, heads)
+        ]
+        through = [
+            dot_nn(jnp.where(weak, g[LANES:, :LANES], 0.0).astype(BF), s) for g, s in zip(grams, solved)
+        ]
+        for g, d, s, h, u, tail in zip(grams, direct, solved, heads, through, tails):
+            local = u[:, :LANES] + d[LANES:]
+            moved = dot_tn(s, tail[0])
+            carried.append(
+                (
+                    local[:SPAN] + local[SPAN:],
+                    (h[1].astype(F32) + u[:, LANES:]).astype(BF),
+                    moved[LANES:].astype(BF),
+                    moved[:LANES] + dot_tn(h[2], tail[1]),
+                    tail[2],
+                )
+            )
+    zero = jnp.zeros((half, half), F32)
+    state = jnp.concatenate(
+        [
+            jnp.concatenate([start[2 * z], zero], axis=1),
+            jnp.concatenate([zero, start[2 * z + 1]], axis=1),
+        ],
+        axis=0,
+    )
+    for c, (local, lead, step, added, kept) in enumerate(carried):
+        low = state.astype(BF)
+        seen = dot_nt(lead, low)
+        y[c * SPAN : (c + 1) * SPAN, :] = local + seen[:SPAN] + seen[SPAN:]
+        state = state * kept + dot_nn(low, step) + added
+
+    gain_row = group_gain[:, column]
+    for block in range(count):
+        rows = slice(block * length, (block + 1) * length)
+        values = y[rows, :]
+        high = values.astype(BF)
+        low = (values - high.astype(F32)).astype(BF)
+        centered = values - (dot_nn(high, mean_mat) + dot_nn(low, mean_mat))
+        variance = dot_nn((centered * centered).astype(BF), mean_mat)
+        gate = proj[rows, 4 * LANES : 5 * LANES].astype(F32)
+        grouped = centered * lax.rsqrt(variance + GROUP_FLOOR) * gain_row
+        out[rows, :LANES] = (grouped * (gate * sigmoid(gate))).astype(BF)
+
+
+def output_kernel(place, received, gain, point, *refs, groups):
+    pieces, (out, w, sems) = refs[:-3], refs[-3:]
+    z, f, t = place[0], place[1], place[2]
+    sources, rows, _ = received.shape
+    count = sources // groups
+    half = LANES // 2
+    split = count * half
+    wide = count * LANES
+    jobs = []
+    slot = 0
+    for at, piece in enumerate(pieces):
+        core, flip, side = at & 1, (at >> 1) & 1, (at >> 2) & 1
+        group = t ^ side
+        for block in range(count):
+            col = pl.multiple_of((block * count + (f ^ (2 * flip) ^ core)) * LANES, LANES)
+            for start, size, shift in (
+                (0, split, group * split),
+                (split, wide, groups * split + group * wide),
+            ):
+                copy = pltpu.make_async_copy(
+                    piece.at[block, pl.ds(start, size), :],
+                    w.at[pl.ds(pl.multiple_of(shift, LANES), size), pl.ds(col, LANES)],
+                    sems.at[slot],
+                )
+                copy.start()
+                jobs.append(copy)
+                slot += 1
+    sums, gates, states = [], [], []
+    for group in range(groups):
+        for block in range(count):
+            source = received[block * groups + group]
+            states.append(source[:, :LANES])
+            sums.append(source[:, LANES : LANES + half])
+            gates.append(source[:, LANES + half :])
+    conv_sum = jnp.concatenate(sums, axis=1).astype(F32)
+    gate = jnp.concatenate(gates, axis=1).astype(F32)
+    mean = jnp.mean(conv_sum, axis=1, keepdims=True)
+    spread = jnp.mean(conv_sum * conv_sum, axis=1, keepdims=True) - mean * mean
+    scaled = (conv_sum - mean) * lax.rsqrt(spread + CHANNEL_FLOOR) * gain[...]
+    shaped = (scaled * sigmoid(scaled)).astype(BF)
+    conv_out = (dot_nn(shaped, point[...]) * (gate * sigmoid(gate))).astype(BF)
+    joined = jnp.concatenate([conv_out] + states, axis=1)
+    for copy in jobs:
+        copy.wait()
+    out[...] = dot_nn(joined, w[...]).astype(BF)
+
+
+def ordered_kernel(place, *refs, blocks_order):
+    *sources, out, sems = refs
+    z = place[0]
+    jobs = [(None, pltpu.make_async_copy(sources[0], out.at[z], sems.at[0]))]
+    for i, ((offset, valid), source) in enumerate(zip(blocks_order, sources[1:])):
+        jobs.append(
+            (valid(z), pltpu.make_async_copy(source, out.at[offset(z)], sems.at[i + 1]))
+        )
+    for condition, copy in jobs:
+        if condition is None:
+            copy.start()
+        else:
+            pl.when(condition)(copy.start)
+    for condition, copy in jobs:
+        if condition is None:
+            copy.wait()
+        else:
+            pl.when(condition)(copy.wait)
+
+
+LINE = (
+    ((0, 1), (1, 2), (2, 3)),
+    ((1, 0), (2, 1), (3, 2)),
+    ((0, 2), (1, 3), (2, 0), (3, 1)),
+    ((2, 3), (1, 0)),
+)
+LINE_ORDER = (
+    (lambda z: jnp.maximum(z - 1, 0), lambda z: z > 0),
+    (lambda z: jnp.minimum(z + 1, 3), lambda z: z < 3),
+    (lambda z: z ^ 2, lambda z: z >= 0),
+    (lambda z: z ^ 3, lambda z: (z == 0) | (z == 3)),
+)
+
+
+def along_line(value):
+    right, left, double = (lax.ppermute(value, "sp", LINE[i]) for i in range(3))
+    return right, left, double, lax.ppermute(double, "sp", LINE[3])
+
+
+def across(value, pairs):
+    targets = sorted({b for _, b in pairs})
+    return lax.ppermute(
+        value, ("sp", "tp"), [(2 * i + s, 2 * i + 1 - s) for i in targets for s in (0, 1)]
+    )
+
+
+def flipped(value, axis, bit):
+    count = lax.axis_size(axis)
+    return lax.ppermute(value, axis, [(i, i ^ bit) for i in range(count)])
+
+
+def head_body(
+    tokens, decay_pace, start_state, norm_gain, conv_value, conv_admit, conv_gate, state_query,
+    state_key, state_value, state_decay, state_gate, conv_taps, conv_gain, point_weight, decay_base,
+    correction, group_gain, output_conv, output_state,
+):
+    width = tokens.shape[-1]
+    length = tokens.shape[1]
+    count, halves = lax.axis_size("sp"), lax.axis_size("tp")
+    part = length // halves
+    place = jnp.stack([lax.axis_index(a) for a in ("sp", "fs", "tp")]).astype(jnp.int32)
+    shard = conv_value.shape[0]
+    columns = 5 * LANES + 3 * LANES // 2
+    slices = pl.pallas_call(
+        split_weights_kernel,
+        out_shape=[jax.ShapeDtypeStruct((shard, columns), BF)] * count,
+        in_specs=[SM] + [VM] * 8,
+        out_specs=[VM] * count,
+        name="split_weights",
+    )(place, conv_value, conv_admit, conv_gate, state_query, state_key, state_value, state_decay, state_gate)
+    taken = [slices[0]] + [
+        lax.ppermute(slices[k], "sp", [(s, (s + k) % count) for s in range(count)])
+        for k in range(1, count)
+    ]
+    out_rows = output_conv.shape[0] + output_state.shape[0]
+    normed, half, rows_out = pl.pallas_call(
+        norm_kernel,
+        out_shape=[
+            jax.ShapeDtypeStruct((length, width), BF),
+            jax.ShapeDtypeStruct((part, width), BF),
+            jax.ShapeDtypeStruct((out_rows, output_conv.shape[1]), BF),
+        ],
+        in_specs=[SM, VM, VM, VM, VM],
+        out_specs=[VM] * 3,
+        name="norm",
+    )(place[2:], tokens.reshape(length, width), norm_gain.reshape(1, width), output_conv, output_state)
+    near = along_line(half)
+    far = [across(a, LINE[i]) for i, a in enumerate(near)]
+    lifted = [flipped(a, "fs", 2) for a in taken]
+    mine = assemble(*taken, *lifted)
+    sibling = flipped(mine, "fs", 1)
+    paces = lax.all_gather(decay_pace[0, :: length // 4], "sp", axis=0, tiled=True)
+    gain_other = flipped(conv_gain, "tp", 1)
+    low = lax.axis_index("tp") == 0
+    gain = jnp.concatenate(
+        [jnp.where(low, conv_gain, gain_other), jnp.where(low, gain_other, conv_gain)]
+    )
+    line_out = along_line(rows_out)
+    ordered = pl.pallas_call(
+        functools.partial(ordered_kernel, blocks_order=LINE_ORDER),
+        out_shape=jax.ShapeDtypeStruct((count,) + rows_out.shape, BF),
+        in_specs=[SM] + [ANY] * 5,
+        out_specs=ANY,
+        scratch_shapes=[pltpu.SemaphoreType.DMA((5,))],
+        name="ordered",
+    )(place, rows_out, *line_out)
+    crossed = flipped(ordered, "tp", 1)
+    pieces = []
+    for a in (ordered, crossed):
+        for b in (a, flipped(a, "fs", 2)):
+            pieces += [b, flipped(b, "fs", 1)]
+    total = length * count
+    rows = total // (count * halves)
+    heads = start_state.shape[1]
+    mixed = pl.pallas_call(
+        functools.partial(mixer_kernel, length=length, halves=halves, blocks_order=LINE_ORDER),
+        out_shape=jax.ShapeDtypeStruct((total, 2 * LANES), BF),
+        in_specs=[SM, SM] + [ANY] * 11 + [VM] * 5,
+        out_specs=VM,
+        scratch_shapes=[
+            pltpu.VMEM((total, width), BF),
+            pltpu.VMEM((width, columns), BF),
+            pltpu.VMEM((total, columns), BF),
+            pltpu.VMEM((total, LANES), F32),
+            pltpu.VMEM((total // 2 + 32, LANES), F32),
+            pltpu.VMEM((total, LANES), F32),
+            pltpu.SemaphoreType.DMA((32,)),
+        ],
+        name="mixer",
+    )(
+        place, paces, normed, *near, *far, mine, sibling,
+        start_state.reshape(heads, *start_state.shape[2:]),
+        decay_base.reshape(1, -1), correction.reshape(1, -1), group_gain.reshape(1, -1), conv_taps,
+    )
+    received = lax.all_to_all(
+        mixed.reshape(count * halves, rows, 2 * LANES), ("sp", "tp"), 0, 0, tiled=True
+    )
+    out = pl.pallas_call(
+        functools.partial(output_kernel, groups=halves),
+        out_shape=jax.ShapeDtypeStruct((rows, width), BF),
+        in_specs=[SM, VM, VM, VM] + [ANY] * 8,
+        out_specs=VM,
+        scratch_shapes=[
+            pltpu.VMEM((halves * out_rows, width), BF),
+            pltpu.SemaphoreType.DMA((64,)),
+        ],
+        name="output",
+    )(place, received, gain.reshape(1, -1), point_weight, *pieces)
+    return out.reshape(1, rows, width)
 
 
 def passed_along(value, axis, steps):
@@ -231,9 +724,17 @@
     return mixed.astype(jnp.bfloat16).reshape(1, -1, width)
 
 
+def layer(*args):
+    sizes = [lax.axis_size(a) for a in ("sp", "fs", "tp")]
+    channels, wide = args[4].shape[1], args[7].shape[1]
+    whole = channels == sizes[0] * LANES // 2 and wide == sizes[0] * LANES
+    square = args[2].shape[-1] == LANES // 2 and args[4].shape[0] == LANES
+    return (head_body if sizes == [4, 4, 2] and whole and square else body)(*args)
+
+
 def solution(mesh):
     return jax.shard_map(
-        body,
+        layer,
         mesh=mesh,
         in_specs=(
             P("fs", "sp", None),

time: 377 us -> 252 us (0.67)
  other arithmetic: 128 us -> 1.25 us
  Pallas kernels: 0 us -> 111 us
  starting transfers between devices: 2.8 us -> 56.8 us
  matrix products: 49.8 us -> 0 us
  blocking collectives: 61.3 us -> 14 us
  waiting for transfers between devices: 89.4 us -> 58 us
  local copies, waits for them, and re-layouts: 27.3 us -> 9.08 us
  between operations: 14.7 us -> 1.11 us
    another operation x6 -> x1, other arithmetic: 120 us -> 0.66 us  [head_body(): jnp.stack([lax.axis_index(a) for a in ('sp', 'fs', 'tp')]).astype(jnp.int32)]
    pallas_call x0 -> x6, Pallas kernels: none -> 111 us  [the longest x1 56.8 us: assemble(): pl.pallas_call(assemble_kernel, out_shape=jax.ShapeDtypeStruct((len(array...]
    all_gather x2 -> x0, waiting for transfers between devices: 89.4 us -> none  [the longest x1 89.4 us: body(): lax.all_gather(stacked, ('sp', 'fs'), axis=0, tiled=True)]
    ppermute x1 -> x28, waiting for transfers between devices: 0.01 us -> 52.8 us  [the longest x6 22.6 us: along_line(): right, left, double = (lax.ppermute(value, 'sp', LINE[i]) for i in range(3))]
    ppermute x1 -> x28, starting transfers between devices: 2.76 us -> 53.3 us  [the longest x6 24.1 us: along_line(): right, left, double = (lax.ppermute(value, 'sp', LINE[i]) for i in range(3))]
    dot_general x23 -> x0, matrix products: 48.2 us -> none  [the longest x4 8.86 us: pair_terms(): jnp.einsum('hbtc,hbic->hbti', left, right, precision=lax.Precision.HIGHEST)]
    all_gather x6 -> x1, blocking collectives: 52.8 us -> 14 us  [head_body(): lax.all_gather(decay_pace[0, ::length // 4], 'sp', axis=0, tiled=True)]
    all_to_all x1 -> x0, blocking collectives: 8.49 us -> none  [body(): lax.all_to_all(local_mix, 'tp', split_axis=0, concat_axis=1, tiled=True)]
  transfers between devices with their start and end apart: 3 -> 29, of which waited for: 1 -> 9; matrix products, arithmetic and copies ran while one was open for 51% -> 3% of each run, Pallas kernels for 0% -> 40%
where the time goes in v1:
time: 252 us; the launch traced here: 251 us
  Pallas kernels  111 us (44%)
  waiting for transfers between devices  58 us (23%)
  starting transfers between devices  56.8 us (23%)
  blocking collectives  14 us (6%)
  local copies, waits for them, and re-layouts  9.08 us (4%)
    pallas_call x1, Pallas kernels, assemble(): pl.pallas_call(assemble_kernel, out_shape=jax.ShapeDtypeStruct((len(array...  56.8 us
    pallas_call x1, Pallas kernels, head_body(): pl.pallas_call(functools.partial(ordered_kernel, blocks_order=LINE_ORDER)...  25.6 us
    ppermute x6, starting transfers between devices, along_line(): right, left, double = (lax.ppermute(value, 'sp', LINE[i]) for i in range(3))  24.1 us
    ppermute x6, waiting for transfers between devices, along_line(): right, left, double = (lax.ppermute(value, 'sp', LINE[i]) for i in range(3))  22.6 us
    pallas_call x1, Pallas kernels, head_body(): pl.pallas_call(functools.partial(mixer_kernel, length=length, halves=halv...  16.5 us
    ppermute x13, waiting for transfers between devices, flipped(): return lax.ppermute(value, axis, [(i, i ^ bit) for i in range(count)])  14.3 us
    all_gather x1, blocking collectives, head_body(): lax.all_gather(decay_pace[0, ::length // 4], 'sp', axis=0, tiled=True)  14 us
    ppermute x13, starting transfers between devices, flipped(): return lax.ppermute(value, axis, [(i, i ^ bit) for i in range(count)])  12.5 us
  transfers between devices with their start and end apart: 29, of which 9 were waited for; matrix products, arithmetic and copies ran while one was open for 3% of the time, Pallas kernels for 40%

profile of v1, /device:TPU:0, one launch (start us, length us, event | category | flops | bytes accessed | tf_op | source)
XLA Modules:
  0.0 250.9 jit_solution(6175264205549011673)
XLA Ops:
  0.0 0.7 pad_add_fusion.place
  0.7 2.7 %split_weights.1 = (bf16[128,832]{1,0:T(8,128)(2,1)}, bf16[128,832]{1,0:T(8,128)(2,1)}, bf16[128,832]{1,0:T(8,128)(2,1)}, bf16[128,832]{1,0:T(8,128)(2,1)}) custom-call(s32[3]{0:T(128)} %pad_add_fusion.place, bf16[128,256]{1,0:T(8,128)(2,1)} %refs_0_.1, bf16[128,256]{1,0:T(8,128)(2,1)} %refs_1_.1, bf16[128,256]{1,0:T(8,128)(2,1)} %refs_2_.1, ...), custom_call_target="tpu_custom_call" | custom-call | tf_op jit(solution)/shard_map/split_weights/pallas_call | solution.py:416
  3.3 3.0 %collective-permute-start.8 = (bf16[128,832]{1,0:T(8,128)(2,1)}, bf16[128,832]{1,0:T(8,128)(2,1)S(1)}, u32[]{:S(2)}, u32[]{:S(2)}) collective-permute-start(bf16[128,832]{1,0:T(8,128)(2,1)} %get-tuple-element.15), channel_id=1, source_target_pairs={{0,8},{8,16},{16,24},{24,0},{1,9},{9,17},{17,25},{25,1},{2,10},{10... | collective-permute-start | bytes 638984 | tf_op jit(solution)/shard_map/ppermute | solution.py:424
  6.4 2.6 %collective-permute-start.9 = (bf16[128,832]{1,0:T(8,128)(2,1)}, bf16[128,832]{1,0:T(8,128)(2,1)S(1)}, u32[]{:S(2)}, u32[]{:S(2)}) collective-permute-start(bf16[128,832]{1,0:T(8,128)(2,1)} %get-tuple-element.16), channel_id=1, source_target_pairs={{0,16},{8,24},{16,0},{24,8},{1,17},{9,25},{17,1},{25,9},{2,18},{10... | collective-permute-start | bytes 638984 | tf_op jit(solution)/shard_map/ppermute | solution.py:424
  9.0 1.3 collective-permute-start.10
  10.3 1.5 collective-permute-start.11
  11.8 3.4 %collective-permute-done.8.refs_1_ = bf16[128,832]{1,0:T(8,128)(2,1)S(1)} collective-permute-done((bf16[128,832]{1,0:T(8,128)(2,1)}, bf16[128,832]{1,0:T(8,128)(2,1)S(1)}, u32[]{:S(2)}, u32[]{:S(2)}) %collective-permute-start.8) | collective-permute-done | bytes 213024 | tf_op jit(solution)/shard_map/ppermute | solution.py:424
  15.2 1.7 collective-permute-start.12
  17.0 2.6 %norm.1 = (bf16[192,2048]{1,0:T(8,128)(2,1)}, bf16[96,2048]{1,0:T(8,128)(2,1)}, bf16[768,128]{1,0:T(8,128)(2,1)}) custom-call(s32[1]{0:T(128)} %bitcast.2.place, bf16[192,2048]{1,0:T(8,128)(2,1)} %bitcast.16, f32[1,2048]{1,0:T(1,128)} %bitcast.18, bf16[256,128]{1,0:T(8,128)(2,1)} %out_conv.1, bf16[512,128]{1,0:T(8,128)(2,1)} %out_state.1), custom_call_target="tpu_custom_call" | custom-call | tf_op jit(solution)/shard_map/norm/pallas_call | solution.py:428
  19.5 12.6 %collective-permute-start.19 = (bf16[768,128]{1,0:T(8,128)(2,1)}, bf16[768,128]{1,0:T(8,128)(2,1)}, u32[]{:S(2)}, u32[]{:S(2)}) collective-permute-start(bf16[768,128]{1,0:T(8,128)(2,1)} %get-tuple-element.18.refs_0_), channel_id=1, source_target_pairs={{0,16},{8,24},{16,0},{24,8},{1,17},{9,25},{17,1},{25,9},{2,18},{10... | collective-permute-start | bytes 589832 | tf_op jit(solution)/shard_map/ppermute | solution.py:388
  32.1 0.5 collective-permute-start.13
  32.6 0.0 collective-permute-done.10.refs_3_
  32.6 1.5 collective-permute-start.14
  34.1 4.0 %collective-permute-done.19.refs_3_ = bf16[768,128]{1,0:T(8,128)(2,1)} collective-permute-done((bf16[768,128]{1,0:T(8,128)(2,1)}, bf16[768,128]{1,0:T(8,128)(2,1)}, u32[]{:S(2)}, u32[]{:S(2)}) %collective-permute-start.19) | collective-permute-done | bytes 196640 | tf_op jit(solution)/shard_map/ppermute | solution.py:388
  38.2 2.0 collective-permute-start.17
  40.2 0.0 collective-permute-done.11.refs_4_
  40.2 1.3 collective-permute-start.18
  41.5 1.3 collective-permute-start.20
  42.8 0.0 collective-permute-done.13.refs_6_
  42.8 0.0 collective-permute-done.14.refs_7_
  42.8 0.6 copy-done.11
  43.5 0.7 copy-done.12
  44.1 56.8 %assemble.1.refs_8_ = bf16[8,128,832]{2,1,0:T(8,128)(2,1)} custom-call(bf16[128,832]{1,0:T(8,128)(2,1)} %get-tuple-element.14.refs_0_, bf16[128,832]{1,0:T(8,128)(2,1)} %copy-done.6, bf16[128,832]{1,0:T(8,128)(2,1)} %copy-done.7, bf16[128,832]{1,0:T(8,128)(2,1)} %copy-done.8, bf16[128,832]{1,0:T(8,128)(2,1)} %copy-done.9, bf16[128,832]{1,0:T(8,128)(2,1)} %copy-done.10, ...), custom_call_target="tpu_custom_call" | custom-call | tf_op jit(solution)/shard_map/assemble/pallas_call | solution.py:80
  100.9 0.0 copy-start.14
  100.9 0.0 copy-start.15
  100.9 3.2 %copy.21 = bf16[8,128,832]{1,2,0:T(8,128)(2,1)S(1)} copy(bf16[8,128,832]{2,1,0:T(8,128)(2,1)} %assemble.1.refs_8_) | data formatting | bytes 3407872 | tf_op jit(solution)/shard_map/assemble/pallas_call | solution.py:80
  104.2 0.1 collective-permute-start.15
  104.3 0.0 collective-permute-done.18.refs_2_
  104.3 0.0 collective-permute-done.20.refs_4_
  104.3 25.6 %ordered.1.refs_0_ = bf16[4,768,128]{2,1,0:T(8,128)(2,1)} custom-call(s32[3]{0:T(128)} %pad_add_fusion.place, bf16[768,128]{1,0:T(8,128)(2,1)} %get-tuple-element.18.refs_0_, bf16[768,128]{1,0:T(8,128)(2,1)} %collective-permute-done.17.refs_1_, bf16[768,128]{1,0:T(8,128)(2,1)} %collective-permute-done.18.refs_2_, ...), custom_call_target="tpu_custom_call" | custom-call | tf_op jit(solution)/shard_map/ordered/pallas_call | solution.py:451
  129.9 1.6 collective-permute-start.24
  131.5 5.7 %collective-permute-start.2 = (bf16[96,2048]{1,0:T(8,128)(2,1)}, bf16[96,2048]{1,0:T(8,128)(2,1)S(1)}, u32[]{:S(2)}, u32[]{:S(2)}) collective-permute-start(bf16[96,2048]{1,0:T(8,128)(2,1)} %get-tuple-element.13), channel_id=1, source_target_pairs={{0,16},{8,24},{16,0},{24,8},{1,17},{9,25},{17,1},{25,9},{2,18},{10... | collective-permute-start | bytes 1179656 | tf_op jit(solution)/shard_map/ppermute | solution.py:388
  137.2 1.3 collective-permute-start
  138.5 1.3 collective-permute-start.1
  139.8 15.3 %collective-permute-done.2.refs_2_ = bf16[96,2048]{1,0:T(8,128)(2,1)S(1)} collective-permute-done((bf16[96,2048]{1,0:T(8,128)(2,1)}, bf16[96,2048]{1,0:T(8,128)(2,1)S(1)}, u32[]{:S(2)}, u32[]{:S(2)}) %collective-permute-start.2) | collective-permute-done | bytes 393248 | tf_op jit(solution)/shard_map/ppermute | solution.py:388
  155.1 1.3 collective-permute-start.3
  156.4 0.0 collective-permute-done.refs_0_
  156.4 0.6 collective-permute-start.6
  157.0 3.3 %collective-permute-done.1.refs_1_ = bf16[96,2048]{1,0:T(8,128)(2,1)} collective-permute-done((bf16[96,2048]{1,0:T(8,128)(2,1)}, bf16[96,2048]{1,0:T(8,128)(2,1)}, u32[]{:S(2)}, u32[]{:S(2)}) %collective-permute-start.1) | collective-permute-done | bytes 393248 | tf_op jit(solution)/shard_map/ppermute | solution.py:388
  160.3 2.6 %collective-permute-start.22 = (bf16[4,768,128]{2,1,0:T(8,128)(2,1)}, bf16[4,768,128]{2,1,0:T(8,128)(2,1)}, u32[]{:S(2)}, u32[]{:S(2)}) collective-permute-start(bf16[4,768,128]{2,1,0:T(8,128)(2,1)} %ordered.1.refs_0_), channel_id=1, source_target_pairs={{0,4},{2,6},{4,0},{6,2},{1,5},{3,7},{5,1},{7,3},{8,12},{10,14},{12... | collective-permute-start | bytes 2359304 | tf_op jit(solution)/shard_map/ppermute | solution.py:401
  162.9 0.0 collective-permute-done.24.refs_4_
  162.9 0.0 collective-permute-start.26
  163.0 5.5 %collective-permute-done.3.refs_3_ = bf16[96,2048]{1,0:T(8,128)(2,1)} collective-permute-done((bf16[96,2048]{1,0:T(8,128)(2,1)S(1)}, bf16[96,2048]{1,0:T(8,128)(2,1)}, u32[]{:S(2)}, u32[]{:S(2)}) %collective-permute-start.3) | collective-permute-done | bytes 393248 | tf_op jit(solution)/shard_map/ppermute | solution.py:389
  168.4 0.7 collective-permute-start.4
  169.1 2.4 collective-permute-start.5
  171.6 0.0 copy-start.5
  171.6 3.4 %collective-permute-start.7 = (bf16[96,2048]{1,0:T(8,128)(2,1)}, bf16[96,2048]{1,0:T(8,128)(2,1)}, u32[]{:S(2)}, u32[]{:S(2)}) collective-permute-start(bf16[96,2048]{1,0:T(8,128)(2,1)} %collective-permute-done.3.refs_3_), channel_id=1, source_target_pairs={{0,1},{1,0},{24,25},{25,24},{2,3},{3,2},{26,27},{27,26},{4,5},{5,4... | collective-permute-start | bytes 1179656 | tf_op jit(solution)/shard_map/ppermute | solution.py:394
  175.1 0.1 slice.3
  175.2 0.6 dynamic-slice
  176.3 7.0 %collective-permute-done.5.refs_5_ = bf16[96,2048]{1,0:T(8,128)(2,1)} collective-permute-done((bf16[96,2048]{1,0:T(8,128)(2,1)}, bf16[96,2048]{1,0:T(8,128)(2,1)}, u32[]{:S(2)}, u32[]{:S(2)}) %collective-permute-start.5) | collective-permute-done | bytes 393248 | tf_op jit(solution)/shard_map/ppermute | solution.py:394
  183.3 0.5 collective-permute-start.25
  183.9 12.0 %collective-permute-done.26.refs_6_ = bf16[4,768,128]{2,1,0:T(8,128)(2,1)} collective-permute-done((bf16[4,768,128]{2,1,0:T(8,128)(2,1)}, bf16[4,768,128]{2,1,0:T(8,128)(2,1)}, u32[]{:S(2)}, u32[]{:S(2)}) %collective-permute-start.26) | collective-permute-done | bytes 786464 | tf_op jit(solution)/shard_map/ppermute | solution.py:401
  195.8 0.5 collective-permute-start.27
  196.3 0.1 bitcast_dynamic-update-slice_fusion
  196.4 14.0 %all-reduce.pace = f32[16]{0:T(128)} all-reduce(f32[16]{0:T(128)S(1)} %bitcast_dynamic-update-slice_fusion), channel_id=2, replica_groups=mesh['sp'=4,'fs'=4,'tp'=2] {'sp'}, use_global_device_ids=true, to_apply=%add | all-reduce | flops 16 | bytes 128 | tf_op jit(solution)/shard_map/all_gather | solution.py:444
  210.4 3.0 %copy.22.refs_9_ = bf16[8,128,832]{2,1,0:T(8,128)(2,1)} copy(bf16[8,128,832]{1,2,0:T(8,128)(2,1)S(1)} %collective-permute-done.15) | data formatting | bytes 3407872 | tf_op jit(solution)/shard_map/ppermute | solution.py:401
  213.4 16.5 %mixer.1 = bf16[768,256]{1,0:T(8,128)(2,1)} custom-call(s32[3]{0:T(128)} %pad_add_fusion.place, f32[16]{0:T(128)} %all-reduce.pace, bf16[192,2048]{1,0:T(8,128)(2,1)} %get-tuple-element.12.own, bf16[96,2048]{1,0:T(8,128)(2,1)} %copy-done.3, bf16[96,2048]{1,0:T(8,128)(2,1)} %collective-permute-done.1.refs_1_, bf16[96,2048]{1,0:T(8,128)(2,1)} %copy-done.2, ...), custom_call_target="tpu_custom_call" | custom-call | tf_op jit(solution)/shard_map/mixer/pallas_call | solution.py:467
  230.0 3.5 %all-to-all-start = ((bf16[8,96,256]{2,1,0:T(8,128)(2,1)}), bf16[8,96,256]{2,1,0:T(8,128)(2,1)S(1)}, u32[]{:S(2)}, u32[]{:S(2)}) async-start(bf16[8,96,256]{2,1,0:T(8,128)(2,1)} %bitcast.15), calls=%async_computation | async-start | bytes 786432 | tf_op jit(solution)/shard_map/all_to_all | solution.py:487
  233.5 1.9 collective-permute-start.16
  235.4 2.3 collective-permute-done.16
  237.7 0.6 pad_maximum_fusion
  238.3 5.2 %all-to-all-done.received = bf16[8,96,256]{2,1,0:T(8,128)(2,1)S(1)} async-done(((bf16[8,96,256]{2,1,0:T(8,128)(2,1)}), bf16[8,96,256]{2,1,0:T(8,128)(2,1)S(1)}, u32[]{:S(2)}, u32[]{:S(2)}) %all-to-all-start) | async-done | bytes 393248 | tf_op jit(solution)/shard_map/all_to_all | solution.py:487
  243.5 0.7 copy-done
  244.2 6.5 %output.1 = bf16[96,2048]{1,0:T(8,128)(2,1)} custom-call(s32[3]{0:T(128)} %pad_add_fusion.place, bf16[8,96,256]{2,1,0:T(8,128)(2,1)} %copy-done, f32[1,512]{1,0:T(1,128)} %bitcast.19, bf16[512,512]{1,0:T(8,128)(2,1)} %point.1, bf16[4,768,128]{2,1,0:T(8,128)(2,1)} %ordered.1.refs_0_, bf16[4,768,128]{2,1,0:T(8,128)(2,1)} %collective-permute-done.21.refs_1_, ...), custom_call_target="tpu_custom_call" | custom-call | tf_op jit(solution)/shard_map/output/pallas_call | solution.py:490
  (42 shorter events, 0.1 us)
Async XLA Ops:
  3.3 11.9 %collective-permute-start.8 = (bf16[128,832]{1,0:T(8,128)(2,1)}, bf16[128,832]{1,0:T(8,128)(2,1)S(1)}, u32[]{:S(2)}, u32[]{:S(2)}) collective-permute-start(bf16[128,832]{1,0:T(8,128)(2,1)} %get-tuple-element.15), channel_id=1, source_target_pairs={{0,8},{8,16},{16,24},{24,0},{1,9},{9,17},{17,25},{25,1},{2,10},{10... | collective-permute-start | bytes 638984 | tf_op jit(solution)/shard_map/ppermute | solution.py:424
  6.4 25.7 %collective-permute-start.9 = (bf16[128,832]{1,0:T(8,128)(2,1)}, bf16[128,832]{1,0:T(8,128)(2,1)S(1)}, u32[]{:S(2)}, u32[]{:S(2)}) collective-permute-start(bf16[128,832]{1,0:T(8,128)(2,1)} %get-tuple-element.16), channel_id=1, source_target_pairs={{0,16},{8,24},{16,0},{24,8},{1,17},{9,25},{17,1},{25,9},{2,18},{10... | collective-permute-start | bytes 638984 | tf_op jit(solution)/shard_map/ppermute | solution.py:424
  9.0 23.7 %collective-permute-start.10 = (bf16[128,832]{1,0:T(8,128)(2,1)}, bf16[128,832]{1,0:T(8,128)(2,1)S(1)}, u32[]{:S(2)}, u32[]{:S(2)}) collective-permute-start(bf16[128,832]{1,0:T(8,128)(2,1)} %get-tuple-element.17), channel_id=1, source_target_pairs={{0,24},{8,0},{16,8},{24,16},{1,25},{9,1},{17,9},{25,17},{2,26},{10... | collective-permute-start | bytes 638984 | tf_op jit(solution)/shard_map/ppermute | solution.py:424
  10.3 29.8 %collective-permute-start.11 = (bf16[128,832]{1,0:T(8,128)(2,1)}, bf16[128,832]{1,0:T(8,128)(2,1)S(1)}, u32[]{:S(2)}, u32[]{:S(2)}) collective-permute-start(bf16[128,832]{1,0:T(8,128)(2,1)} %get-tuple-element.14.refs_0_), channel_id=1, source_target_pairs={{0,4},{2,6},{4,0},{6,2},{1,5},{3,7},{5,1},{7,3},{8,12},{10,14},{12... | collective-permute-start | bytes 638984 | tf_op jit(solution)/shard_map/ppermute | solution.py:401
  15.2 27.6 %copy-start.6 = (bf16[128,832]{1,0:T(8,128)(2,1)}, bf16[128,832]{1,0:T(8,128)(2,1)S(1)}, u32[]{:S(2)}) copy-start(bf16[128,832]{1,0:T(8,128)(2,1)S(1)} %collective-permute-done.8.refs_1_) | copy-start | bytes 638980
  15.2 26.2 %collective-permute-start.12 = (bf16[128,832]{1,0:T(8,128)(2,1)S(1)}, bf16[128,832]{1,0:T(8,128)(2,1)S(1)}, u32[]{:S(2)}, u32[]{:S(2)}) collective-permute-start(bf16[128,832]{1,0:T(8,128)(2,1)S(1)} %collective-permute-done.8.refs_1_), channel_id=1, source_target_pairs={{0,4},{2,6},{4,0},{6,2},{1,5},{3,7},{5,1},{7,3},{8,12},{10,14},{12... | collective-permute-start | bytes 638984 | tf_op jit(solution)/shard_map/ppermute | solution.py:401
  19.5 18.6 %collective-permute-start.19 = (bf16[768,128]{1,0:T(8,128)(2,1)}, bf16[768,128]{1,0:T(8,128)(2,1)}, u32[]{:S(2)}, u32[]{:S(2)}) collective-permute-start(bf16[768,128]{1,0:T(8,128)(2,1)} %get-tuple-element.18.refs_0_), channel_id=1, source_target_pairs={{0,16},{8,24},{16,0},{24,8},{1,17},{9,25},{17,1},{25,9},{2,18},{10... | collective-permute-start | bytes 589832 | tf_op jit(solution)/shard_map/ppermute | solution.py:388
  32.1 10.7 %copy-start.7 = (bf16[128,832]{1,0:T(8,128)(2,1)}, bf16[128,832]{1,0:T(8,128)(2,1)S(1)}, u32[]{:S(2)}) copy-start(bf16[128,832]{1,0:T(8,128)(2,1)S(1)} %collective-permute-done.9.refs_2_) | copy-start | bytes 638980
  32.1 10.7 %collective-permute-start.13 = (bf16[128,832]{1,0:T(8,128)(2,1)S(1)}, bf16[128,832]{1,0:T(8,128)(2,1)S(1)}, u32[]{:S(2)}, u32[]{:S(2)}) collective-permute-start(bf16[128,832]{1,0:T(8,128)(2,1)S(1)} %collective-permute-done.9.refs_2_), channel_id=1, source_target_pairs={{0,4},{2,6},{4,0},{6,2},{1,5},{3,7},{5,1},{7,3},{8,12},{10,14},{12... | collective-permute-start | bytes 638984 | tf_op jit(solution)/shard_map/ppermute | solution.py:401
  32.6 10.2 %copy-start.8 = (bf16[128,832]{1,0:T(8,128)(2,1)}, bf16[128,832]{1,0:T(8,128)(2,1)S(1)}, u32[]{:S(2)}) copy-start(bf16[128,832]{1,0:T(8,128)(2,1)S(1)} %collective-permute-done.10.refs_3_) | copy-start | bytes 638980
  32.6 10.2 %collective-permute-start.14 = (bf16[128,832]{1,0:T(8,128)(2,1)S(1)}, bf16[128,832]{1,0:T(8,128)(2,1)S(1)}, u32[]{:S(2)}, u32[]{:S(2)}) collective-permute-start(bf16[128,832]{1,0:T(8,128)(2,1)S(1)} %collective-permute-done.10.refs_3_), channel_id=1, source_target_pairs={{0,4},{2,6},{4,0},{6,2},{1,5},{3,7},{5,1},{7,3},{8,12},{10,14},{12... | collective-permute-start | bytes 638984 | tf_op jit(solution)/shard_map/ppermute | solution.py:401
  38.2 66.1 %collective-permute-start.17 = (bf16[768,128]{1,0:T(8,128)(2,1)}, bf16[768,128]{1,0:T(8,128)(2,1)}, u32[]{:S(2)}, u32[]{:S(2)}) collective-permute-start(bf16[768,128]{1,0:T(8,128)(2,1)} %get-tuple-element.18.refs_0_), channel_id=1, source_target_pairs={{0,8},{8,16},{16,24},{1,9},{9,17},{17,25},{2,10},{10,18},{18,26},{... | collective-permute-start | bytes 589832 | tf_op jit(solution)/shard_map/ppermute | solution.py:388
  40.2 2.7 %copy-start.9 = (bf16[128,832]{1,0:T(8,128)(2,1)}, bf16[128,832]{1,0:T(8,128)(2,1)S(1)}, u32[]{:S(2)}) copy-start(bf16[128,832]{1,0:T(8,128)(2,1)S(1)} %collective-permute-done.11.refs_4_) | copy-start | bytes 638980
  40.2 64.1 %collective-permute-start.18 = (bf16[768,128]{1,0:T(8,128)(2,1)}, bf16[768,128]{1,0:T(8,128)(2,1)}, u32[]{:S(2)}, u32[]{:S(2)}) collective-permute-start(bf16[768,128]{1,0:T(8,128)(2,1)} %get-tuple-element.18.refs_0_), channel_id=1, source_target_pairs={{8,0},{16,8},{24,16},{9,1},{17,9},{25,17},{10,2},{18,10},{26,18},{... | collective-permute-start | bytes 589832 | tf_op jit(solution)/shard_map/ppermute | solution.py:388
  41.5 1.4 copy-start.10
  41.5 62.8 %collective-permute-start.20 = (bf16[768,128]{1,0:T(8,128)(2,1)}, bf16[768,128]{1,0:T(8,128)(2,1)}, u32[]{:S(2)}, u32[]{:S(2)}) collective-permute-start(bf16[768,128]{1,0:T(8,128)(2,1)} %collective-permute-done.19.refs_3_), channel_id=1, source_target_pairs={{16,24},{8,0},{17,25},{9,1},{18,26},{10,2},{19,27},{11,3},{20,28},... | collective-permute-start | bytes 589832 | tf_op jit(solution)/shard_map/ppermute | solution.py:389
  42.8 0.7 copy-start.11
  43.5 0.7 copy-start.12
  100.9 74.1 %copy-start.14 = (f32[1,192]{1,0:T(1,128)S(1)}, f32[1,192]{1,0:T(1,128)}, u32[]{:S(2)}) copy-start(f32[1,192]{1,0:T(1,128)} %param.21) | copy-start | bytes 2308
  100.9 74.2 %copy-start.15 = (u32[32]{0:T(128)S(1)}, u32[32]{0:T(128)}, u32[]{:S(2)}) copy-start(u32[32]{0:T(128)} %constant.18) | copy-start | bytes 388
  104.2 91.7 %collective-permute-start.15 = (bf16[8,128,832]{1,2,0:T(8,128)(2,1)S(1)}, bf16[8,128,832]{1,2,0:T(8,128)(2,1)S(1)}, u32[]{:S(2)}, u32[]{:S(2)}) collective-permute-start(bf16[8,128,832]{1,2,0:T(8,128)(2,1)S(1)} %copy.21), channel_id=1, source_target_pairs={{0,2},{2,0},{4,6},{6,4},{1,3},{3,1},{5,7},{7,5},{8,10},{10,8},{12,... | collective-permute-start | bytes 5111816 | tf_op jit(solution)/shard_map/ppermute | solution.py:401
  129.9 33.0 %collective-permute-start.24 = (bf16[4,768,128]{2,1,0:T(8,128)(2,1)}, bf16[4,768,128]{2,1,0:T(8,128)(2,1)}, u32[]{:S(2)}, u32[]{:S(2)}) collective-permute-start(bf16[4,768,128]{2,1,0:T(8,128)(2,1)} %ordered.1.refs_0_), channel_id=1, source_target_pairs={{0,1},{1,0},{2,3},{3,2},{4,5},{5,4},{6,7},{7,6},{8,9},{9,8},{10,11... | collective-permute-start | bytes 2359304 | tf_op jit(solution)/shard_map/ppermute | solution.py:401
  131.5 23.6 %collective-permute-start.2 = (bf16[96,2048]{1,0:T(8,128)(2,1)}, bf16[96,2048]{1,0:T(8,128)(2,1)S(1)}, u32[]{:S(2)}, u32[]{:S(2)}) collective-permute-start(bf16[96,2048]{1,0:T(8,128)(2,1)} %get-tuple-element.13), channel_id=1, source_target_pairs={{0,16},{8,24},{16,0},{24,8},{1,17},{9,25},{17,1},{25,9},{2,18},{10... | collective-permute-start | bytes 1179656 | tf_op jit(solution)/shard_map/ppermute | solution.py:388
  137.2 19.2 %collective-permute-start = (bf16[96,2048]{1,0:T(8,128)(2,1)}, bf16[96,2048]{1,0:T(8,128)(2,1)S(1)}, u32[]{:S(2)}, u32[]{:S(2)}) collective-permute-start(bf16[96,2048]{1,0:T(8,128)(2,1)} %get-tuple-element.13), channel_id=1, source_target_pairs={{0,8},{8,16},{16,24},{1,9},{9,17},{17,25},{2,10},{10,18},{18,26},{... | collective-permute-start | bytes 1179656 | tf_op jit(solution)/shard_map/ppermute | solution.py:388
  138.5 21.8 %collective-permute-start.1 = (bf16[96,2048]{1,0:T(8,128)(2,1)}, bf16[96,2048]{1,0:T(8,128)(2,1)}, u32[]{:S(2)}, u32[]{:S(2)}) collective-permute-start(bf16[96,2048]{1,0:T(8,128)(2,1)} %get-tuple-element.13), channel_id=1, source_target_pairs={{8,0},{16,8},{24,16},{9,1},{17,9},{25,17},{10,2},{18,10},{26,18},{... | collective-permute-start | bytes 1179656 | tf_op jit(solution)/shard_map/ppermute | solution.py:388
  155.1 1.3 copy-start.2
  155.1 13.3 %collective-permute-start.3 = (bf16[96,2048]{1,0:T(8,128)(2,1)S(1)}, bf16[96,2048]{1,0:T(8,128)(2,1)}, u32[]{:S(2)}, u32[]{:S(2)}) collective-permute-start(bf16[96,2048]{1,0:T(8,128)(2,1)S(1)} %collective-permute-done.2.refs_2_), channel_id=1, source_target_pairs={{16,24},{8,0},{17,25},{9,1},{18,26},{10,2},{19,27},{11,3},{20,28},... | collective-permute-start | bytes 1179656 | tf_op jit(solution)/shard_map/ppermute | solution.py:389
  156.4 12.7 %copy-start.3 = (bf16[96,2048]{1,0:T(8,128)(2,1)}, bf16[96,2048]{1,0:T(8,128)(2,1)S(1)}, u32[]{:S(2)}) copy-start(bf16[96,2048]{1,0:T(8,128)(2,1)S(1)} %collective-permute-done.refs_0_) | copy-start | bytes 1179652
  156.4 12.7 %collective-permute-start.6 = (bf16[96,2048]{1,0:T(8,128)(2,1)S(1)}, bf16[96,2048]{1,0:T(8,128)(2,1)S(1)}, u32[]{:S(2)}, u32[]{:S(2)}) collective-permute-start(bf16[96,2048]{1,0:T(8,128)(2,1)S(1)} %collective-permute-done.2.refs_2_), channel_id=1, source_target_pairs={{0,1},{1,0},{8,9},{9,8},{16,17},{17,16},{24,25},{25,24},{2,3},{3,2... | collective-permute-start | bytes 1179656 | tf_op jit(solution)/shard_map/ppermute | solution.py:394
  160.3 23.0 %collective-permute-start.22 = (bf16[4,768,128]{2,1,0:T(8,128)(2,1)}, bf16[4,768,128]{2,1,0:T(8,128)(2,1)}, u32[]{:S(2)}, u32[]{:S(2)}) collective-permute-start(bf16[4,768,128]{2,1,0:T(8,128)(2,1)} %ordered.1.refs_0_), channel_id=1, source_target_pairs={{0,4},{2,6},{4,0},{6,2},{1,5},{3,7},{5,1},{7,3},{8,12},{10,14},{12... | collective-permute-start | bytes 2359304 | tf_op jit(solution)/shard_map/ppermute | solution.py:401
  162.9 32.9 %collective-permute-start.26 = (bf16[4,768,128]{2,1,0:T(8,128)(2,1)}, bf16[4,768,128]{2,1,0:T(8,128)(2,1)}, u32[]{:S(2)}, u32[]{:S(2)}) collective-permute-start(bf16[4,768,128]{2,1,0:T(8,128)(2,1)} %collective-permute-done.24.refs_4_), channel_id=1, source_target_pairs={{0,4},{2,6},{4,0},{6,2},{1,5},{3,7},{5,1},{7,3},{8,12},{10,14},{12... | collective-permute-start | bytes 2359304 | tf_op jit(solution)/shard_map/ppermute | solution.py:401
  168.4 3.2 %collective-permute-start.4 = (bf16[96,2048]{1,0:T(8,128)(2,1)S(1)}, bf16[96,2048]{1,0:T(8,128)(2,1)S(1)}, u32[]{:S(2)}, u32[]{:S(2)}) collective-permute-start(bf16[96,2048]{1,0:T(8,128)(2,1)S(1)} %collective-permute-done.refs_0_), channel_id=1, source_target_pairs={{8,9},{9,8},{16,17},{17,16},{24,25},{25,24},{10,11},{11,10},{18,19... | collective-permute-start | bytes 1179656 | tf_op jit(solution)/shard_map/ppermute | solution.py:394
  169.1 2.5 copy-start.4
  169.1 14.2 %collective-permute-start.5 = (bf16[96,2048]{1,0:T(8,128)(2,1)}, bf16[96,2048]{1,0:T(8,128)(2,1)}, u32[]{:S(2)}, u32[]{:S(2)}) collective-permute-start(bf16[96,2048]{1,0:T(8,128)(2,1)} %collective-permute-done.1.refs_1_), channel_id=1, source_target_pairs={{0,1},{1,0},{8,9},{9,8},{16,17},{17,16},{2,3},{3,2},{10,11},{11,10... | collective-permute-start | bytes 1179656 | tf_op jit(solution)/shard_map/ppermute | solution.py:394
  171.6 3.4 %copy-start.5 = (bf16[96,2048]{1,0:T(8,128)(2,1)}, bf16[96,2048]{1,0:T(8,128)(2,1)S(1)}, u32[]{:S(2)}) copy-start(bf16[96,2048]{1,0:T(8,128)(2,1)S(1)} %collective-permute-done.4.refs_4_) | copy-start | bytes 1179652
  171.6 41.8 %collective-permute-start.7 = (bf16[96,2048]{1,0:T(8,128)(2,1)}, bf16[96,2048]{1,0:T(8,128)(2,1)}, u32[]{:S(2)}, u32[]{:S(2)}) collective-permute-start(bf16[96,2048]{1,0:T(8,128)(2,1)} %collective-permute-done.3.refs_3_), channel_id=1, source_target_pairs={{0,1},{1,0},{24,25},{25,24},{2,3},{3,2},{26,27},{27,26},{4,5},{5,4... | collective-permute-start | bytes 1179656 | tf_op jit(solution)/shard_map/ppermute | solution.py:394
  183.3 54.9 %collective-permute-start.21 = (bf16[4,768,128]{2,1,0:T(8,128)(2,1)}, bf16[4,768,128]{2,1,0:T(8,128)(2,1)}, u32[]{:S(2)}, u32[]{:S(2)}) collective-permute-start(bf16[4,768,128]{2,1,0:T(8,128)(2,1)} %ordered.1.refs_0_), channel_id=1, source_target_pairs={{0,2},{2,0},{4,6},{6,4},{1,3},{3,1},{5,7},{7,5},{8,10},{10,8},{12,... | collective-permute-start | bytes 2359304 | tf_op jit(solution)/shard_map/ppermute | solution.py:401
  183.3 54.9 %collective-permute-start.25 = (bf16[4,768,128]{2,1,0:T(8,128)(2,1)}, bf16[4,768,128]{2,1,0:T(8,128)(2,1)}, u32[]{:S(2)}, u32[]{:S(2)}) collective-permute-start(bf16[4,768,128]{2,1,0:T(8,128)(2,1)} %collective-permute-done.24.refs_4_), channel_id=1, source_target_pairs={{0,2},{2,0},{4,6},{6,4},{1,3},{3,1},{5,7},{7,5},{8,10},{10,8},{12,... | collective-permute-start | bytes 2359304 | tf_op jit(solution)/shard_map/ppermute | solution.py:401
  195.8 42.5 %collective-permute-start.23 = (bf16[4,768,128]{2,1,0:T(8,128)(2,1)}, bf16[4,768,128]{2,1,0:T(8,128)(2,1)}, u32[]{:S(2)}, u32[]{:S(2)}) collective-permute-start(bf16[4,768,128]{2,1,0:T(8,128)(2,1)} %collective-permute-done.22.refs_2_), channel_id=1, source_target_pairs={{0,2},{2,0},{4,6},{6,4},{1,3},{3,1},{5,7},{7,5},{8,10},{10,8},{12,... | collective-permute-start | bytes 2359304 | tf_op jit(solution)/shard_map/ppermute | solution.py:401
  195.8 42.5 %collective-permute-start.27 = (bf16[4,768,128]{2,1,0:T(8,128)(2,1)}, bf16[4,768,128]{2,1,0:T(8,128)(2,1)S(1)}, u32[]{:S(2)}, u32[]{:S(2)}) collective-permute-start(bf16[4,768,128]{2,1,0:T(8,128)(2,1)} %collective-permute-done.26.refs_6_), channel_id=1, source_target_pairs={{0,2},{2,0},{4,6},{6,4},{1,3},{3,1},{5,7},{7,5},{8,10},{10,8},{12,... | collective-permute-start | bytes 2359304 | tf_op jit(solution)/shard_map/ppermute | solution.py:401
  213.4 20.0 %copy-start.13 = (f32[256]{0:T(256)S(1)}, f32[256]{0:T(256)}, u32[]{:S(2)}) copy-start(f32[256]{0:T(256)} %param.33) | copy-start | bytes 3076
  230.0 13.5 %all-to-all-start = ((bf16[8,96,256]{2,1,0:T(8,128)(2,1)}), bf16[8,96,256]{2,1,0:T(8,128)(2,1)S(1)}, u32[]{:S(2)}, u32[]{:S(2)}) async-start(bf16[8,96,256]{2,1,0:T(8,128)(2,1)} %bitcast.15), calls=%async_computation | async-start | bytes 786432 | tf_op jit(solution)/shard_map/all_to_all | solution.py:487
  233.5 4.2 %collective-permute-start.16 = (f32[256]{0:T(256)S(1)}, f32[256]{0:T(256)S(1)}, u32[]{:S(2)}, u32[]{:S(2)}) collective-permute-start(f32[256]{0:T(256)S(1)} %copy-done.13), channel_id=1, source_target_pairs={{0,1},{1,0},{2,3},{3,2},{4,5},{5,4},{6,7},{7,6},{8,9},{9,8},{10,11... | collective-permute-start | bytes 3080 | tf_op jit(solution)/shard_map/ppermute | solution.py:401
  238.3 5.2 %copy-start.1 = (bf16[4,768,128]{2,1,0:T(8,128)(2,1)}, bf16[4,768,128]{2,1,0:T(8,128)(2,1)S(1)}, u32[]{:S(2)}) copy-start(bf16[4,768,128]{2,1,0:T(8,128)(2,1)S(1)} %collective-permute-done.27.refs_7_) | copy-start | bytes 2359300
  243.5 0.7 copy-start

commit v2 on v1

--- a/solution.py
+++ b/solution.py
@@ -12,9 +12,9 @@
 GROUP_FLOOR = 1.0
 LANES = 128
 SPAN = 64
+SPARE = 32
 BF = jnp.bfloat16
 F32 = jnp.float32
-ANY = pl.BlockSpec(memory_space=pl.ANY)
 VM = pl.BlockSpec(memory_space=pltpu.VMEM)
 SM = pl.BlockSpec(memory_space=pltpu.SMEM)
 
@@ -54,89 +54,84 @@
             pair = ref[:, pl.ds(pl.multiple_of((target // 2) * LANES, LANES), LANES)]
             start = len(states) * LANES + at * half
             out[:, start : start + half] = jnp.where(odd, pair[:, half:], pair[:, :half])
-
-
-def norm_kernel(place, tokens, gain, out_conv, out_state, normed, part, rows_out):
+        out[:, start + half :] = jnp.zeros((out.shape[0], half), BF)
+
+
+def three_terms(a):
+    high = a.astype(BF).astype(F32)
+    middle = (a - high).astype(BF).astype(F32)
+    return high, middle, a - high - middle
+
+
+def norm_kernel(place, tokens, gain, out_conv, out_state, pace, conv_gain, normed, part, rows_out):
     count = part.shape[0]
     floats = tokens[...].astype(F32)
     inverse = lax.rsqrt(jnp.mean(floats * floats, axis=1, keepdims=True) + NORM_FLOOR)
     normed[...] = (floats * inverse * gain[...]).astype(BF)
     part[...] = normed[pl.ds(pl.multiple_of(place[0] * count, 16), count), :]
-    split = out_conv.shape[0]
+    split, wide = out_conv.shape[0], out_state.shape[0]
     rows_out[:split, :] = out_conv[...]
-    rows_out[split:, :] = out_state[...]
+    rows_out[split : split + wide, :] = out_state[...]
+    run = pace.shape[1] // 4
+    paces = jnp.concatenate(
+        [jnp.broadcast_to(pace[:, r * run : r * run + 1], (1, LANES)) for r in range(4)], axis=0
+    )
+    gains = jnp.concatenate(
+        [conv_gain[:, i * LANES : (i + 1) * LANES] for i in range(split // LANES)], axis=0
+    )
+    spare = jnp.concatenate(
+        list(three_terms(paces))
+        + list(three_terms(gains))
+        + [jnp.zeros((SPARE - 12 - 3 * gains.shape[0], LANES), F32)],
+        axis=0,
+    )
+    rows_out[split + wide :, :] = spare.astype(BF)
 
 
 def assemble_kernel(*refs):
-    *sources, out, sem = refs
-    copies = [pltpu.make_async_copy(s, out.at[i], sem.at[i]) for i, s in enumerate(sources)]
-    for copy in copies:
-        copy.start()
-    for copy in copies:
-        copy.wait()
+    *sources, out = refs
+    size = sources[0].shape[0]
+    for i, source in enumerate(sources):
+        out[i * size : (i + 1) * size, :] = source[...]
 
 
 def assemble(*arrays):
     return pl.pallas_call(
         assemble_kernel,
-        out_shape=jax.ShapeDtypeStruct((len(arrays),) + arrays[0].shape, arrays[0].dtype),
-        in_specs=[ANY] * len(arrays),
-        out_specs=ANY,
-        scratch_shapes=[pltpu.SemaphoreType.DMA((len(arrays),))],
+        out_shape=jax.ShapeDtypeStruct(
+            (len(arrays) * arrays[0].shape[0], arrays[0].shape[1]), arrays[0].dtype
+        ),
+        in_specs=[VM] * len(arrays),
+        out_specs=VM,
         name="assemble",
     )(*arrays)
 
 
-def mixer_kernel(
-    place, pace, own, *refs, length, halves, blocks_order
-):
+def mixer_kernel(place, own, *refs, length, halves, blocks_order):
     near = refs[: len(blocks_order)]
     far = refs[len(blocks_order) : 2 * len(blocks_order)]
     (
-        mine, sibling, start, base, correction, group_gain, taps, out,
-        x, w, proj, log_keep, conv_rows, y, sems,
+        mine, sibling, shards, start, base, correction, group_gain, taps, out,
+        x, w, proj, log_keep, conv_rows, y,
     ) = refs[2 * len(blocks_order) :]
     z, f, t = place[0], place[1], place[2]
     total_rows = x.shape[0]
     count = total_rows // length
     part = length // halves
-    jobs = []
-    slot = 0
-    for i in range(mine.shape[0]):
+    for i in range(mine.shape[0] // LANES):
         level, step = i // count, i % count
         source = lax.rem(z - step + count, count)
         for ref, flip in ((mine, 0), (sibling, 1)):
             row = (source * count + (f ^ (2 * level) ^ flip)) * LANES
-            jobs.append(
-                (None, pltpu.make_async_copy(
-                    ref.at[i], w.at[pl.ds(pl.multiple_of(row, LANES), LANES), :], sems.at[slot]
-                ))
-            )
-            slot += 1
-    jobs.append(
-        (None, pltpu.make_async_copy(
-            own, x.at[pl.ds(pl.multiple_of(z * length, 64), length), :], sems.at[slot]
-        ))
-    )
-    slot += 1
+            w[pl.ds(pl.multiple_of(row, LANES), LANES), :] = ref[i * LANES : (i + 1) * LANES, :]
+    x[pl.ds(pl.multiple_of(z * length, 64), length), :] = own[...]
     for (offset, valid), a, b in zip(blocks_order, near, far):
-        position = offset(z)
-        for ref, half in ((a, t), (b, 1 - t)):
-            row = pl.multiple_of(position * length + half * part, 32)
-            jobs.append(
-                (valid(z), pltpu.make_async_copy(ref, x.at[pl.ds(row, part), :], sems.at[slot]))
-            )
-            slot += 1
-    for condition, copy in jobs:
-        if condition is None:
-            copy.start()
-        else:
-            pl.when(condition)(copy.start)
-    for condition, copy in jobs:
-        if condition is None:
-            copy.wait()
-        else:
-            pl.when(condition)(copy.wait)
+
+        @pl.when(valid(z))
+        def _(offset=offset, a=a, b=b):
+            at = offset(z) * length
+            x[pl.ds(pl.multiple_of(at + t * part, 32), part), :] = a[...]
+            x[pl.ds(pl.multiple_of(at + (1 - t) * part, 32), part), :] = b[...]
 
     half = LANES // 2
     lane = iota((1, LANES), 1)
@@ -158,9 +153,11 @@
         proj[rows, :] = dot_nn(x[rows, :], w[...]).astype(BF)
         decay_in = proj[rows, 3 * LANES : 4 * LANES].astype(F32)
         rate = -jnp.exp(base_row + jnp.tanh(decay_in))
+        spare = shards[block, shards.shape[1] - SPARE :, :].astype(F32)
+        paces = spare[0:4, :] + spare[4:8, :] + spare[8:12, :]
         for r in range(4):
             log_keep[block * length + r * run : block * length + (r + 1) * run, :] = (
-                rate[r * run : (r + 1) * run, :] * pace[block * 4 + r]
+                rate[r * run : (r + 1) * run, :] * paces[r : r + 1, :]
             )
 
     left = 5 * LANES
@@ -303,16 +300,15 @@
         out[rows, :LANES] = (grouped * (gate * sigmoid(gate))).astype(BF)
 
 
-def output_kernel(place, received, gain, point, *refs, groups):
-    pieces, (out, w, sems) = refs[:-3], refs[-3:]
+def output_kernel(place, received, point, *refs, groups):
+    pieces, (out, w) = refs[:-2], refs[-2:]
     z, f, t = place[0], place[1], place[2]
     sources, rows, _ = received.shape
     count = sources // groups
     half = LANES // 2
     split = count * half
     wide = count * LANES
-    jobs = []
-    slot = 0
+    gains = []
     for at, piece in enumerate(pieces):
         core, flip, side = at & 1, (at >> 1) & 1, (at >> 2) & 1
         group = t ^ side
@@ -322,14 +318,18 @@
                 (0, split, group * split),
                 (split, wide, groups * split + group * wide),
             ):
-                copy = pltpu.make_async_copy(
-                    piece.at[block, pl.ds(start, size), :],
-                    w.at[pl.ds(pl.multiple_of(shift, LANES), size), pl.ds(col, LANES)],
-                    sems.at[slot],
-                )
-                copy.start()
-                jobs.append(copy)
-                slot += 1
+                w[pl.ds(pl.multiple_of(shift, LANES), size), pl.ds(col, LANES)] = piece[
+                    block, start : start + size, :
+                ]
+        if core == flip == 0:
+            spare = piece[0, split + wide :, :].astype(F32)
+            tall = split // LANES
+            parts = [spare[12 + i * tall : 12 + (i + 1) * tall, :] for i in range(3)]
+            total = parts[0] + parts[1] + parts[2]
+            gains.append(jnp.concatenate([total[i : i + 1] for i in range(tall)], axis=1))
+    gain = jnp.concatenate(
+        [jnp.where(t == 0, gains[0], gains[1]), jnp.where(t == 0, gains[1], gains[0])], axis=1
+    )
     sums, gates, states = [], [], []
     for group in range(groups):
         for block in range(count):
@@ -341,33 +341,22 @@
     gate = jnp.concatenate(gates, axis=1).astype(F32)
     mean = jnp.mean(conv_sum, axis=1, keepdims=True)
     spread = jnp.mean(conv_sum * conv_sum, axis=1, keepdims=True) - mean * mean
-    scaled = (conv_sum - mean) * lax.rsqrt(spread + CHANNEL_FLOOR) * gain[...]
+    scaled = (conv_sum - mean) * lax.rsqrt(spread + CHANNEL_FLOOR) * gain
     shaped = (scaled * sigmoid(scaled)).astype(BF)
     conv_out = (dot_nn(shaped, point[...]) * (gate * sigmoid(gate))).astype(BF)
     joined = jnp.concatenate([conv_out] + states, axis=1)
-    for copy in jobs:
-        copy.wait()
     out[...] = dot_nn(joined, w[...]).astype(BF)
 
 
 def ordered_kernel(place, *refs, blocks_order):
-    *sources, out, sems = refs
+    own, *sources, out = refs
     z = place[0]
-    jobs = [(None, pltpu.make_async_copy(sources[0], out.at[z], sems.at[0]))]
-    for i, ((offset, valid), source) in enumerate(zip(blocks_order, sources[1:])):
-        jobs.append(
-            (valid(z), pltpu.make_async_copy(source, out.at[offset(z)], sems.at[i + 1]))
-        )
-    for condition, copy in jobs:
-        if condition is None:
-            copy.start()
-        else:
-            pl.when(condition)(copy.start)
-    for condition, copy in jobs:
-        if condition is None:
-            copy.wait()
-        else:
-            pl.when(condition)(copy.wait)
+    out[z] = own[...]
+    for (offset, valid), source in zip(blocks_order, sources):
+
+        @pl.when(valid(z))
+        def _(offset=offset, source=source):
+            out[offset(z)] = source[...]
 
 
 LINE = (
@@ -412,7 +401,7 @@
     part = length // halves
     place = jnp.stack([lax.axis_index(a) for a in ("sp", "fs", "tp")]).astype(jnp.int32)
     shard = conv_value.shape[0]
-    columns = 5 * LANES + 3 * LANES // 2
+    columns = 7 * LANES
     slices = pl.pallas_call(
         split_weights_kernel,
         out_shape=[jax.ShapeDtypeStruct((shard, columns), BF)] * count,
@@ -430,30 +419,28 @@
         out_shape=[
             jax.ShapeDtypeStruct((length, width), BF),
             jax.ShapeDtypeStruct((part, width), BF),
-            jax.ShapeDtypeStruct((out_rows, output_conv.shape[1]), BF),
+            jax.ShapeDtypeStruct((out_rows + SPARE, output_conv.shape[1]), BF),
         ],
-        in_specs=[SM, VM, VM, VM, VM],
+        in_specs=[SM] + [VM] * 6,
         out_specs=[VM] * 3,
         name="norm",
-    )(place[2:], tokens.reshape(length, width), norm_gain.reshape(1, width), output_conv, output_state)
+    )(
+        place[2:], tokens.reshape(length, width), norm_gain.reshape(1, width), output_conv,
+        output_state, decay_pace, conv_gain.reshape(1, -1),
+    )
+    rows_out, _ = lax.optimization_barrier((rows_out, taken[1]))
+    line_out = along_line(rows_out)
+    half, _ = lax.optimization_barrier((half, line_out[2]))
     near = along_line(half)
     far = [across(a, LINE[i]) for i, a in enumerate(near)]
     lifted = [flipped(a, "fs", 2) for a in taken]
     mine = assemble(*taken, *lifted)
     sibling = flipped(mine, "fs", 1)
-    paces = lax.all_gather(decay_pace[0, :: length // 4], "sp", axis=0, tiled=True)
-    gain_other = flipped(conv_gain, "tp", 1)
-    low = lax.axis_index("tp") == 0
-    gain = jnp.concatenate(
-        [jnp.where(low, conv_gain, gain_other), jnp.where(low, gain_other, conv_gain)]
-    )
-    line_out = along_line(rows_out)
     ordered = pl.pallas_call(
         functools.partial(ordered_kernel, blocks_order=LINE_ORDER),
         out_shape=jax.ShapeDtypeStruct((count,) + rows_out.shape, BF),
-        in_specs=[SM] + [ANY] * 5,
-        out_specs=ANY,
-        scratch_shapes=[pltpu.SemaphoreType.DMA((5,))],
+        in_specs=[SM] + [VM] * 5,
+        out_specs=VM,
         name="ordered",
     )(place, rows_out, *line_out)
     crossed = flipped(ordered, "tp", 1)
@@ -467,7 +454,7 @@
     mixed = pl.pallas_call(
         functools.partial(mixer_kernel, length=length, halves=halves, blocks_order=LINE_ORDER),
         out_shape=jax.ShapeDtypeStruct((total, 2 * LANES), BF),
-        in_specs=[SM, SM] + [ANY] * 11 + [VM] * 5,
+        in_specs=[SM] + [VM] * 17,
         out_specs=VM,
         scratch_shapes=[
             pltpu.VMEM((total, width), BF),
@@ -476,11 +463,10 @@
             pltpu.VMEM((total, LANES), F32),
             pltpu.VMEM((total // 2 + 32, LANES), F32),
             pltpu.VMEM((total, LANES), F32),
-            pltpu.SemaphoreType.DMA((32,)),
         ],
         name="mixer",
     )(
-        place, paces, normed, *near, *far, mine, sibling,
+        place, normed, *near, *far, mine, sibling, ordered,
         start_state.reshape(heads, *start_state.shape[2:]),
         decay_base.reshape(1, -1), correction.reshape(1, -1), group_gain.reshape(1, -1), conv_taps,
     )
@@ -490,14 +476,11 @@
     out = pl.pallas_call(
         functools.partial(output_kernel, groups=halves),
         out_shape=jax.ShapeDtypeStruct((rows, width), BF),
-        in_specs=[SM, VM, VM, VM] + [ANY] * 8,
+        in_specs=[SM] + [VM] * 10,
         out_specs=VM,
-        scratch_shapes=[
-            pltpu.VMEM((halves * out_rows, width), BF),
-            pltpu.SemaphoreType.DMA((64,)),
-        ],
+        scratch_shapes=[pltpu.VMEM((halves * out_rows, width), BF)],
         name="output",
-    )(place, received, gain.reshape(1, -1), point_weight, *pieces)
+    )(place, received, point_weight, *pieces)
     return out.reshape(1, rows, width)
 
 

time: 252 us -> 158 us (0.63)
  Pallas kernels: 111 us -> 34 us
  blocking collectives: 14 us -> 0 us
  waiting for transfers between devices: 58 us -> 66 us
  local copies, waits for them, and re-layouts: 9.08 us -> 3.94 us
  starting transfers between devices: 56.8 us -> 52.6 us
    pallas_call x1, Pallas kernels: 56.8 us -> 2.97 us  [assemble(): pl.pallas_call(assemble_kernel, out_shape=jax.ShapeDtypeStruct((len(array...]
    pallas_call x1, Pallas kernels: 25.6 us -> 2.26 us  [head_body(): pl.pallas_call(functools.partial(ordered_kernel, blocks_order=LINE_ORDER)...]
    ppermute x4, waiting for transfers between devices: 7.05 us -> 21.4 us  [across(): lax.ppermute(value, ('sp', 'tp'), [(2 * i + s, 2 * i + 1 - s) for i in ta...]
    ppermute x13 -> x12, waiting for transfers between devices: 14.3 us -> 0.03 us  [flipped(): return lax.ppermute(value, axis, [(i, i ^ bit) for i in range(count)])]
    all_gather x1 -> x0, blocking collectives: 14 us -> none  [head_body(): lax.all_gather(decay_pace[0, ::length // 4], 'sp', axis=0, tiled=True)]
    all_to_all x1, waiting for transfers between devices: 5.17 us -> 12.3 us  [head_body(): lax.all_to_all(mixed.reshape(count * halves, rows, 2 * LANES), ('sp', 'tp...]
    ppermute x2, waiting for transfers between devices: 5.46 us -> 9.91 us  [along_line(): return (right, left, double, lax.ppermute(double, 'sp', LINE[3]))]
    ppermute x6, waiting for transfers between devices: 22.6 us -> 18.9 us  [along_line(): right, left, double = (lax.ppermute(value, 'sp', LINE[i]) for i in range(3))]
  transfers between devices with their start and end apart: 29 -> 28, of which waited for: 9 -> 11; matrix products, arithmetic and copies ran while one was open for 3% -> 0% of each run, Pallas kernels for 40% -> 15%
where the time goes in v2:
time: 158 us; the launch traced here: 157 us
  waiting for transfers between devices  66 us (42%)
  starting transfers between devices  52.6 us (33%)
  Pallas kernels  34 us (22%)
  local copies, waits for them, and re-layouts  3.94 us (2%)
    ppermute x4, waiting for transfers between devices, across(): lax.ppermute(value, ('sp', 'tp'), [(2 * i + s, 2 * i + 1 - s) for i in ta...  21.4 us
    ppermute x6, starting transfers between devices, along_line(): right, left, double = (lax.ppermute(value, 'sp', LINE[i]) for i in range(3))  21.2 us
    ppermute x6, waiting for transfers between devices, along_line(): right, left, double = (lax.ppermute(value, 'sp', LINE[i]) for i in range(3))  18.9 us
    pallas_call x1, Pallas kernels, head_body(): pl.pallas_call(functools.partial(mixer_kernel, length=length, halves=halv...  16.5 us
    all_to_all x1, waiting for transfers between devices, head_body(): lax.all_to_all(mixed.reshape(count * halves, rows, 2 * LANES), ('sp', 'tp...  12.3 us
    ppermute x2, waiting for transfers between devices, along_line(): return (right, left, double, lax.ppermute(double, 'sp', LINE[3]))  9.91 us
    ppermute x12, starting transfers between devices, flipped(): return lax.ppermute(value, axis, [(i, i ^ bit) for i in range(count)])  9.88 us
    ppermute x4, starting transfers between devices, across(): lax.ppermute(value, ('sp', 'tp'), [(2 * i + s, 2 * i + 1 - s) for i in ta...  7.09 us
  transfers between devices with their start and end apart: 28, of which 11 were waited for; matrix products, arithmetic and copies ran while one was open for 0% of the time, Pallas kernels for 15%

profile of v2, /device:TPU:0, one launch (start us, length us, event | category | flops | bytes accessed | tf_op | source)
XLA Modules:
  0.0 157.4 jit_solution(4758385599461921593)
XLA Ops:
  0.0 0.6 pad_add_fusion.place
  0.6 2.7 %split_weights.1 = (bf16[128,896]{1,0:T(8,128)(2,1)}, bf16[128,896]{1,0:T(8,128)(2,1)}, bf16[128,896]{1,0:T(8,128)(2,1)}, bf16[128,896]{1,0:T(8,128)(2,1)}) custom-call(s32[3]{0:T(128)} %pad_add_fusion.place, bf16[128,256]{1,0:T(8,128)(2,1)} %refs_0_.1, bf16[128,256]{1,0:T(8,128)(2,1)} %refs_1_.1, bf16[128,256]{1,0:T(8,128)(2,1)} %refs_2_.1, ...), custom_call_target="tpu_custom_call" | custom-call | tf_op jit(solution)/shard_map/split_weights/pallas_call | solution.py:405
  3.3 3.0 %collective-permute-start = (bf16[128,896]{1,0:T(8,128)(2,1)}, bf16[128,896]{1,0:T(8,128)(2,1)S(1)}, u32[]{:S(2)}, u32[]{:S(2)}) collective-permute-start(bf16[128,896]{1,0:T(8,128)(2,1)} %get-tuple-element.17), channel_id=1, source_target_pairs={{0,8},{8,16},{16,24},{24,0},{1,9},{9,17},{17,25},{25,1},{2,10},{10... | collective-permute-start | bytes 688136 | tf_op jit(solution)/shard_map/ppermute | solution.py:413
  6.3 2.6 %collective-permute-start.10 = (bf16[128,896]{1,0:T(8,128)(2,1)}, bf16[128,896]{1,0:T(8,128)(2,1)S(1)}, u32[]{:S(2)}, u32[]{:S(2)}) collective-permute-start(bf16[128,896]{1,0:T(8,128)(2,1)} %get-tuple-element.21), channel_id=1, source_target_pairs={{0,16},{8,24},{16,0},{24,8},{1,17},{9,25},{17,1},{25,9},{2,18},{10... | collective-permute-start | bytes 688136 | tf_op jit(solution)/shard_map/ppermute | solution.py:413
  8.9 1.3 collective-permute-start.11
  10.3 1.5 collective-permute-start.12
  11.8 3.4 %collective-permute-done.refs_1_ = bf16[128,896]{1,0:T(8,128)(2,1)S(1)} collective-permute-done((bf16[128,896]{1,0:T(8,128)(2,1)}, bf16[128,896]{1,0:T(8,128)(2,1)S(1)}, u32[]{:S(2)}, u32[]{:S(2)}) %collective-permute-start) | collective-permute-done | bytes 229408 | tf_op jit(solution)/shard_map/ppermute | solution.py:413
  15.1 1.7 %collective-permute-start.13 = (bf16[128,896]{1,0:T(8,128)(2,1)S(1)}, bf16[128,896]{1,0:T(8,128)(2,1)S(1)}, u32[]{:S(2)}, u32[]{:S(2)}) collective-permute-start(bf16[128,896]{1,0:T(8,128)(2,1)S(1)} %collective-permute-done.refs_1_), channel_id=1, source_target_pairs={{0,4},{2,6},{4,0},{6,2},{1,5},{3,7},{5,1},{7,3},{8,12},{10,14},{12... | collective-permute-start | bytes 688136 | tf_op jit(solution)/shard_map/ppermute | solution.py:390
  16.9 2.6 %norm.1 = (bf16[192,2048]{1,0:T(8,128)(2,1)}, bf16[96,2048]{1,0:T(8,128)(2,1)}, bf16[800,128]{1,0:T(8,128)(2,1)}) custom-call(s32[1]{0:T(128)} %bitcast.2.place, bf16[192,2048]{1,0:T(8,128)(2,1)} %bitcast.13, f32[1,2048]{1,0:T(1,128)} %bitcast.15, bf16[256,128]{1,0:T(8,128)(2,1)} %out_conv.1, bf16[512,128]{1,0:T(8,128)(2,1)} %out_state.1, f32[1,192]{1,0:T(1,128)} %pace.1, ...), custom_call_target="tpu_custom_call" | custom-call | tf_op jit(solution)/shard_map/norm/pallas_call | solution.py:417
  19.5 12.7 %collective-permute-start.1 = (bf16[800,128]{1,0:T(8,128)(2,1)}, bf16[800,128]{1,0:T(8,128)(2,1)S(1)}, u32[]{:S(2)}, u32[]{:S(2)}) collective-permute-start(bf16[800,128]{1,0:T(8,128)(2,1)} %get-tuple-element.18.refs_0_), channel_id=1, source_target_pairs={{0,16},{8,24},{16,0},{24,8},{1,17},{9,25},{17,1},{25,9},{2,18},{10... | collective-permute-start | bytes 614408 | tf_op jit(solution)/shard_map/ppermute | solution.py:377
  32.2 0.0 collective-permute-done.10.refs_2_
  32.2 0.5 collective-permute-start.14
  32.7 0.0 collective-permute-done.11.refs_3_
  32.7 1.5 collective-permute-start.15
  34.2 0.0 collective-permute-done.12.refs_4_
  34.2 1.3 collective-permute-start.17
  35.5 2.8 %collective-permute-done.1.refs_3_ = bf16[800,128]{1,0:T(8,128)(2,1)S(1)} collective-permute-done((bf16[800,128]{1,0:T(8,128)(2,1)}, bf16[800,128]{1,0:T(8,128)(2,1)S(1)}, u32[]{:S(2)}, u32[]{:S(2)}) %collective-permute-start.1) | collective-permute-done | bytes 204832 | tf_op jit(solution)/shard_map/ppermute | solution.py:377
  38.3 1.3 collective-permute-start.18
  39.6 1.3 collective-permute-start.19
  40.9 0.0 collective-permute-done.14.refs_6_
  41.0 0.0 collective-permute-done.15.refs_7_
  41.0 0.6 copy-done.17
  41.6 0.7 copy-done.18
  42.3 3.0 %assemble.1.refs_8_ = bf16[1024,896]{1,0:T(8,128)(2,1)} custom-call(bf16[128,896]{1,0:T(8,128)(2,1)} %get-tuple-element.20.refs_0_, bf16[128,896]{1,0:T(8,128)(2,1)} %copy-done.12, bf16[128,896]{1,0:T(8,128)(2,1)} %copy-done.13, bf16[128,896]{1,0:T(8,128)(2,1)} %copy-done.14, bf16[128,896]{1,0:T(8,128)(2,1)} %copy-done.15, bf16[128,896]{1,0:T(8,128)(2,1)} %copy-done.16, ...), custom_call_target="tpu_custom_call" | custom-call | tf_op jit(solution)/shard_map/assemble/pallas_call | solution.py:99
  45.3 0.0 collective-permute-start.16
  45.3 0.0 collective-permute-done.17.refs_1_
  45.3 0.9 collective-permute-done.18.refs_2_
  46.2 2.2 %collective-permute-done.19.refs_4_ = bf16[800,128]{1,0:T(8,128)(2,1)S(1)} collective-permute-done((bf16[800,128]{1,0:T(8,128)(2,1)S(1)}, bf16[800,128]{1,0:T(8,128)(2,1)S(1)}, u32[]{:S(2)}, u32[]{:S(2)}) %collective-permute-start.19) | collective-permute-done | bytes 204832 | tf_op jit(solution)/shard_map/ppermute | solution.py:378
  48.4 0.7 copy-done.22
  49.1 2.3 %ordered.1.refs_10_.refs_0_ = bf16[4,800,128]{2,1,0:T(8,128)(2,1)} custom-call(s32[3]{0:T(128)} %pad_add_fusion.place, bf16[800,128]{1,0:T(8,128)(2,1)} %get-tuple-element.18.refs_0_, bf16[800,128]{1,0:T(8,128)(2,1)} %copy-done.20, bf16[800,128]{1,0:T(8,128)(2,1)} %copy-done.21, bf16[800,128]{1,0:T(8,128)(2,1)} %copy-done.19, bf16[800,128]{1,0:T(8,128)(2,1)} %copy-done.22), custom_call_target="tpu_custom_call" | custom-call | tf_op jit(solution)/shard_map/ordered/pallas_call | solution.py:439
  51.3 1.5 collective-permute-start.23
  52.8 2.2 %collective-permute-start.4 = (bf16[96,2048]{1,0:T(8,128)(2,1)}, bf16[96,2048]{1,0:T(8,128)(2,1)S(1)}, u32[]{:S(2)}, u32[]{:S(2)}) collective-permute-start(bf16[96,2048]{1,0:T(8,128)(2,1)} %get-tuple-element.19), channel_id=1, source_target_pairs={{0,16},{8,24},{16,0},{24,8},{1,17},{9,25},{17,1},{25,9},{2,18},{10... | collective-permute-start | bytes 1179656 | tf_op jit(solution)/shard_map/ppermute | solution.py:377
  55.0 2.5 %collective-permute-start.2 = (bf16[96,2048]{1,0:T(8,128)(2,1)}, bf16[96,2048]{1,0:T(8,128)(2,1)S(1)}, u32[]{:S(2)}, u32[]{:S(2)}) collective-permute-start(bf16[96,2048]{1,0:T(8,128)(2,1)} %get-tuple-element.19), channel_id=1, source_target_pairs={{0,8},{8,16},{16,24},{1,9},{9,17},{17,25},{2,10},{10,18},{18,26},{... | collective-permute-start | bytes 1179656 | tf_op jit(solution)/shard_map/ppermute | solution.py:377
  57.5 1.3 collective-permute-start.3
  58.8 14.7 %collective-permute-done.4.refs_2_ = bf16[96,2048]{1,0:T(8,128)(2,1)S(1)} collective-permute-done((bf16[96,2048]{1,0:T(8,128)(2,1)}, bf16[96,2048]{1,0:T(8,128)(2,1)S(1)}, u32[]{:S(2)}, u32[]{:S(2)}) %collective-permute-start.4) | collective-permute-done | bytes 393248 | tf_op jit(solution)/shard_map/ppermute | solution.py:377
  73.5 1.3 collective-permute-start.5
  74.8 1.0 collective-permute-start.21
  75.8 0.0 collective-permute-done.23.refs_4_
  75.8 1.1 collective-permute-start.25
  76.9 0.6 collective-permute-done.3.refs_1_
  77.5 0.7 collective-permute-start.6
  78.2 7.7 %collective-permute-done.5.refs_3_ = bf16[96,2048]{1,0:T(8,128)(2,1)S(1)} collective-permute-done((bf16[96,2048]{1,0:T(8,128)(2,1)S(1)}, bf16[96,2048]{1,0:T(8,128)(2,1)S(1)}, u32[]{:S(2)}, u32[]{:S(2)}) %collective-permute-start.5) | collective-permute-done | bytes 393248 | tf_op jit(solution)/shard_map/ppermute | solution.py:378
  85.9 2.4 %collective-permute-start.7 = (bf16[96,2048]{1,0:T(8,128)(2,1)S(1)}, bf16[96,2048]{1,0:T(8,128)(2,1)S(1)}, u32[]{:S(2)}, u32[]{:S(2)}) collective-permute-start(bf16[96,2048]{1,0:T(8,128)(2,1)S(1)} %collective-permute-done.3.refs_1_), channel_id=1, source_target_pairs={{0,1},{1,0},{8,9},{9,8},{16,17},{17,16},{2,3},{3,2},{10,11},{11,10... | collective-permute-start | bytes 1179656 | tf_op jit(solution)/shard_map/ppermute | solution.py:383
  88.3 1.6 collective-permute-start.8
  89.9 9.9 %collective-permute-done.7.refs_5_ = bf16[96,2048]{1,0:T(8,128)(2,1)S(1)} collective-permute-done((bf16[96,2048]{1,0:T(8,128)(2,1)S(1)}, bf16[96,2048]{1,0:T(8,128)(2,1)S(1)}, u32[]{:S(2)}, u32[]{:S(2)}) %collective-permute-start.7) | collective-permute-done | bytes 393248 | tf_op jit(solution)/shard_map/ppermute | solution.py:383
  99.8 2.4 %collective-permute-start.9 = (bf16[96,2048]{1,0:T(8,128)(2,1)S(1)}, bf16[96,2048]{1,0:T(8,128)(2,1)S(1)}, u32[]{:S(2)}, u32[]{:S(2)}) collective-permute-start(bf16[96,2048]{1,0:T(8,128)(2,1)S(1)} %collective-permute-done.5.refs_3_), channel_id=1, source_target_pairs={{0,1},{1,0},{24,25},{25,24},{2,3},{3,2},{26,27},{27,26},{4,5},{5,4... | collective-permute-start | bytes 1179656 | tf_op jit(solution)/shard_map/ppermute | solution.py:383
  102.2 6.0 %collective-permute-done.8.refs_6_ = bf16[96,2048]{1,0:T(8,128)(2,1)S(1)} collective-permute-done((bf16[96,2048]{1,0:T(8,128)(2,1)S(1)}, bf16[96,2048]{1,0:T(8,128)(2,1)S(1)}, u32[]{:S(2)}, u32[]{:S(2)}) %collective-permute-start.8) | collective-permute-done | bytes 393248 | tf_op jit(solution)/shard_map/ppermute | solution.py:383
  108.2 0.0 collective-permute-start.20
  108.2 0.0 collective-permute-done.21.refs_2_
  108.2 0.5 collective-permute-start.22
  108.7 5.6 %collective-permute-done.9.refs_7_ = bf16[96,2048]{1,0:T(8,128)(2,1)S(1)} collective-permute-done((bf16[96,2048]{1,0:T(8,128)(2,1)S(1)}, bf16[96,2048]{1,0:T(8,128)(2,1)S(1)}, u32[]{:S(2)}, u32[]{:S(2)}) %collective-permute-start.9) | collective-permute-done | bytes 393248 | tf_op jit(solution)/shard_map/ppermute | solution.py:383
  114.3 0.0 collective-permute-start.24
  114.3 0.0 collective-permute-done.25.refs_6_
  114.3 0.5 collective-permute-start.26
  114.8 0.0 collective-permute-done.16.refs_9_
  114.8 0.2 copy-done.11
  115.0 1.0 copy-done
  116.0 16.5 %mixer.1 = bf16[768,256]{1,0:T(8,128)(2,1)} custom-call(s32[3]{0:T(128)} %pad_add_fusion.place, bf16[192,2048]{1,0:T(8,128)(2,1)} %get-tuple-element.14.own, bf16[96,2048]{1,0:T(8,128)(2,1)} %copy-done.5, bf16[96,2048]{1,0:T(8,128)(2,1)} %copy-done.6, bf16[96,2048]{1,0:T(8,128)(2,1)} %copy-done.4, bf16[96,2048]{1,0:T(8,128)(2,1)} %copy-done.7, ...), custom_call_target="tpu_custom_call" | custom-call | tf_op jit(solution)/shard_map/mixer/pallas_call | solution.py:454
  132.5 4.8 %all-to-all-start = ((bf16[8,96,256]{2,1,0:T(8,128)(2,1)}), bf16[8,96,256]{2,1,0:T(8,128)(2,1)S(1)}, u32[]{:S(2)}, u32[]{:S(2)}) async-start(bf16[8,96,256]{2,1,0:T(8,128)(2,1)} %bitcast.12), calls=%async_computation | async-start | bytes 786432 | tf_op jit(solution)/shard_map/all_to_all | solution.py:473
  137.3 0.0 collective-permute-done.20.refs_1_
  137.3 12.3 %all-to-all-done.received = bf16[8,96,256]{2,1,0:T(8,128)(2,1)S(1)} async-done(((bf16[8,96,256]{2,1,0:T(8,128)(2,1)}), bf16[8,96,256]{2,1,0:T(8,128)(2,1)S(1)}, u32[]{:S(2)}, u32[]{:S(2)}) %all-to-all-start) | async-done | bytes 393248 | tf_op jit(solution)/shard_map/all_to_all | solution.py:473
  149.6 0.0 collective-permute-done.26.refs_7_
  149.6 0.7 copy-done.1
  150.4 7.0 %output.1 = bf16[96,2048]{1,0:T(8,128)(2,1)} custom-call(s32[3]{0:T(128)} %pad_add_fusion.place, bf16[8,96,256]{2,1,0:T(8,128)(2,1)} %copy-done.1, bf16[512,512]{1,0:T(8,128)(2,1)} %point.1, bf16[4,800,128]{2,1,0:T(8,128)(2,1)} %ordered.1.refs_10_.refs_0_, bf16[4,800,128]{2,1,0:T(8,128)(2,1)} %collective-permute-done.20.refs_1_, ...), custom_call_target="tpu_custom_call" | custom-call | tf_op jit(solution)/shard_map/output/pallas_call | solution.py:476
  (45 shorter events, 0.1 us)
Async XLA Ops:
  3.3 11.9 %collective-permute-start = (bf16[128,896]{1,0:T(8,128)(2,1)}, bf16[128,896]{1,0:T(8,128)(2,1)S(1)}, u32[]{:S(2)}, u32[]{:S(2)}) collective-permute-start(bf16[128,896]{1,0:T(8,128)(2,1)} %get-tuple-element.17), channel_id=1, source_target_pairs={{0,8},{8,16},{16,24},{24,0},{1,9},{9,17},{17,25},{25,1},{2,10},{10... | collective-permute-start | bytes 688136 | tf_op jit(solution)/shard_map/ppermute | solution.py:413
  6.3 25.9 %collective-permute-start.10 = (bf16[128,896]{1,0:T(8,128)(2,1)}, bf16[128,896]{1,0:T(8,128)(2,1)S(1)}, u32[]{:S(2)}, u32[]{:S(2)}) collective-permute-start(bf16[128,896]{1,0:T(8,128)(2,1)} %get-tuple-element.21), channel_id=1, source_target_pairs={{0,16},{8,24},{16,0},{24,8},{1,17},{9,25},{17,1},{25,9},{2,18},{10... | collective-permute-start | bytes 688136 | tf_op jit(solution)/shard_map/ppermute | solution.py:413
  8.9 23.8 %collective-permute-start.11 = (bf16[128,896]{1,0:T(8,128)(2,1)}, bf16[128,896]{1,0:T(8,128)(2,1)S(1)}, u32[]{:S(2)}, u32[]{:S(2)}) collective-permute-start(bf16[128,896]{1,0:T(8,128)(2,1)} %get-tuple-element.22), channel_id=1, source_target_pairs={{0,24},{8,0},{16,8},{24,16},{1,25},{9,1},{17,9},{25,17},{2,26},{10... | collective-permute-start | bytes 688136 | tf_op jit(solution)/shard_map/ppermute | solution.py:413
  10.3 24.0 %collective-permute-start.12 = (bf16[128,896]{1,0:T(8,128)(2,1)}, bf16[128,896]{1,0:T(8,128)(2,1)S(1)}, u32[]{:S(2)}, u32[]{:S(2)}) collective-permute-start(bf16[128,896]{1,0:T(8,128)(2,1)} %get-tuple-element.20.refs_0_), channel_id=1, source_target_pairs={{0,4},{2,6},{4,0},{6,2},{1,5},{3,7},{5,1},{7,3},{8,12},{10,14},{12... | collective-permute-start | bytes 688136 | tf_op jit(solution)/shard_map/ppermute | solution.py:390
  15.1 25.8 %copy-start.12 = (bf16[128,896]{1,0:T(8,128)(2,1)}, bf16[128,896]{1,0:T(8,128)(2,1)S(1)}, u32[]{:S(2)}) copy-start(bf16[128,896]{1,0:T(8,128)(2,1)S(1)} %collective-permute-done.refs_1_) | copy-start | bytes 688132
  15.1 24.5 %collective-permute-start.13 = (bf16[128,896]{1,0:T(8,128)(2,1)S(1)}, bf16[128,896]{1,0:T(8,128)(2,1)S(1)}, u32[]{:S(2)}, u32[]{:S(2)}) collective-permute-start(bf16[128,896]{1,0:T(8,128)(2,1)S(1)} %collective-permute-done.refs_1_), channel_id=1, source_target_pairs={{0,4},{2,6},{4,0},{6,2},{1,5},{3,7},{5,1},{7,3},{8,12},{10,14},{12... | collective-permute-start | bytes 688136 | tf_op jit(solution)/shard_map/ppermute | solution.py:390
  19.5 18.8 %collective-permute-start.1 = (bf16[800,128]{1,0:T(8,128)(2,1)}, bf16[800,128]{1,0:T(8,128)(2,1)S(1)}, u32[]{:S(2)}, u32[]{:S(2)}) collective-permute-start(bf16[800,128]{1,0:T(8,128)(2,1)} %get-tuple-element.18.refs_0_), channel_id=1, source_target_pairs={{0,16},{8,24},{16,0},{24,8},{1,17},{9,25},{17,1},{25,9},{2,18},{10... | collective-permute-start | bytes 614408 | tf_op jit(solution)/shard_map/ppermute | solution.py:377
  32.2 8.8 %copy-start.13 = (bf16[128,896]{1,0:T(8,128)(2,1)}, bf16[128,896]{1,0:T(8,128)(2,1)S(1)}, u32[]{:S(2)}) copy-start(bf16[128,896]{1,0:T(8,128)(2,1)S(1)} %collective-permute-done.10.refs_2_) | copy-start | bytes 688132
  32.2 8.7 %collective-permute-start.14 = (bf16[128,896]{1,0:T(8,128)(2,1)S(1)}, bf16[128,896]{1,0:T(8,128)(2,1)S(1)}, u32[]{:S(2)}, u32[]{:S(2)}) collective-permute-start(bf16[128,896]{1,0:T(8,128)(2,1)S(1)} %collective-permute-done.10.refs_2_), channel_id=1, source_target_pairs={{0,4},{2,6},{4,0},{6,2},{1,5},{3,7},{5,1},{7,3},{8,12},{10,14},{12... | collective-permute-start | bytes 688136 | tf_op jit(solution)/shard_map/ppermute | solution.py:390
  32.7 8.3 %copy-start.14 = (bf16[128,896]{1,0:T(8,128)(2,1)}, bf16[128,896]{1,0:T(8,128)(2,1)S(1)}, u32[]{:S(2)}) copy-start(bf16[128,896]{1,0:T(8,128)(2,1)S(1)} %collective-permute-done.11.refs_3_) | copy-start | bytes 688132
  32.7 8.3 %collective-permute-start.15 = (bf16[128,896]{1,0:T(8,128)(2,1)S(1)}, bf16[128,896]{1,0:T(8,128)(2,1)S(1)}, u32[]{:S(2)}, u32[]{:S(2)}) collective-permute-start(bf16[128,896]{1,0:T(8,128)(2,1)S(1)} %collective-permute-done.11.refs_3_), channel_id=1, source_target_pairs={{0,4},{2,6},{4,0},{6,2},{1,5},{3,7},{5,1},{7,3},{8,12},{10,14},{12... | collective-permute-start | bytes 688136 | tf_op jit(solution)/shard_map/ppermute | solution.py:390
  34.2 6.8 %copy-start.15 = (bf16[128,896]{1,0:T(8,128)(2,1)}, bf16[128,896]{1,0:T(8,128)(2,1)S(1)}, u32[]{:S(2)}) copy-start(bf16[128,896]{1,0:T(8,128)(2,1)S(1)} %collective-permute-done.12.refs_4_) | copy-start | bytes 688132
  34.2 11.1 %collective-permute-start.17 = (bf16[800,128]{1,0:T(8,128)(2,1)}, bf16[800,128]{1,0:T(8,128)(2,1)S(1)}, u32[]{:S(2)}, u32[]{:S(2)}) collective-permute-start(bf16[800,128]{1,0:T(8,128)(2,1)} %get-tuple-element.18.refs_0_), channel_id=1, source_target_pairs={{0,8},{8,16},{16,24},{1,9},{9,17},{17,25},{2,10},{10,18},{18,26},{... | collective-permute-start | bytes 614408 | tf_op jit(solution)/shard_map/ppermute | solution.py:377
  38.3 10.0 %copy-start.19 = (bf16[800,128]{1,0:T(8,128)(2,1)}, bf16[800,128]{1,0:T(8,128)(2,1)S(1)}, u32[]{:S(2)}) copy-start(bf16[800,128]{1,0:T(8,128)(2,1)S(1)} %collective-permute-done.1.refs_3_) | copy-start | bytes 614404
  38.3 7.8 %collective-permute-start.18 = (bf16[800,128]{1,0:T(8,128)(2,1)}, bf16[800,128]{1,0:T(8,128)(2,1)S(1)}, u32[]{:S(2)}, u32[]{:S(2)}) collective-permute-start(bf16[800,128]{1,0:T(8,128)(2,1)} %get-tuple-element.18.refs_0_), channel_id=1, source_target_pairs={{8,0},{16,8},{24,16},{9,1},{17,9},{25,17},{10,2},{18,10},{26,18},{... | collective-permute-start | bytes 614408 | tf_op jit(solution)/shard_map/ppermute | solution.py:377
  39.6 1.4 copy-start.16
  39.6 8.7 %collective-permute-start.19 = (bf16[800,128]{1,0:T(8,128)(2,1)S(1)}, bf16[800,128]{1,0:T(8,128)(2,1)S(1)}, u32[]{:S(2)}, u32[]{:S(2)}) collective-permute-start(bf16[800,128]{1,0:T(8,128)(2,1)S(1)} %collective-permute-done.1.refs_3_), channel_id=1, source_target_pairs={{16,24},{8,0},{17,25},{9,1},{18,26},{10,2},{19,27},{11,3},{20,28},... | collective-permute-start | bytes 614408 | tf_op jit(solution)/shard_map/ppermute | solution.py:378
  40.9 0.7 copy-start.17
  41.6 0.7 copy-start.18
  45.3 69.5 %collective-permute-start.16 = (bf16[1024,896]{1,0:T(8,128)(2,1)}, bf16[1024,896]{1,0:T(8,128)(2,1)S(1)}, u32[]{:S(2)}, u32[]{:S(2)}) collective-permute-start(bf16[1024,896]{1,0:T(8,128)(2,1)} %assemble.1.refs_8_), channel_id=1, source_target_pairs={{0,2},{2,0},{4,6},{6,4},{1,3},{3,1},{5,7},{7,5},{8,10},{10,8},{12,... | collective-permute-start | bytes 5505032 | tf_op jit(solution)/shard_map/ppermute | solution.py:390
  45.3 3.1 %copy-start.20 = (bf16[800,128]{1,0:T(8,128)(2,1)}, bf16[800,128]{1,0:T(8,128)(2,1)S(1)}, u32[]{:S(2)}) copy-start(bf16[800,128]{1,0:T(8,128)(2,1)S(1)} %collective-permute-done.17.refs_1_) | copy-start | bytes 614404
  46.2 2.2 %copy-start.21 = (bf16[800,128]{1,0:T(8,128)(2,1)}, bf16[800,128]{1,0:T(8,128)(2,1)S(1)}, u32[]{:S(2)}) copy-start(bf16[800,128]{1,0:T(8,128)(2,1)S(1)} %collective-permute-done.18.refs_2_) | copy-start | bytes 614404
  48.4 0.7 copy-start.22
  51.3 24.5 %collective-permute-start.23 = (bf16[4,800,128]{2,1,0:T(8,128)(2,1)}, bf16[4,800,128]{2,1,0:T(8,128)(2,1)S(1)}, u32[]{:S(2)}, u32[]{:S(2)}) collective-permute-start(bf16[4,800,128]{2,1,0:T(8,128)(2,1)} %ordered.1.refs_10_.refs_0_), channel_id=1, source_target_pairs={{0,1},{1,0},{2,3},{3,2},{4,5},{5,4},{6,7},{7,6},{8,9},{9,8},{10,11... | collective-permute-start | bytes 2457608 | tf_op jit(solution)/shard_map/ppermute | solution.py:390
  52.8 20.7 %collective-permute-start.4 = (bf16[96,2048]{1,0:T(8,128)(2,1)}, bf16[96,2048]{1,0:T(8,128)(2,1)S(1)}, u32[]{:S(2)}, u32[]{:S(2)}) collective-permute-start(bf16[96,2048]{1,0:T(8,128)(2,1)} %get-tuple-element.19), channel_id=1, source_target_pairs={{0,16},{8,24},{16,0},{24,8},{1,17},{9,25},{17,1},{25,9},{2,18},{10... | collective-permute-start | bytes 1179656 | tf_op jit(solution)/shard_map/ppermute | solution.py:377
  55.0 19.8 %collective-permute-start.2 = (bf16[96,2048]{1,0:T(8,128)(2,1)}, bf16[96,2048]{1,0:T(8,128)(2,1)S(1)}, u32[]{:S(2)}, u32[]{:S(2)}) collective-permute-start(bf16[96,2048]{1,0:T(8,128)(2,1)} %get-tuple-element.19), channel_id=1, source_target_pairs={{0,8},{8,16},{16,24},{1,9},{9,17},{17,25},{2,10},{10,18},{18,26},{... | collective-permute-start | bytes 1179656 | tf_op jit(solution)/shard_map/ppermute | solution.py:377
  57.5 19.9 %collective-permute-start.3 = (bf16[96,2048]{1,0:T(8,128)(2,1)}, bf16[96,2048]{1,0:T(8,128)(2,1)S(1)}, u32[]{:S(2)}, u32[]{:S(2)}) collective-permute-start(bf16[96,2048]{1,0:T(8,128)(2,1)} %get-tuple-element.19), channel_id=1, source_target_pairs={{8,0},{16,8},{24,16},{9,1},{17,9},{25,17},{10,2},{18,10},{26,18},{... | collective-permute-start | bytes 1179656 | tf_op jit(solution)/shard_map/ppermute | solution.py:377
  73.5 41.3 %copy-start.4 = (bf16[96,2048]{1,0:T(8,128)(2,1)}, bf16[96,2048]{1,0:T(8,128)(2,1)S(1)}, u32[]{:S(2)}) copy-start(bf16[96,2048]{1,0:T(8,128)(2,1)S(1)} %collective-permute-done.4.refs_2_) | copy-start | bytes 1179652
  73.5 12.4 %collective-permute-start.5 = (bf16[96,2048]{1,0:T(8,128)(2,1)S(1)}, bf16[96,2048]{1,0:T(8,128)(2,1)S(1)}, u32[]{:S(2)}, u32[]{:S(2)}) collective-permute-start(bf16[96,2048]{1,0:T(8,128)(2,1)S(1)} %collective-permute-done.4.refs_2_), channel_id=1, source_target_pairs={{16,24},{8,0},{17,25},{9,1},{18,26},{10,2},{19,27},{11,3},{20,28},... | collective-permute-start | bytes 1179656 | tf_op jit(solution)/shard_map/ppermute | solution.py:378
  74.8 40.0 %copy-start.5 = (bf16[96,2048]{1,0:T(8,128)(2,1)}, bf16[96,2048]{1,0:T(8,128)(2,1)S(1)}, u32[]{:S(2)}) copy-start(bf16[96,2048]{1,0:T(8,128)(2,1)S(1)} %collective-permute-done.2.refs_0_) | copy-start | bytes 1179652
  74.8 33.4 %collective-permute-start.21 = (bf16[4,800,128]{2,1,0:T(8,128)(2,1)}, bf16[4,800,128]{2,1,0:T(8,128)(2,1)S(1)}, u32[]{:S(2)}, u32[]{:S(2)}) collective-permute-start(bf16[4,800,128]{2,1,0:T(8,128)(2,1)} %ordered.1.refs_10_.refs_0_), channel_id=1, source_target_pairs={{0,4},{2,6},{4,0},{6,2},{1,5},{3,7},{5,1},{7,3},{8,12},{10,14},{12... | collective-permute-start | bytes 2457608 | tf_op jit(solution)/shard_map/ppermute | solution.py:390
  75.8 73.8 %copy-start.2 = (bf16[4,800,128]{2,1,0:T(8,128)(2,1)}, bf16[4,800,128]{2,1,0:T(8,128)(2,1)S(1)}, u32[]{:S(2)}) copy-start(bf16[4,800,128]{2,1,0:T(8,128)(2,1)S(1)} %collective-permute-done.23.refs_4_) | copy-start | bytes 2457604
  75.8 38.5 %collective-permute-start.25 = (bf16[4,800,128]{2,1,0:T(8,128)(2,1)S(1)}, bf16[4,800,128]{2,1,0:T(8,128)(2,1)}, u32[]{:S(2)}, u32[]{:S(2)}) collective-permute-start(bf16[4,800,128]{2,1,0:T(8,128)(2,1)S(1)} %collective-permute-done.23.refs_4_), channel_id=1, source_target_pairs={{0,4},{2,6},{4,0},{6,2},{1,5},{3,7},{5,1},{7,3},{8,12},{10,14},{12... | collective-permute-start | bytes 2457608 | tf_op jit(solution)/shard_map/ppermute | solution.py:390
  77.5 37.3 %copy-start.6 = (bf16[96,2048]{1,0:T(8,128)(2,1)}, bf16[96,2048]{1,0:T(8,128)(2,1)S(1)}, u32[]{:S(2)}) copy-start(bf16[96,2048]{1,0:T(8,128)(2,1)S(1)} %collective-permute-done.3.refs_1_) | copy-start | bytes 1179652
  77.5 10.8 %collective-permute-start.6 = (bf16[96,2048]{1,0:T(8,128)(2,1)S(1)}, bf16[96,2048]{1,0:T(8,128)(2,1)S(1)}, u32[]{:S(2)}, u32[]{:S(2)}) collective-permute-start(bf16[96,2048]{1,0:T(8,128)(2,1)S(1)} %collective-permute-done.2.refs_0_), channel_id=1, source_target_pairs={{8,9},{9,8},{16,17},{17,16},{24,25},{25,24},{10,11},{11,10},{18,19... | collective-permute-start | bytes 1179656 | tf_op jit(solution)/shard_map/ppermute | solution.py:383
  85.9 28.9 %copy-start.7 = (bf16[96,2048]{1,0:T(8,128)(2,1)}, bf16[96,2048]{1,0:T(8,128)(2,1)S(1)}, u32[]{:S(2)}) copy-start(bf16[96,2048]{1,0:T(8,128)(2,1)S(1)} %collective-permute-done.5.refs_3_) | copy-start | bytes 1179652
  85.9 13.9 %collective-permute-start.7 = (bf16[96,2048]{1,0:T(8,128)(2,1)S(1)}, bf16[96,2048]{1,0:T(8,128)(2,1)S(1)}, u32[]{:S(2)}, u32[]{:S(2)}) collective-permute-start(bf16[96,2048]{1,0:T(8,128)(2,1)S(1)} %collective-permute-done.3.refs_1_), channel_id=1, source_target_pairs={{0,1},{1,0},{8,9},{9,8},{16,17},{17,16},{2,3},{3,2},{10,11},{11,10... | collective-permute-start | bytes 1179656 | tf_op jit(solution)/shard_map/ppermute | solution.py:383
  88.3 26.5 %copy-start.8 = (bf16[96,2048]{1,0:T(8,128)(2,1)}, bf16[96,2048]{1,0:T(8,128)(2,1)S(1)}, u32[]{:S(2)}) copy-start(bf16[96,2048]{1,0:T(8,128)(2,1)S(1)} %collective-permute-done.6.refs_4_) | copy-start | bytes 1179652
  88.3 19.8 %collective-permute-start.8 = (bf16[96,2048]{1,0:T(8,128)(2,1)S(1)}, bf16[96,2048]{1,0:T(8,128)(2,1)S(1)}, u32[]{:S(2)}, u32[]{:S(2)}) collective-permute-start(bf16[96,2048]{1,0:T(8,128)(2,1)S(1)} %collective-permute-done.4.refs_2_), channel_id=1, source_target_pairs={{0,1},{1,0},{8,9},{9,8},{16,17},{17,16},{24,25},{25,24},{2,3},{3,2... | collective-permute-start | bytes 1179656 | tf_op jit(solution)/shard_map/ppermute | solution.py:383
  99.7 15.1 %copy-start.9 = (bf16[96,2048]{1,0:T(8,128)(2,1)}, bf16[96,2048]{1,0:T(8,128)(2,1)S(1)}, u32[]{:S(2)}) copy-start(bf16[96,2048]{1,0:T(8,128)(2,1)S(1)} %collective-permute-done.7.refs_5_) | copy-start | bytes 1179652
  99.8 14.5 %collective-permute-start.9 = (bf16[96,2048]{1,0:T(8,128)(2,1)S(1)}, bf16[96,2048]{1,0:T(8,128)(2,1)S(1)}, u32[]{:S(2)}, u32[]{:S(2)}) collective-permute-start(bf16[96,2048]{1,0:T(8,128)(2,1)S(1)} %collective-permute-done.5.refs_3_), channel_id=1, source_target_pairs={{0,1},{1,0},{24,25},{25,24},{2,3},{3,2},{26,27},{27,26},{4,5},{5,4... | collective-permute-start | bytes 1179656 | tf_op jit(solution)/shard_map/ppermute | solution.py:383
  108.2 6.7 %copy-start.10 = (bf16[96,2048]{1,0:T(8,128)(2,1)}, bf16[96,2048]{1,0:T(8,128)(2,1)S(1)}, u32[]{:S(2)}) copy-start(bf16[96,2048]{1,0:T(8,128)(2,1)S(1)} %collective-permute-done.8.refs_6_) | copy-start | bytes 1179652
  108.2 29.1 %collective-permute-start.20 = (bf16[4,800,128]{2,1,0:T(8,128)(2,1)}, bf16[4,800,128]{2,1,0:T(8,128)(2,1)}, u32[]{:S(2)}, u32[]{:S(2)}) collective-permute-start(bf16[4,800,128]{2,1,0:T(8,128)(2,1)} %ordered.1.refs_10_.refs_0_), channel_id=1, source_target_pairs={{0,2},{2,0},{4,6},{6,4},{1,3},{3,1},{5,7},{7,5},{8,10},{10,8},{12,... | collective-permute-start | bytes 2457608 | tf_op jit(solution)/shard_map/ppermute | solution.py:390
  108.2 41.4 %copy-start.3 = (bf16[4,800,128]{2,1,0:T(8,128)(2,1)}, bf16[4,800,128]{2,1,0:T(8,128)(2,1)S(1)}, u32[]{:S(2)}) copy-start(bf16[4,800,128]{2,1,0:T(8,128)(2,1)S(1)} %collective-permute-done.21.refs_2_) | copy-start | bytes 2457604
  108.2 29.1 %collective-permute-start.22 = (bf16[4,800,128]{2,1,0:T(8,128)(2,1)S(1)}, bf16[4,800,128]{2,1,0:T(8,128)(2,1)}, u32[]{:S(2)}, u32[]{:S(2)}) collective-permute-start(bf16[4,800,128]{2,1,0:T(8,128)(2,1)S(1)} %collective-permute-done.21.refs_2_), channel_id=1, source_target_pairs={{0,2},{2,0},{4,6},{6,4},{1,3},{3,1},{5,7},{7,5},{8,10},{10,8},{12,... | collective-permute-start | bytes 2457608 | tf_op jit(solution)/shard_map/ppermute | solution.py:390
  114.3 0.7 copy-start.11
  114.3 23.0 %collective-permute-start.24 = (bf16[4,800,128]{2,1,0:T(8,128)(2,1)S(1)}, bf16[4,800,128]{2,1,0:T(8,128)(2,1)}, u32[]{:S(2)}, u32[]{:S(2)}) collective-permute-start(bf16[4,800,128]{2,1,0:T(8,128)(2,1)S(1)} %collective-permute-done.23.refs_4_), channel_id=1, source_target_pairs={{0,2},{2,0},{4,6},{6,4},{1,3},{3,1},{5,7},{7,5},{8,10},{10,8},{12,... | collective-permute-start | bytes 2457608 | tf_op jit(solution)/shard_map/ppermute | solution.py:390
  114.3 35.3 %collective-permute-start.26 = (bf16[4,800,128]{2,1,0:T(8,128)(2,1)}, bf16[4,800,128]{2,1,0:T(8,128)(2,1)}, u32[]{:S(2)}, u32[]{:S(2)}) collective-permute-start(bf16[4,800,128]{2,1,0:T(8,128)(2,1)} %collective-permute-done.25.refs_6_), channel_id=1, source_target_pairs={{0,2},{2,0},{4,6},{6,4},{1,3},{3,1},{5,7},{7,5},{8,10},{10,8},{12,... | collective-permute-start | bytes 2457608 | tf_op jit(solution)/shard_map/ppermute | solution.py:390
  114.8 1.2 copy-start
  132.5 17.1 %all-to-all-start = ((bf16[8,96,256]{2,1,0:T(8,128)(2,1)}), bf16[8,96,256]{2,1,0:T(8,128)(2,1)S(1)}, u32[]{:S(2)}, u32[]{:S(2)}) async-start(bf16[8,96,256]{2,1,0:T(8,128)(2,1)} %bitcast.12), calls=%async_computation | async-start | bytes 786432 | tf_op jit(solution)/shard_map/all_to_all | solution.py:473
  149.6 0.8 copy-start.1

commit v3 on v0

--- a/solution.py
+++ b/solution.py
@@ -1,11 +1,527 @@
+import functools
+
 import jax
 import jax.numpy as jnp
 from jax import lax
+from jax.experimental import pallas as pl
+from jax.experimental.pallas import tpu as pltpu
 from jax.sharding import PartitionSpec as P
 
 NORM_FLOOR = 0.1
 CHANNEL_FLOOR = 0.1
 GROUP_FLOOR = 1.0
+LANES = 128
+SPAN = 64
+SPARE = 16
+BF = jnp.bfloat16
+F32 = jnp.float32
+VM = pl.BlockSpec(memory_space=pltpu.VMEM)
+
+
+def dot_nn(a, b):
+    return lax.dot_general(a, b, (((1,), (0,)), ((), ())), preferred_element_type=F32)
+
+
+def dot_nt(a, b):
+    return lax.dot_general(a, b, (((1,), (1,)), ((), ())), preferred_element_type=F32)
+
+
+def dot_tn(a, b):
+    return lax.dot_general(a, b, (((0,), (0,)), ((), ())), preferred_element_type=F32)
+
+
+def sigmoid(x):
+    return 1.0 / (1.0 + jnp.exp(-x))
+
+
+def iota(shape, dim):
+    return lax.broadcasted_iota(jnp.int32, shape, dim)
+
+
+def three_terms(a):
+    high = a.astype(BF).astype(F32)
+    middle = (a - high).astype(BF).astype(F32)
+    return high, middle, a - high - middle
+
+
+def here():
+    return [lax.axis_index(a) for a in ("sp", "fs", "tp")]
+
+
+def split_weights_kernel(*refs):
+    pace, convs, states, outs = refs[0], refs[1:4], refs[4:9], refs[9:]
+    run = pace.shape[1] // 4
+    paces = jnp.concatenate(
+        [jnp.broadcast_to(pace[:, r * run : r * run + 1], (1, LANES // 2)) for r in range(4)], axis=0
+    )
+    rest = jnp.zeros((convs[0].shape[0] - 12, LANES // 2), F32)
+    spare = jnp.concatenate([*three_terms(paces), rest], axis=0).astype(BF)
+    half = LANES // 2
+    z = here()[0]
+    for step, out in enumerate(outs):
+        target = z ^ step
+        for at, ref in enumerate(states):
+            out[:, at * LANES : (at + 1) * LANES] = ref[
+                :, pl.ds(pl.multiple_of(target * LANES, LANES), LANES)
+            ]
+        odd = lax.rem(target, 2) == 1
+        for at, ref in enumerate(convs):
+            pair = ref[:, pl.ds(pl.multiple_of((target // 2) * LANES, LANES), LANES)]
+            start = len(states) * LANES + at * half
+            out[:, start : start + half] = jnp.where(odd, pair[:, half:], pair[:, :half])
+        out[:, start + half :] = spare
+
+
+def norm_kernel(tokens, gain, out_conv, out_state, conv_gain, normed, part, rows_out):
+    count = part.shape[0]
+    floats = tokens[...].astype(F32)
+    inverse = lax.rsqrt(jnp.mean(floats * floats, axis=1, keepdims=True) + NORM_FLOOR)
+    normed[...] = (floats * inverse * gain[...]).astype(BF)
+    part[...] = normed[pl.ds(pl.multiple_of(here()[2] * count, 16), count), :]
+    split, wide = out_conv.shape[0], out_state.shape[0]
+    rows_out[:split, :] = out_conv[...]
+    rows_out[split : split + wide, :] = out_state[...]
+    gains = jnp.concatenate(
+        [conv_gain[:, i * LANES : (i + 1) * LANES] for i in range(split // LANES)], axis=0
+    )
+    spare = jnp.concatenate(
+        list(three_terms(gains)) + [jnp.zeros((SPARE - 3 * gains.shape[0], LANES), F32)],
+        axis=0,
+    )
+    rows_out[split + wide :, :] = spare.astype(BF)
+
+
+def assemble_kernel(*refs):
+    *sources, out = refs
+    size = sources[0].shape[0]
+    for i, source in enumerate(sources):
+        out[i * size : (i + 1) * size, :] = source[...]
+
+
+def call(kernel, outs, *args, scratch=(), held=(), whole=(), room=10, **settings):
+    specs, operands = [], []
+    for at, arg in enumerate(args):
+        specs.append(pl.BlockSpec(memory_space=pl.ANY) if at in whole else VM)
+        apart = at in held or at in whole
+        operands.append(pltpu.with_memory_space_constraint(arg, pltpu.HBM if apart else pltpu.VMEM))
+    return pl.pallas_call(
+        functools.partial(kernel, **settings) if settings else kernel,
+        out_shape=[pltpu.VMEM(*o) if isinstance(o, tuple) else o for o in outs],
+        in_specs=specs,
+        out_specs=[VM] * len(outs),
+        scratch_shapes=[pltpu.VMEM(*a) if isinstance(a, tuple) else a for a in scratch],
+        compiler_params=pltpu.CompilerParams(vmem_limit_bytes=room << 20),
+    )(*operands)
+
+
+def masks():
+    half = LANES // 2
+    lane = iota((1, LANES), 1)
+    first = (lane < half).astype(F32)
+    ri, ci = iota((LANES, LANES), 0), iota((LANES, LANES), 1)
+    return first, 1.0 - first, ri, ci, (ri // half) == (ci // half)
+
+
+def stage_terms(x, w, paces, base_row, corr_row, conv_part, gate_part, local, lead, step, added, kept, proj, log_keep):
+    length = x.shape[0]
+    first, second, ri, ci, same = masks()
+    sum_mat = jnp.where(same, 1.0, 0.0).astype(BF)
+    strict = same & (ri > ci)
+    weak = same & (ri >= ci)
+    eye = jnp.where(ri == ci, 1.0, 0.0).astype(F32)
+    run = length // 4
+    proj[...] = dot_nn(x[...], w[...])
+    gate_part[...] = proj[:, 4 * LANES : 5 * LANES].astype(BF)
+    conv_part[...] = proj[:, 5 * LANES : 7 * LANES].astype(BF)
+    rate = -jnp.exp(base_row + jnp.tanh(proj[:, 3 * LANES : 4 * LANES].astype(BF).astype(F32)))
+    for r in range(4):
+        log_keep[r * run : (r + 1) * run, :] = rate[r * run : (r + 1) * run, :] * paces[r : r + 1, :]
+
+    chunks = length // SPAN
+    tri = jnp.where(iota((SPAN, SPAN), 0) >= iota((SPAN, SPAN), 1), 1.0, 0.0).astype(F32)
+
+    def stack(a):
+        return jnp.concatenate([a * first, a * second], axis=0).astype(BF)
+
+    sums = lax.dot_general(
+        tri,
+        jnp.concatenate([log_keep[c * SPAN : (c + 1) * SPAN, :] for c in range(chunks)], axis=1),
+        (((1,), (0,)), ((), ())),
+        precision=lax.Precision.HIGHEST,
+        preferred_element_type=F32,
+    )
+    levels = []
+    size = 1
+    while size < SPAN:
+        inside = (ri // (2 * size)) == (ci // (2 * size))
+        levels.append(inside & ((ri & size) != 0) & ((ci & size) == 0))
+        size *= 2
+    grams, tails, heads = [], [], []
+    for c in range(chunks):
+        rows = slice(c * SPAN, (c + 1) * SPAN)
+        total = sums[:, c * LANES : (c + 1) * LANES]
+        before = total - log_keep[rows, :]
+        last = total[SPAN - 1 : SPAN, :]
+        q = proj[rows, 0:LANES].astype(BF).astype(F32)
+        k = proj[rows, LANES : 2 * LANES].astype(BF).astype(F32)
+        v = proj[rows, 2 * LANES : 3 * LANES]
+        norm = dot_nn((k * k).astype(BF), sum_mat)
+        unit = k * lax.rsqrt(jnp.maximum(norm, 1.0))
+        write = unit * corr_row
+        back = jnp.exp(-total)
+        rest = jnp.exp(last - total)
+        lead_remove = stack(-unit * jnp.exp(before))
+        lead_query = stack(q * jnp.exp(total))
+        grams.append(
+            dot_nt(
+                jnp.concatenate([lead_remove, lead_query], axis=0),
+                jnp.concatenate([stack(write * back), stack(k * back)], axis=0),
+            )
+        )
+        tails.append((stack(write * rest), stack(k * rest)))
+        heads.append((lead_remove, lead_query, stack(v)))
+        kept[c] = jnp.broadcast_to(jnp.exp(last), kept.shape[1:])
+    system = [jnp.where(strict, g[:LANES, :LANES], 0.0) for g in grams]
+    inverse = [eye + jnp.where(levels[0], a, 0.0) for a in system]
+    for level in levels[1:]:
+        low = [i.astype(BF) for i in inverse]
+        inner = [
+            dot_nn(i, jnp.where(level, a, 0.0).astype(BF)).astype(BF) for i, a in zip(low, system)
+        ]
+        inverse = [i + dot_nn(n, b) for i, n, b in zip(inverse, inner, low)]
+    direct = [
+        dot_nn(
+            jnp.concatenate(
+                [
+                    jnp.where(strict, g[:LANES, LANES:], 0.0),
+                    jnp.where(weak, g[LANES:, LANES:], 0.0),
+                ],
+                axis=0,
+            ).astype(BF),
+            h[2],
+        )
+        for g, h in zip(grams, heads)
+    ]
+    solved = [
+        dot_nn(i.astype(BF), jnp.concatenate([d[:LANES].astype(BF), h[0]], axis=1)).astype(BF)
+        for i, d, h in zip(inverse, direct, heads)
+    ]
+    through = [
+        dot_nn(jnp.where(weak, g[LANES:, :LANES], 0.0).astype(BF), s) for g, s in zip(grams, solved)
+    ]
+    for c, (d, s, h, u, tail) in enumerate(zip(direct, solved, heads, through, tails)):
+        own = u[:, :LANES] + d[LANES:]
+        moved = dot_tn(s, tail[0])
+        local[c] = own[:SPAN] + own[SPAN:]
+        lead[c] = (h[1].astype(F32) + u[:, LANES:]).astype(BF)
+        step[c] = moved[LANES:].astype(BF)
+        added[c] = moved[:LANES] + dot_tn(h[2], tail[1])
+
+
+def own_kernel(x, mine, sibling, base, correction, w, *outs):
+    z, f, _ = here()
+    count = lax.axis_size("sp")
+    for i in range(mine.shape[0] // LANES):
+        level, step = i // count, i % count
+        source = z ^ step
+        for ref, flip in ((mine, 0), (sibling, 1)):
+            row = (source * lax.axis_size("fs") + (f ^ (2 * level) ^ flip)) * LANES
+            w[pl.ds(pl.multiple_of(row, LANES), LANES), :] = ref[i * LANES : (i + 1) * LANES, :]
+    block_terms_in(z, x, w, base, correction, outs)
+
+
+def block_terms_in(position, x, w, base, correction, refs):
+    row = (position * lax.axis_size("fs") + here()[1]) * LANES
+    spare = w[pl.ds(pl.multiple_of(row, LANES), 16), w.shape[1] - LANES :].astype(F32)
+    paces = spare[0:4, :] + spare[4:8, :] + spare[8:12, :]
+    paces = jnp.concatenate([paces[:, LANES // 2 :]] * 2, axis=1)
+    stage_terms(x, w, paces, base[...], correction[...], *refs)
+
+
+def prepare_kernel(start, base, correction, group_gain, taps, state, *outs):
+    z = here()[0]
+    half = LANES // 2
+    column = pl.ds(pl.multiple_of(z * LANES, LANES), LANES)
+    *rows, tap_rows = outs
+    for row, ref in zip(rows, (base, correction, group_gain)):
+        row[...] = ref[:, column]
+    zero = jnp.zeros((half, half), F32)
+    state[:half, :] = jnp.concatenate([start[2 * z], zero], axis=1)
+    state[half:, :] = jnp.concatenate([zero, start[2 * z + 1]], axis=1)
+    tap = taps[:, pl.ds(pl.multiple_of((z // 2) * LANES, LANES), LANES)]
+    tap_rows[: taps.shape[0], :] = tap
+
+
+def block_kernel(*refs, step, conditions):
+    count = len(conditions)
+    sources = refs[: 2 * count]
+    w, base, correction = refs[2 * count : 2 * count + 3]
+    *outs, proj, log_keep, x = refs[2 * count + 3 :]
+    z, _, t = here()
+    part = x.shape[0] // 2
+    for at, holds in enumerate(conditions):
+        a, b = sources[2 * at : 2 * at + 2]
+
+        def put(a=a, b=b):
+            x[pl.ds(pl.multiple_of(t * part, 32), part), :] = a[...]
+            x[pl.ds(pl.multiple_of((1 - t) * part, 32), part), :] = b[...]
+
+        put() if holds is None else pl.when(holds(z))(put)
+    block_terms_in(z ^ step, x, w, base, correction, (*outs, proj, log_keep))
+
+
+def final_kernel(*refs, count, width):
+    slots = [refs[7 * i : 7 * (i + 1)] for i in range(count)]
+    start, rows_in, tap, out, conv, gates, local, lead, step, added, kept, conv_rows, y = refs[
+        7 * count :
+    ]
+    z = here()[0]
+    half = LANES // 2
+    first, second, _, _, same = masks()
+    mean_mat = jnp.where(same, 1.0 / half, 0.0).astype(BF)
+    length = conv.shape[1]
+    total_rows = count * length
+    for at, slot in enumerate(slots):
+        position = z ^ at
+        for target, source in zip((conv, gates, local, lead, step, added, kept), slot):
+            target[position] = source[...]
+
+    middle = total_rows // 2
+    pad = conv_rows.shape[0] - middle
+    for block in range(count):
+        pair = conv[block, :, :LANES].astype(F32)
+        conv_in = (pair * pltpu.roll(sigmoid(pair), half, 1)).astype(BF).astype(F32)
+        at = block * length
+        if at < middle:
+            conv_rows[pad + at : pad + at + length, :] = conv_in * first
+            if at + length == middle:
+                conv_rows[:pad, :] = pltpu.roll(conv_in[length - pad :, :], half, 1) * second
+        else:
+            rows = slice(pad + at - middle, pad + at - middle + length)
+            conv_rows[rows, :] = conv_rows[rows, :] + pltpu.roll(conv_in, half, 1) * second
+        out[at : at + length, LANES + half : 2 * LANES] = conv[block, :, LANES : LANES + half]
+    tap = tap[:width, :]
+    odd = (lax.rem(z, 2) == 1).astype(F32)
+    left = iota((1, LANES), 1) < half
+    tap = jnp.where(left == (odd < 0.5), tap, pltpu.roll(tap, half, 1))
+    shift = pad - (width - 1)
+    strip = 96
+    for at in range(0, middle, strip):
+        total = jnp.zeros((strip, LANES), F32)
+        for j in range(width):
+            total = total + tap[j : j + 1, :] * conv_rows[at + shift + j : at + shift + j + strip, :]
+        total = total.astype(BF)
+        out[at : at + strip, LANES : LANES + half] = total[:, :half]
+        out[middle + at : middle + at + strip, LANES : LANES + half] = total[:, half:]
+
+    state = start[...]
+    chunks = length // SPAN
+    for c in range(count * chunks):
+        at = (c // chunks, c % chunks)
+        low = state.astype(BF)
+        seen = dot_nt(lead[at], low)
+        y[c * SPAN : (c + 1) * SPAN, :] = local[at] + seen[:SPAN] + seen[SPAN:]
+        state = state * kept[at][:1] + dot_nn(low, step[at]) + added[at]
+
+    gain_row = rows_in[...]
+    for block in range(count):
+        rows = slice(block * length, (block + 1) * length)
+        values = y[rows, :]
+        high = values.astype(BF)
+        low = (values - high.astype(F32)).astype(BF)
+        centered = values - (dot_nn(high, mean_mat) + dot_nn(low, mean_mat))
+        variance = dot_nn((centered * centered).astype(BF), mean_mat)
+        gate = gates[block].astype(F32)
+        grouped = centered * lax.rsqrt(variance + GROUP_FLOOR) * gain_row
+        out[rows, :LANES] = (grouped * (gate * sigmoid(gate))).astype(BF)
+
+
+def output_kernel(received, point, *refs, groups):
+    *pieces, out, w = refs
+    _, f, t = here()
+    count = pieces[0].shape[0]
+    split = count * LANES // 2
+    wide = count * LANES
+    gains = []
+    for at, piece in enumerate(pieces):
+        core, flip, side = at & 1, (at >> 1) & 1, (at >> 2) & 1
+        group = t ^ side
+        for block in range(count):
+            col = pl.multiple_of((block * count + (f ^ (2 * flip) ^ core)) * LANES, LANES)
+            for start, size, shift in (
+                (0, split, group * split),
+                (split, wide, groups * split + group * wide),
+            ):
+                w[pl.ds(pl.multiple_of(shift, LANES), size), pl.ds(col, LANES)] = piece[
+                    block, start : start + size, :
+                ]
+        if core == flip == 0:
+            spare = piece[0, split + wide :, :].astype(F32)
+            tall = split // LANES
+            parts = [spare[i * tall : (i + 1) * tall, :] for i in range(3)]
+            total = parts[0] + parts[1] + parts[2]
+            gains.append(jnp.concatenate([total[i : i + 1] for i in range(tall)], axis=1))
+    gain = jnp.concatenate(
+        [jnp.where(t == 0, gains[0], gains[1]), jnp.where(t == 0, gains[1], gains[0])], axis=1
+    )
+    half = LANES // 2
+    sums, gates, states = [], [], []
+    for group in range(groups):
+        for block in range(count):
+            source = received[block * groups + group]
+            states.append(source[:, :LANES])
+            sums.append(source[:, LANES : LANES + half])
+            gates.append(source[:, LANES + half :])
+    conv_sum = jnp.concatenate(sums, axis=1).astype(F32)
+    gate = jnp.concatenate(gates, axis=1).astype(F32)
+    mean = jnp.mean(conv_sum, axis=1, keepdims=True)
+    spread = jnp.mean(conv_sum * conv_sum, axis=1, keepdims=True) - mean * mean
+    scaled = (conv_sum - mean) * lax.rsqrt(spread + CHANNEL_FLOOR) * gain
+    shaped = (scaled * sigmoid(scaled)).astype(BF)
+    conv_out = (dot_nn(shaped, point[...]) * (gate * sigmoid(gate))).astype(BF)
+    joined = jnp.concatenate([conv_out] + states, axis=1)
+    out[...] = dot_nn(joined, w[...]).astype(BF)
+
+
+def ordered_kernel(own, *refs):
+    *sources, out = refs
+    z = here()[0]
+    out[z] = own[...]
+    for step, choices in ARRIVALS:
+        for at, holds in choices:
+
+            def put(step=step, at=at):
+                out[z ^ step] = sources[at][...]
+
+            put() if holds is None else pl.when(holds(z))(put)
+
+
+LINE = (
+    ((0, 1), (1, 0), (2, 3), (3, 2)),
+    ((0, 2), (1, 3), (2, 0), (3, 1)),
+    ((1, 2), (2, 1)),
+    ((2, 3), (1, 0)),
+)
+FORWARD = {3: 1}
+
+
+def inner(z):
+    return (z == 1) | (z == 2)
+
+
+def outer(z):
+    return (z == 0) | (z == 3)
+
+
+ARRIVALS = (
+    (1, ((0, None),)),
+    (2, ((1, None),)),
+    (3, ((2, inner), (3, outer))),
+)
+
+
+def along_line(value):
+    moved = []
+    for i, pairs in enumerate(LINE):
+        moved.append(lax.ppermute(moved[FORWARD[i]] if i in FORWARD else value, "sp", pairs))
+    return moved
+
+
+def across(value, pairs):
+    targets = sorted({b for _, b in pairs})
+    return lax.ppermute(
+        value, ("sp", "tp"), [(2 * i + s, 2 * i + 1 - s) for i in targets for s in (0, 1)]
+    )
+
+
+def flipped(value, axis, bit):
+    count = lax.axis_size(axis)
+    return lax.ppermute(value, axis, [(i, i ^ bit) for i in range(count)])
+
+
+def head_body(
+    tokens, decay_pace, start_state, norm_gain, conv_value, conv_admit, conv_gate, state_query,
+    state_key, state_value, state_decay, state_gate, conv_taps, conv_gain, point_weight, decay_base,
+    correction, group_gain, output_conv, output_state,
+):
+    width = tokens.shape[-1]
+    length = tokens.shape[1]
+    count, halves = lax.axis_size("sp"), lax.axis_size("tp")
+    part = length // halves
+    shard = conv_value.shape[0]
+    columns = 7 * LANES
+    slices = call(
+        split_weights_kernel, [((shard, columns), BF)] * count,
+        decay_pace, conv_value, conv_admit, conv_gate, state_query, state_key, state_value, state_decay,
+        state_gate, held=range(9),
+    )
+    taken = [slices[0]] + [flipped(slices[k], "sp", k) for k in range(1, count)]
+    out_rows = output_conv.shape[0] + output_state.shape[0]
+    normed, half, rows_out = call(
+        norm_kernel,
+        [pltpu.HBM((length, width), BF), ((part, width), BF), ((out_rows + SPARE, output_conv.shape[1]), BF)],
+        tokens.reshape(length, width), norm_gain.reshape(1, width), output_conv,
+        output_state, conv_gain.reshape(1, -1), held=range(5),
+    )
+    line_out = along_line(rows_out)
+    near = along_line(half)
+    far = [across(a, LINE[i]) for i, a in enumerate(near)]
+    lifted = [flipped(a, "fs", 2) for a in taken]
+    (mine,) = call(assemble_kernel, [((2 * count * shard, columns), BF)], *taken, *lifted)
+    sibling = flipped(mine, "fs", 1)
+    (ordered,) = call(ordered_kernel, [((count,) + rows_out.shape, BF)], rows_out, *line_out)
+    crossed = flipped(ordered, "tp", 1)
+    pieces = []
+    for a in (ordered, crossed):
+        for b in (a, flipped(a, "fs", 2)):
+            pieces += [b, flipped(b, "fs", 1)]
+    total = length * count
+    rows = total // (count * halves)
+    chunks = length // SPAN
+    terms = [
+        ((length, 2 * LANES), BF),
+        ((length, LANES), BF),
+        ((chunks, SPAN, LANES), F32),
+        ((chunks, LANES, LANES), BF),
+        ((chunks, LANES, LANES), BF),
+        ((chunks, LANES, LANES), F32),
+        ((chunks, 8, LANES), F32),
+    ]
+    work = [((length, columns), F32), ((length, LANES), F32)]
+    heads = start_state.shape[1]
+    kernel = conv_taps.shape[0]
+    begin, *small, gains, tap = call(
+        prepare_kernel,
+        [((LANES, LANES), F32)] + [((1, LANES), F32)] * 3 + [((-(-kernel // 8) * 8, LANES), F32)],
+        start_state.reshape(heads, *start_state.shape[2:]), decay_base.reshape(1, -1),
+        correction.reshape(1, -1), group_gain.reshape(1, -1), conv_taps, held=range(5),
+    )
+    w, *slots = call(
+        own_kernel, [((width, columns), BF)] + terms,
+        normed, mine, sibling, *small, held=(0,), scratch=work,
+    )
+    for step, choices in ARRIVALS:
+        sources = [a for i, _ in choices for a in (near[i], far[i])]
+        slots += call(
+            block_kernel, terms, *sources, w, *small,
+            scratch=work + [((length, width), BF)],
+            step=step, conditions=tuple(holds for _, holds in choices),
+        )
+    mixed = call(
+        final_kernel, [((total, 2 * LANES), BF)], *slots, begin, gains, tap,
+        count=count, width=kernel,
+        scratch=[((count,) + a, b) for a, b in terms]
+        + [((total // 2 + 32, LANES), F32), ((total, LANES), F32)],
+    )[0]
+    received = lax.all_to_all(
+        mixed.reshape(count * halves, rows, 2 * LANES), ("sp", "tp"), 0, 0, tiled=True
+    )
+    (out,) = call(
+        output_kernel, [jax.ShapeDtypeStruct((rows, width), BF)],
+        received, point_weight, *pieces, held=(1,), room=20, groups=halves,
+        scratch=[((halves * out_rows, width), BF)],
+    )
+    return out.reshape(1, rows, width)
 
 
 def passed_along(value, axis, steps):
@@ -231,9 +747,17 @@
     return mixed.astype(jnp.bfloat16).reshape(1, -1, width)
 
 
+def layer(*args):
+    sizes = [lax.axis_size(a) for a in ("sp", "fs", "tp")]
+    channels, wide = args[4].shape[1], args[7].shape[1]
+    whole = channels == sizes[0] * LANES // 2 and wide == sizes[0] * LANES
+    square = args[2].shape[-1] == LANES // 2 and args[4].shape[0] == LANES
+    return (head_body if sizes == [4, 4, 2] and whole and square else body)(*args)
+
+
 def solution(mesh):
     return jax.shard_map(
-        body,
+        layer,
         mesh=mesh,
         in_specs=(
             P("fs", "sp", None),

time: 377 us -> 152 us (0.40)
  other arithmetic: 128 us -> 0 us
  blocking collectives: 61.3 us -> 0 us
  matrix products: 49.8 us -> 0 us
  starting transfers between devices: 2.8 us -> 45.1 us
  Pallas kernels: 0 us -> 29.4 us
  local copies, waits for them, and re-layouts: 27.3 us -> 0 us
  between operations: 14.7 us -> 0.17 us
  waiting for transfers between devices: 89.4 us -> 77.1 us
    another operation x6 -> x0, other arithmetic: 120 us -> none  [the longest x3 119 us: block_terms(): jax.scipy.linalg.solve_triangular(system, right_side, lower=True, unit_di...]
    all_gather x2 -> x0, waiting for transfers between devices: 89.4 us -> none  [the longest x1 89.4 us: body(): lax.all_gather(stacked, ('sp', 'fs'), axis=0, tiled=True)]
    ppermute x1 -> x27, waiting for transfers between devices: 0.01 us -> 65.3 us  [the longest x8 31.6 us: along_line(): lax.ppermute(moved[FORWARD[i]] if i in FORWARD else value, 'sp', pairs)]
    all_gather x6 -> x0, blocking collectives: 52.8 us -> none  [the longest x2 31.8 us: entering_2(): lax.all_gather(a.astype(kind), axis)]
    dot_general x23 -> x0, matrix products: 48.2 us -> none  [the longest x4 8.86 us: pair_terms(): jnp.einsum('hbtc,hbic->hbti', left, right, precision=lax.Precision.HIGHEST)]
    ppermute x1 -> x27, starting transfers between devices: 2.76 us -> 36 us  [the longest x15 15.9 us: flipped(): return lax.ppermute(value, axis, [(i, i ^ bit) for i in range(count)])]
    pallas_call x0 -> x11, Pallas kernels: none -> 29.4 us  [call(): pl.pallas_call(functools.partial(kernel, **settings) if settings else ker...]
    all_to_all x0 -> x1, waiting for transfers between devices: none -> 11.8 us  [head_body(): lax.all_to_all(mixed.reshape(count * halves, rows, 2 * LANES), ('sp', 'tp...]
  transfers between devices with their start and end apart: 3 -> 28, of which waited for: 1 -> 11; matrix products, arithmetic and copies ran while one was open for 51% -> 0% of each run, Pallas kernels for 0% -> 14%
where the time goes in v3:
time: 152 us
  waiting for transfers between devices  77.1 us (51%)
  starting transfers between devices  45.1 us (30%)
  Pallas kernels  29.4 us (19%)
    ppermute x8, waiting for transfers between devices, along_line(): lax.ppermute(moved[FORWARD[i]] if i in FORWARD else value, 'sp', pairs)  31.6 us
    pallas_call x11, Pallas kernels, call(): pl.pallas_call(functools.partial(kernel, **settings) if settings else ker...  29.4 us
    ppermute x15, waiting for transfers between devices, flipped(): return lax.ppermute(value, axis, [(i, i ^ bit) for i in range(count)])  17.9 us
    ppermute x15, starting transfers between devices, flipped(): return lax.ppermute(value, axis, [(i, i ^ bit) for i in range(count)])  15.9 us
    ppermute x4, waiting for transfers between devices, across(): lax.ppermute(value, ('sp', 'tp'), [(2 * i + s, 2 * i + 1 - s) for i in ta...  15.8 us
    ppermute x8, starting transfers between devices, along_line(): lax.ppermute(moved[FORWARD[i]] if i in FORWARD else value, 'sp', pairs)  14.8 us
    all_to_all x1, waiting for transfers between devices, head_body(): lax.all_to_all(mixed.reshape(count * halves, rows, 2 * LANES), ('sp', 'tp...  11.8 us
    all_to_all x1, starting transfers between devices, head_body(): lax.all_to_all(mixed.reshape(count * halves, rows, 2 * LANES), ('sp', 'tp...  9.03 us
  transfers between devices with their start and end apart: 28, of which 11 were waited for; matrix products, arithmetic and copies ran while one was open for 0% of the time, Pallas kernels for 14%

profile of v3, /device:TPU:0, one launch (start us, length us, event | category | flops | bytes accessed | tf_op | source)
XLA Modules:
  0.0 151.7 jit_solution(10441211583049269551)
XLA Ops:
  0.0 2.0 %shard_map.191 = (bf16[128,896]{1,0:T(8,128)(2,1)S(1)}, bf16[128,896]{1,0:T(8,128)(2,1)S(1)}, bf16[128,896]{1,0:T(8,128)(2,1)S(1)}, bf16[128,896]{1,0:T(8,128)(2,1)S(1)}) custom-call(f32[1,192]{1,0:T(1,128)} %refs_0_.1, bf16[128,256]{1,0:T(8,128)(2,1)} %refs_1_.1, bf16[128,256]{1,0:T(8,128)(2,1)} %refs_2_.1, bf16[128,256]{1,0:T(8,128)(2,1)} %refs_3_.1, ...), custom_call_target="tpu_custom_call" | custom-call | tf_op jit(solution)/shard_map/pallas_call | solution.py:107
  2.0 3.1 %collective-permute-start = (bf16[128,896]{1,0:T(8,128)(2,1)S(1)}, bf16[128,896]{1,0:T(8,128)(2,1)S(1)}, u32[]{:S(2)}, u32[]{:S(2)}) collective-permute-start(bf16[128,896]{1,0:T(8,128)(2,1)S(1)} %get-tuple-element.48), channel_id=1, source_target_pairs={{0,8},{8,0},{16,24},{24,16},{1,9},{9,1},{17,25},{25,17},{2,10},{10... | collective-permute-start | bytes 688136 | tf_op jit(solution)/shard_map/ppermute | solution.py:439
  5.1 2.6 %collective-permute-start.1 = (bf16[128,896]{1,0:T(8,128)(2,1)S(1)}, bf16[128,896]{1,0:T(8,128)(2,1)S(1)}, u32[]{:S(2)}, u32[]{:S(2)}) collective-permute-start(bf16[128,896]{1,0:T(8,128)(2,1)S(1)} %get-tuple-element.49), channel_id=1, source_target_pairs={{0,16},{8,24},{16,0},{24,8},{1,17},{9,25},{17,1},{25,9},{2,18},{10... | collective-permute-start | bytes 688136 | tf_op jit(solution)/shard_map/ppermute | solution.py:439
  7.7 0.0 collective-permute-start.2
  7.7 1.7 %collective-permute-start.3 = (bf16[128,896]{1,0:T(8,128)(2,1)S(1)}, bf16[128,896]{1,0:T(8,128)(2,1)S(1)}, u32[]{:S(2)}, u32[]{:S(2)}) collective-permute-start(bf16[128,896]{1,0:T(8,128)(2,1)S(1)} %get-tuple-element.47.refs_0_), channel_id=1, source_target_pairs={{0,4},{2,6},{4,0},{6,2},{1,5},{3,7},{5,1},{7,3},{8,12},{10,14},{12... | collective-permute-start | bytes 688136 | tf_op jit(solution)/shard_map/ppermute | solution.py:439
  9.4 5.4 %collective-permute-done.refs_1_ = bf16[128,896]{1,0:T(8,128)(2,1)S(1)} collective-permute-done((bf16[128,896]{1,0:T(8,128)(2,1)S(1)}, bf16[128,896]{1,0:T(8,128)(2,1)S(1)}, u32[]{:S(2)}, u32[]{:S(2)}) %collective-permute-start) | collective-permute-done | bytes 229408 | tf_op jit(solution)/shard_map/ppermute | solution.py:439
  14.9 1.7 %collective-permute-start.4 = (bf16[128,896]{1,0:T(8,128)(2,1)S(1)}, bf16[128,896]{1,0:T(8,128)(2,1)S(1)}, u32[]{:S(2)}, u32[]{:S(2)}) collective-permute-start(bf16[128,896]{1,0:T(8,128)(2,1)S(1)} %collective-permute-done.refs_1_), channel_id=1, source_target_pairs={{0,4},{2,6},{4,0},{6,2},{1,5},{3,7},{5,1},{7,3},{8,12},{10,14},{12... | collective-permute-start | bytes 688136 | tf_op jit(solution)/shard_map/ppermute | solution.py:439
  16.6 7.7 %collective-permute-done.1.refs_2_ = bf16[128,896]{1,0:T(8,128)(2,1)S(1)} collective-permute-done((bf16[128,896]{1,0:T(8,128)(2,1)S(1)}, bf16[128,896]{1,0:T(8,128)(2,1)S(1)}, u32[]{:S(2)}, u32[]{:S(2)}) %collective-permute-start.1) | collective-permute-done | bytes 229408 | tf_op jit(solution)/shard_map/ppermute | solution.py:439
  24.3 1.5 %collective-permute-start.5 = (bf16[128,896]{1,0:T(8,128)(2,1)S(1)}, bf16[128,896]{1,0:T(8,128)(2,1)S(1)}, u32[]{:S(2)}, u32[]{:S(2)}) collective-permute-start(bf16[128,896]{1,0:T(8,128)(2,1)S(1)} %collective-permute-done.1.refs_2_), channel_id=1, source_target_pairs={{0,4},{2,6},{4,0},{6,2},{1,5},{3,7},{5,1},{7,3},{8,12},{10,14},{12... | collective-permute-start | bytes 688136 | tf_op jit(solution)/shard_map/ppermute | solution.py:439
  25.8 0.0 collective-permute-done.2.refs_3_
  25.8 0.5 collective-permute-start.6
  26.3 2.4 %shard_map.190 = (bf16[192,2048]{1,0:T(8,128)(2,1)}, bf16[96,2048]{1,0:T(8,128)(2,1)S(1)}, bf16[784,128]{1,0:T(8,128)(2,1)S(1)}) custom-call(bf16[192,2048]{1,0:T(8,128)(2,1)} %bitcast.9, f32[1,2048]{1,0:T(1,128)} %bitcast.11, bf16[256,128]{1,0:T(8,128)(2,1)} %out_conv.1, bf16[512,128]{1,0:T(8,128)(2,1)} %out_state.1, f32[1,256]{1,0:T(1,128)} %bitcast.15), custom_call_target="tpu_custom_call" | custom-call | tf_op jit(solution)/shard_map/pallas_call | solution.py:107
  28.8 4.6 %collective-permute-start.17 = (bf16[784,128]{1,0:T(8,128)(2,1)S(1)}, bf16[784,128]{1,0:T(8,128)(2,1)S(1)}, u32[]{:S(2)}, u32[]{:S(2)}) collective-permute-start(bf16[784,128]{1,0:T(8,128)(2,1)S(1)} %get-tuple-element.86.own), channel_id=1, source_target_pairs={{0,16},{8,24},{16,0},{24,8},{1,17},{9,25},{17,1},{25,9},{2,18},{10... | collective-permute-start | bytes 602120 | tf_op jit(solution)/shard_map/ppermute | solution.py:426
  33.4 0.0 collective-permute-done.3.refs_4_
  33.4 0.0 collective-permute-done.4.refs_5_
  33.4 0.0 collective-permute-done.5.refs_6_
  33.4 0.0 collective-permute-done.6.refs_7_
  33.4 0.1 shard_map.192.mine
  33.6 0.1 collective-permute-start.7
  33.6 1.5 %collective-permute-start.16 = (bf16[784,128]{1,0:T(8,128)(2,1)S(1)}, bf16[784,128]{1,0:T(8,128)(2,1)S(1)}, u32[]{:S(2)}, u32[]{:S(2)}) collective-permute-start(bf16[784,128]{1,0:T(8,128)(2,1)S(1)} %get-tuple-element.86.own), channel_id=1, source_target_pairs={{0,8},{8,0},{16,24},{24,16},{1,9},{9,1},{17,25},{25,17},{2,10},{10... | collective-permute-start | bytes 602120 | tf_op jit(solution)/shard_map/ppermute | solution.py:426
  35.2 0.7 collective-permute-start.18
  35.9 6.7 %collective-permute-done.17.refs_1_ = bf16[784,128]{1,0:T(8,128)(2,1)S(1)} collective-permute-done((bf16[784,128]{1,0:T(8,128)(2,1)S(1)}, bf16[784,128]{1,0:T(8,128)(2,1)S(1)}, u32[]{:S(2)}, u32[]{:S(2)}) %collective-permute-start.17) | collective-permute-done | bytes 200736 | tf_op jit(solution)/shard_map/ppermute | solution.py:426
  42.5 1.3 collective-permute-start.19
  43.8 0.1 collective-permute-done.16.refs_0_
  43.9 0.0 collective-permute-done.18.refs_2_
  43.9 6.2 %collective-permute-done.19.refs_3_ = bf16[784,128]{1,0:T(8,128)(2,1)S(1)} collective-permute-done((bf16[784,128]{1,0:T(8,128)(2,1)S(1)}, bf16[784,128]{1,0:T(8,128)(2,1)S(1)}, u32[]{:S(2)}, u32[]{:S(2)}) %collective-permute-start.19) | collective-permute-done | bytes 200736 | tf_op jit(solution)/shard_map/ppermute | solution.py:426
  50.1 0.1 shard_map.199.refs_0_
  50.2 1.6 %collective-permute-start.23 = (bf16[4,784,128]{2,1,0:T(8,128)(2,1)S(1)}, bf16[4,784,128]{2,1,0:T(8,128)(2,1)S(1)}, u32[]{:S(2)}, u32[]{:S(2)}) collective-permute-start(bf16[4,784,128]{2,1,0:T(8,128)(2,1)S(1)} %shard_map.199.refs_0_), channel_id=1, source_target_pairs={{0,1},{1,0},{2,3},{3,2},{4,5},{5,4},{6,7},{7,6},{8,9},{9,8},{10,11... | collective-permute-start | bytes 2408456 | tf_op jit(solution)/shard_map/ppermute | solution.py:439
  51.8 0.4 collective-permute-start.10
  52.1 0.7 collective-permute-start.12
  52.8 4.4 %collective-permute-start.8 = (bf16[96,2048]{1,0:T(8,128)(2,1)S(1)}, bf16[96,2048]{1,0:T(8,128)(2,1)S(1)}, u32[]{:S(2)}, u32[]{:S(2)}) collective-permute-start(bf16[96,2048]{1,0:T(8,128)(2,1)S(1)} %get-tuple-element.60), channel_id=1, source_target_pairs={{0,8},{8,0},{16,24},{24,16},{1,9},{9,1},{17,25},{25,17},{2,10},{10... | collective-permute-start | bytes 1179656 | tf_op jit(solution)/shard_map/ppermute | solution.py:426
  57.2 11.3 %collective-permute-done.10.refs_0_ = bf16[96,2048]{1,0:T(8,128)(2,1)S(1)} collective-permute-done((bf16[96,2048]{1,0:T(8,128)(2,1)S(1)}, bf16[96,2048]{1,0:T(8,128)(2,1)S(1)}, u32[]{:S(2)}, u32[]{:S(2)}) %collective-permute-start.10) | collective-permute-done | bytes 393248 | tf_op jit(solution)/shard_map/ppermute | solution.py:426
  68.5 1.3 collective-permute-start.14
  69.8 0.0 collective-permute-done.12.refs_0_
  69.8 0.1 collective-permute-start.21
  69.9 0.0 collective-permute-done.23.refs_4_
  69.9 2.0 %collective-permute-start.25 = (bf16[4,784,128]{2,1,0:T(8,128)(2,1)S(1)}, bf16[4,784,128]{2,1,0:T(8,128)(2,1)}, u32[]{:S(2)}, u32[]{:S(2)}) collective-permute-start(bf16[4,784,128]{2,1,0:T(8,128)(2,1)S(1)} %collective-permute-done.23.refs_4_), channel_id=1, source_target_pairs={{0,4},{2,6},{4,0},{6,2},{1,5},{3,7},{5,1},{7,3},{8,12},{10,14},{12... | collective-permute-start | bytes 2408456 | tf_op jit(solution)/shard_map/ppermute | solution.py:439
  71.9 0.0 collective-permute-done.8.refs_0_
  71.9 0.7 collective-permute-start.13
  72.6 7.4 %collective-permute-done.14.refs_2_ = bf16[96,2048]{1,0:T(8,128)(2,1)S(1)} collective-permute-done((bf16[96,2048]{1,0:T(8,128)(2,1)S(1)}, bf16[96,2048]{1,0:T(8,128)(2,1)S(1)}, u32[]{:S(2)}, u32[]{:S(2)}) %collective-permute-start.14) | collective-permute-done | bytes 393248 | tf_op jit(solution)/shard_map/ppermute | solution.py:426
  80.0 0.7 collective-permute-start.11
  80.7 1.3 collective-permute-start.9
  82.0 10.0 %collective-permute-done.11.refs_1_ = bf16[96,2048]{1,0:T(8,128)(2,1)S(1)} collective-permute-done((bf16[96,2048]{1,0:T(8,128)(2,1)S(1)}, bf16[96,2048]{1,0:T(8,128)(2,1)S(1)}, u32[]{:S(2)}, u32[]{:S(2)}) %collective-permute-start.11) | collective-permute-done | bytes 393248 | tf_op jit(solution)/shard_map/ppermute | solution.py:432
  92.0 2.6 %collective-permute-start.15 = (bf16[96,2048]{1,0:T(8,128)(2,1)S(1)}, bf16[96,2048]{1,0:T(8,128)(2,1)S(1)}, u32[]{:S(2)}, u32[]{:S(2)}) collective-permute-start(bf16[96,2048]{1,0:T(8,128)(2,1)S(1)} %collective-permute-done.14.refs_2_), channel_id=1, source_target_pairs={{0,1},{1,0},{24,25},{25,24},{2,3},{3,2},{26,27},{27,26},{4,5},{5,4... | collective-permute-start | bytes 1179656 | tf_op jit(solution)/shard_map/ppermute | solution.py:432
  94.6 5.8 %collective-permute-done.9.refs_1_ = bf16[96,2048]{1,0:T(8,128)(2,1)S(1)} collective-permute-done((bf16[96,2048]{1,0:T(8,128)(2,1)S(1)}, bf16[96,2048]{1,0:T(8,128)(2,1)S(1)}, u32[]{:S(2)}, u32[]{:S(2)}) %collective-permute-start.9) | collective-permute-done | bytes 393248 | tf_op jit(solution)/shard_map/ppermute | solution.py:432
  100.4 0.0 collective-permute-start.20
  100.4 0.0 collective-permute-done.21.refs_2_
  100.4 0.5 collective-permute-start.24
  100.9 4.6 %collective-permute-done.25.refs_6_ = bf16[4,784,128]{2,1,0:T(8,128)(2,1)} collective-permute-done((bf16[4,784,128]{2,1,0:T(8,128)(2,1)S(1)}, bf16[4,784,128]{2,1,0:T(8,128)(2,1)}, u32[]{:S(2)}, u32[]{:S(2)}) %collective-permute-start.25) | collective-permute-done | bytes 802848 | tf_op jit(solution)/shard_map/ppermute | solution.py:439
  105.5 0.0 collective-permute-start.22
  105.5 0.0 collective-permute-done.7.sibling
  105.5 0.5 collective-permute-start.26
  106.0 1.1 shard_map.193
  107.1 4.6 %shard_map.194 = (bf16[2048,896]{1,0:T(8,128)(2,1)S(1)}, bf16[192,256]{1,0:T(8,128)(2,1)S(1)}, bf16[192,128]{1,0:T(8,128)(2,1)S(1)}, f32[3,64,128]{2,1,0:T(8,128...) custom-call(bf16[192,2048]{1,0:T(8,128)(2,1)} %get-tuple-element.46., ...), custom_call_target="tpu_custom_call" | custom-call | tf_op jit(solution)/shard_map/pallas_call | solution.py:107
  111.7 3.2 %shard_map.196 = (bf16[192,256]{1,0:T(8,128)(2,1)S(1)}, bf16[192,128]{1,0:T(8,128)(2,1)S(1)}, f32[3,64,128]{2,1,0:T(8,128)S(1)}, bf16[3,128,128]{2,1,0:T(8,128)(...) custom-call(bf16[96,2048]{1,0:T(8,128)(2,1)S(1)} %collective-permute-done.10.refs_0, ...), custom_call_target="tpu_custom_call" | custom-call | tf_op jit(solution)/shard_map/pallas_call | solution.py:107
  114.9 3.2 %shard_map.195 = (bf16[192,256]{1,0:T(8,128)(2,1)S(1)}, bf16[192,128]{1,0:T(8,128)(2,1)S(1)}, f32[3,64,128]{2,1,0:T(8,128)S(1)}, bf16[3,128,128]{2,1,0:T(8,128)(...) custom-call(bf16[96,2048]{1,0:T(8,128)(2,1)S(1)} %collective-permute-done.8.refs_0_, ...), custom_call_target="tpu_custom_call" | custom-call | tf_op jit(solution)/shard_map/pallas_call | solution.py:107
  118.1 3.4 %shard_map.197 = (bf16[192,256]{1,0:T(8,128)(2,1)S(1)}, bf16[192,128]{1,0:T(8,128)(2,1)S(1)}, f32[3,64,128]{2,1,0:T(8,128)S(1)}, bf16[3,128,128]{2,1,0:T(8,128)(...) custom-call(bf16[96,2048]{1,0:T(8,128)(2,1)S(1)} %collective-permute-done.12.refs_0, ...), custom_call_target="tpu_custom_call" | custom-call | tf_op jit(solution)/shard_map/pallas_call | solution.py:107
  121.5 3.2 %shard_map.198 = bf16[768,256]{1,0:T(8,128)(2,1)} custom-call(bf16[192,256]{1,0:T(8,128)(2,1)S(1)} %get-tuple-element.53.refs_0_, bf16[192,128]{1,0:T(8,128)(2,1)S(1)} %get-tuple-element.54.refs_1_, f32[3,64,128]{2,1,0:T(8,128)S(1)} %get-tuple-element.55.refs_2_, bf16[3,128,128]{2,1,0:T(8,128)(2,1)S(1)} %get-tuple-element.56.refs_3_, ...), custom_call_target="tpu_custom_call" | custom-call | tf_op jit(solution)/shard_map/pallas_call | solution.py:107
  124.7 9.0 %all-to-all-start = ((bf16[8,96,256]{2,1,0:T(8,128)(2,1)}), bf16[8,96,256]{2,1,0:T(8,128)(2,1)S(1)}, u32[]{:S(2)}, u32[]{:S(2)}) async-start(bf16[8,96,256]{2,1,0:T(8,128)(2,1)} %bitcast.7), calls=%async_computation | async-start | bytes 786432 | tf_op jit(solution)/shard_map/all_to_all | solution.py:516
  133.7 0.0 collective-permute-done.20.refs_1_
  133.7 0.0 collective-permute-done.24.refs_5_
  133.7 0.0 collective-permute-done.22.refs_3_
  133.8 11.8 %all-to-all-done.received = bf16[8,96,256]{2,1,0:T(8,128)(2,1)S(1)} async-done(((bf16[8,96,256]{2,1,0:T(8,128)(2,1)}), bf16[8,96,256]{2,1,0:T(8,128)(2,1)S(1)}, u32[]{:S(2)}, u32[]{:S(2)}) %all-to-all-start) | async-done | bytes 393248 | tf_op jit(solution)/shard_map/all_to_all | solution.py:516
  145.6 6.2 %shard_map.200 = bf16[96,2048]{1,0:T(8,128)(2,1)} custom-call(bf16[8,96,256]{2,1,0:T(8,128)(2,1)S(1)} %all-to-all-done.received, bf16[512,512]{1,0:T(8,128)(2,1)} %point.1, bf16[4,784,128]{2,1,0:T(8,128)(2,1)S(1)} %shard_map.199.refs_0_, bf16[4,784,128]{2,1,0:T(8,128)(2,1)} %collective-permute-done.20.refs_1_, ...), custom_call_target="tpu_custom_call" | custom-call | tf_op jit(solution)/shard_map/pallas_call | solution.py:107
  (3 shorter events, 0.0 us)
Async XLA Ops:
  2.0 12.9 %collective-permute-start = (bf16[128,896]{1,0:T(8,128)(2,1)S(1)}, bf16[128,896]{1,0:T(8,128)(2,1)S(1)}, u32[]{:S(2)}, u32[]{:S(2)}) collective-permute-start(bf16[128,896]{1,0:T(8,128)(2,1)S(1)} %get-tuple-element.48), channel_id=1, source_target_pairs={{0,8},{8,0},{16,24},{24,16},{1,9},{9,1},{17,25},{25,17},{2,10},{10... | collective-permute-start | bytes 688136 | tf_op jit(solution)/shard_map/ppermute | solution.py:439
  5.1 19.2 %collective-permute-start.1 = (bf16[128,896]{1,0:T(8,128)(2,1)S(1)}, bf16[128,896]{1,0:T(8,128)(2,1)S(1)}, u32[]{:S(2)}, u32[]{:S(2)}) collective-permute-start(bf16[128,896]{1,0:T(8,128)(2,1)S(1)} %get-tuple-element.49), channel_id=1, source_target_pairs={{0,16},{8,24},{16,0},{24,8},{1,17},{9,25},{17,1},{25,9},{2,18},{10... | collective-permute-start | bytes 688136 | tf_op jit(solution)/shard_map/ppermute | solution.py:439
  7.7 18.1 %collective-permute-start.2 = (bf16[128,896]{1,0:T(8,128)(2,1)S(1)}, bf16[128,896]{1,0:T(8,128)(2,1)S(1)}, u32[]{:S(2)}, u32[]{:S(2)}) collective-permute-start(bf16[128,896]{1,0:T(8,128)(2,1)S(1)} %get-tuple-element.50), channel_id=1, source_target_pairs={{0,24},{8,16},{16,8},{24,0},{1,25},{9,17},{17,9},{25,1},{2,26},{10... | collective-permute-start | bytes 688136 | tf_op jit(solution)/shard_map/ppermute | solution.py:439
  7.7 25.7 %collective-permute-start.3 = (bf16[128,896]{1,0:T(8,128)(2,1)S(1)}, bf16[128,896]{1,0:T(8,128)(2,1)S(1)}, u32[]{:S(2)}, u32[]{:S(2)}) collective-permute-start(bf16[128,896]{1,0:T(8,128)(2,1)S(1)} %get-tuple-element.47.refs_0_), channel_id=1, source_target_pairs={{0,4},{2,6},{4,0},{6,2},{1,5},{3,7},{5,1},{7,3},{8,12},{10,14},{12... | collective-permute-start | bytes 688136 | tf_op jit(solution)/shard_map/ppermute | solution.py:439
  14.9 18.5 %collective-permute-start.4 = (bf16[128,896]{1,0:T(8,128)(2,1)S(1)}, bf16[128,896]{1,0:T(8,128)(2,1)S(1)}, u32[]{:S(2)}, u32[]{:S(2)}) collective-permute-start(bf16[128,896]{1,0:T(8,128)(2,1)S(1)} %collective-permute-done.refs_1_), channel_id=1, source_target_pairs={{0,4},{2,6},{4,0},{6,2},{1,5},{3,7},{5,1},{7,3},{8,12},{10,14},{12... | collective-permute-start | bytes 688136 | tf_op jit(solution)/shard_map/ppermute | solution.py:439
  24.3 9.1 %collective-permute-start.5 = (bf16[128,896]{1,0:T(8,128)(2,1)S(1)}, bf16[128,896]{1,0:T(8,128)(2,1)S(1)}, u32[]{:S(2)}, u32[]{:S(2)}) collective-permute-start(bf16[128,896]{1,0:T(8,128)(2,1)S(1)} %collective-permute-done.1.refs_2_), channel_id=1, source_target_pairs={{0,4},{2,6},{4,0},{6,2},{1,5},{3,7},{5,1},{7,3},{8,12},{10,14},{12... | collective-permute-start | bytes 688136 | tf_op jit(solution)/shard_map/ppermute | solution.py:439
  25.8 7.6 %collective-permute-start.6 = (bf16[128,896]{1,0:T(8,128)(2,1)S(1)}, bf16[128,896]{1,0:T(8,128)(2,1)S(1)}, u32[]{:S(2)}, u32[]{:S(2)}) collective-permute-start(bf16[128,896]{1,0:T(8,128)(2,1)S(1)} %collective-permute-done.2.refs_3_), channel_id=1, source_target_pairs={{0,4},{2,6},{4,0},{6,2},{1,5},{3,7},{5,1},{7,3},{8,12},{10,14},{12... | collective-permute-start | bytes 688136 | tf_op jit(solution)/shard_map/ppermute | solution.py:439
  28.8 13.7 %collective-permute-start.17 = (bf16[784,128]{1,0:T(8,128)(2,1)S(1)}, bf16[784,128]{1,0:T(8,128)(2,1)S(1)}, u32[]{:S(2)}, u32[]{:S(2)}) collective-permute-start(bf16[784,128]{1,0:T(8,128)(2,1)S(1)} %get-tuple-element.86.own), channel_id=1, source_target_pairs={{0,16},{8,24},{16,0},{24,8},{1,17},{9,25},{17,1},{25,9},{2,18},{10... | collective-permute-start | bytes 602120 | tf_op jit(solution)/shard_map/ppermute | solution.py:426
  33.6 72.0 %collective-permute-start.7 = (bf16[1024,896]{1,0:T(8,128)(2,1)S(1)}, bf16[1024,896]{1,0:T(8,128)(2,1)S(1)}, u32[]{:S(2)}, u32[]{:S(2)}) collective-permute-start(bf16[1024,896]{1,0:T(8,128)(2,1)S(1)} %shard_map.192.mine), channel_id=1, source_target_pairs={{0,2},{2,0},{4,6},{6,4},{1,3},{3,1},{5,7},{7,5},{8,10},{10,8},{12,... | collective-permute-start | bytes 5505032 | tf_op jit(solution)/shard_map/ppermute | solution.py:439
  33.6 10.3 %collective-permute-start.16 = (bf16[784,128]{1,0:T(8,128)(2,1)S(1)}, bf16[784,128]{1,0:T(8,128)(2,1)S(1)}, u32[]{:S(2)}, u32[]{:S(2)}) collective-permute-start(bf16[784,128]{1,0:T(8,128)(2,1)S(1)} %get-tuple-element.86.own), channel_id=1, source_target_pairs={{0,8},{8,0},{16,24},{24,16},{1,9},{9,1},{17,25},{25,17},{2,10},{10... | collective-permute-start | bytes 602120 | tf_op jit(solution)/shard_map/ppermute | solution.py:426
  35.2 8.7 %collective-permute-start.18 = (bf16[784,128]{1,0:T(8,128)(2,1)S(1)}, bf16[784,128]{1,0:T(8,128)(2,1)S(1)}, u32[]{:S(2)}, u32[]{:S(2)}) collective-permute-start(bf16[784,128]{1,0:T(8,128)(2,1)S(1)} %get-tuple-element.86.own), channel_id=1, source_target_pairs={{8,16},{16,8},{9,17},{17,9},{10,18},{18,10},{11,19},{19,11},{12,20... | collective-permute-start | bytes 602120 | tf_op jit(solution)/shard_map/ppermute | solution.py:426
  42.5 7.6 %collective-permute-start.19 = (bf16[784,128]{1,0:T(8,128)(2,1)S(1)}, bf16[784,128]{1,0:T(8,128)(2,1)S(1)}, u32[]{:S(2)}, u32[]{:S(2)}) collective-permute-start(bf16[784,128]{1,0:T(8,128)(2,1)S(1)} %collective-permute-done.17.refs_1_), channel_id=1, source_target_pairs={{16,24},{8,0},{17,25},{9,1},{18,26},{10,2},{19,27},{11,3},{20,28},... | collective-permute-start | bytes 602120 | tf_op jit(solution)/shard_map/ppermute | solution.py:426
  50.2 19.7 %collective-permute-start.23 = (bf16[4,784,128]{2,1,0:T(8,128)(2,1)S(1)}, bf16[4,784,128]{2,1,0:T(8,128)(2,1)S(1)}, u32[]{:S(2)}, u32[]{:S(2)}) collective-permute-start(bf16[4,784,128]{2,1,0:T(8,128)(2,1)S(1)} %shard_map.199.refs_0_), channel_id=1, source_target_pairs={{0,1},{1,0},{2,3},{3,2},{4,5},{5,4},{6,7},{7,6},{8,9},{9,8},{10,11... | collective-permute-start | bytes 2408456 | tf_op jit(solution)/shard_map/ppermute | solution.py:439
  51.8 16.8 %collective-permute-start.10 = (bf16[96,2048]{1,0:T(8,128)(2,1)S(1)}, bf16[96,2048]{1,0:T(8,128)(2,1)S(1)}, u32[]{:S(2)}, u32[]{:S(2)}) collective-permute-start(bf16[96,2048]{1,0:T(8,128)(2,1)S(1)} %get-tuple-element.60), channel_id=1, source_target_pairs={{0,16},{8,24},{16,0},{24,8},{1,17},{9,25},{17,1},{25,9},{2,18},{10... | collective-permute-start | bytes 1179656 | tf_op jit(solution)/shard_map/ppermute | solution.py:426
  52.1 17.7 %collective-permute-start.12 = (bf16[96,2048]{1,0:T(8,128)(2,1)S(1)}, bf16[96,2048]{1,0:T(8,128)(2,1)S(1)}, u32[]{:S(2)}, u32[]{:S(2)}) collective-permute-start(bf16[96,2048]{1,0:T(8,128)(2,1)S(1)} %get-tuple-element.60), channel_id=1, source_target_pairs={{8,16},{16,8},{9,17},{17,9},{10,18},{18,10},{11,19},{19,11},{12,20... | collective-permute-start | bytes 1179656 | tf_op jit(solution)/shard_map/ppermute | solution.py:426
  52.8 19.1 %collective-permute-start.8 = (bf16[96,2048]{1,0:T(8,128)(2,1)S(1)}, bf16[96,2048]{1,0:T(8,128)(2,1)S(1)}, u32[]{:S(2)}, u32[]{:S(2)}) collective-permute-start(bf16[96,2048]{1,0:T(8,128)(2,1)S(1)} %get-tuple-element.60), channel_id=1, source_target_pairs={{0,8},{8,0},{16,24},{24,16},{1,9},{9,1},{17,25},{25,17},{2,10},{10... | collective-permute-start | bytes 1179656 | tf_op jit(solution)/shard_map/ppermute | solution.py:426
  68.5 11.4 %collective-permute-start.14 = (bf16[96,2048]{1,0:T(8,128)(2,1)S(1)}, bf16[96,2048]{1,0:T(8,128)(2,1)S(1)}, u32[]{:S(2)}, u32[]{:S(2)}) collective-permute-start(bf16[96,2048]{1,0:T(8,128)(2,1)S(1)} %collective-permute-done.10.refs_0_), channel_id=1, source_target_pairs={{16,24},{8,0},{17,25},{9,1},{18,26},{10,2},{19,27},{11,3},{20,28},... | collective-permute-start | bytes 1179656 | tf_op jit(solution)/shard_map/ppermute | solution.py:426
  69.8 30.6 %collective-permute-start.21 = (bf16[4,784,128]{2,1,0:T(8,128)(2,1)S(1)}, bf16[4,784,128]{2,1,0:T(8,128)(2,1)S(1)}, u32[]{:S(2)}, u32[]{:S(2)}) collective-permute-start(bf16[4,784,128]{2,1,0:T(8,128)(2,1)S(1)} %shard_map.199.refs_0_), channel_id=1, source_target_pairs={{0,4},{2,6},{4,0},{6,2},{1,5},{3,7},{5,1},{7,3},{8,12},{10,14},{12... | collective-permute-start | bytes 2408456 | tf_op jit(solution)/shard_map/ppermute | solution.py:439
  69.9 35.6 %collective-permute-start.25 = (bf16[4,784,128]{2,1,0:T(8,128)(2,1)S(1)}, bf16[4,784,128]{2,1,0:T(8,128)(2,1)}, u32[]{:S(2)}, u32[]{:S(2)}) collective-permute-start(bf16[4,784,128]{2,1,0:T(8,128)(2,1)S(1)} %collective-permute-done.23.refs_4_), channel_id=1, source_target_pairs={{0,4},{2,6},{4,0},{6,2},{1,5},{3,7},{5,1},{7,3},{8,12},{10,14},{12... | collective-permute-start | bytes 2408456 | tf_op jit(solution)/shard_map/ppermute | solution.py:439
  71.9 8.7 %collective-permute-start.13 = (bf16[96,2048]{1,0:T(8,128)(2,1)S(1)}, bf16[96,2048]{1,0:T(8,128)(2,1)S(1)}, u32[]{:S(2)}, u32[]{:S(2)}) collective-permute-start(bf16[96,2048]{1,0:T(8,128)(2,1)S(1)} %collective-permute-done.12.refs_0_), channel_id=1, source_target_pairs={{8,9},{9,8},{16,17},{17,16},{10,11},{11,10},{18,19},{19,18},{12,13... | collective-permute-start | bytes 1179656 | tf_op jit(solution)/shard_map/ppermute | solution.py:432
  80.0 12.0 %collective-permute-start.11 = (bf16[96,2048]{1,0:T(8,128)(2,1)S(1)}, bf16[96,2048]{1,0:T(8,128)(2,1)S(1)}, u32[]{:S(2)}, u32[]{:S(2)}) collective-permute-start(bf16[96,2048]{1,0:T(8,128)(2,1)S(1)} %collective-permute-done.10.refs_0_), channel_id=1, source_target_pairs={{0,1},{1,0},{8,9},{9,8},{16,17},{17,16},{24,25},{25,24},{2,3},{3,2... | collective-permute-start | bytes 1179656 | tf_op jit(solution)/shard_map/ppermute | solution.py:432
  80.7 19.7 %collective-permute-start.9 = (bf16[96,2048]{1,0:T(8,128)(2,1)S(1)}, bf16[96,2048]{1,0:T(8,128)(2,1)S(1)}, u32[]{:S(2)}, u32[]{:S(2)}) collective-permute-start(bf16[96,2048]{1,0:T(8,128)(2,1)S(1)} %collective-permute-done.8.refs_0_), channel_id=1, source_target_pairs={{0,1},{1,0},{8,9},{9,8},{16,17},{17,16},{24,25},{25,24},{2,3},{3,2... | collective-permute-start | bytes 1179656 | tf_op jit(solution)/shard_map/ppermute | solution.py:432
  92.0 26.1 %collective-permute-start.15 = (bf16[96,2048]{1,0:T(8,128)(2,1)S(1)}, bf16[96,2048]{1,0:T(8,128)(2,1)S(1)}, u32[]{:S(2)}, u32[]{:S(2)}) collective-permute-start(bf16[96,2048]{1,0:T(8,128)(2,1)S(1)} %collective-permute-done.14.refs_2_), channel_id=1, source_target_pairs={{0,1},{1,0},{24,25},{25,24},{2,3},{3,2},{26,27},{27,26},{4,5},{5,4... | collective-permute-start | bytes 1179656 | tf_op jit(solution)/shard_map/ppermute | solution.py:432
  100.4 33.4 %collective-permute-start.20 = (bf16[4,784,128]{2,1,0:T(8,128)(2,1)S(1)}, bf16[4,784,128]{2,1,0:T(8,128)(2,1)}, u32[]{:S(2)}, u32[]{:S(2)}) collective-permute-start(bf16[4,784,128]{2,1,0:T(8,128)(2,1)S(1)} %shard_map.199.refs_0_), channel_id=1, source_target_pairs={{0,2},{2,0},{4,6},{6,4},{1,3},{3,1},{5,7},{7,5},{8,10},{10,8},{12,... | collective-permute-start | bytes 2408456 | tf_op jit(solution)/shard_map/ppermute | solution.py:439
  100.4 33.4 %collective-permute-start.24 = (bf16[4,784,128]{2,1,0:T(8,128)(2,1)S(1)}, bf16[4,784,128]{2,1,0:T(8,128)(2,1)}, u32[]{:S(2)}, u32[]{:S(2)}) collective-permute-start(bf16[4,784,128]{2,1,0:T(8,128)(2,1)S(1)} %collective-permute-done.23.refs_4_), channel_id=1, source_target_pairs={{0,2},{2,0},{4,6},{6,4},{1,3},{3,1},{5,7},{7,5},{8,10},{10,8},{12,... | collective-permute-start | bytes 2408456 | tf_op jit(solution)/shard_map/ppermute | solution.py:439
  105.5 28.2 %collective-permute-start.22 = (bf16[4,784,128]{2,1,0:T(8,128)(2,1)S(1)}, bf16[4,784,128]{2,1,0:T(8,128)(2,1)}, u32[]{:S(2)}, u32[]{:S(2)}) collective-permute-start(bf16[4,784,128]{2,1,0:T(8,128)(2,1)S(1)} %collective-permute-done.21.refs_2_), channel_id=1, source_target_pairs={{0,2},{2,0},{4,6},{6,4},{1,3},{3,1},{5,7},{7,5},{8,10},{10,8},{12,... | collective-permute-start | bytes 2408456 | tf_op jit(solution)/shard_map/ppermute | solution.py:439
  105.5 28.2 %collective-permute-start.26 = (bf16[4,784,128]{2,1,0:T(8,128)(2,1)}, bf16[4,784,128]{2,1,0:T(8,128)(2,1)}, u32[]{:S(2)}, u32[]{:S(2)}) collective-permute-start(bf16[4,784,128]{2,1,0:T(8,128)(2,1)} %collective-permute-done.25.refs_6_), channel_id=1, source_target_pairs={{0,2},{2,0},{4,6},{6,4},{1,3},{3,1},{5,7},{7,5},{8,10},{10,8},{12,... | collective-permute-start | bytes 2408456 | tf_op jit(solution)/shard_map/ppermute | solution.py:439
  124.7 20.9 %all-to-all-start = ((bf16[8,96,256]{2,1,0:T(8,128)(2,1)}), bf16[8,96,256]{2,1,0:T(8,128)(2,1)S(1)}, u32[]{:S(2)}, u32[]{:S(2)}) async-start(bf16[8,96,256]{2,1,0:T(8,128)(2,1)} %bitcast.7), calls=%async_computation | async-start | bytes 786432 | tf_op jit(solution)/shard_map/all_to_all | solution.py:516

commit v4 on v3

--- a/solution.py
+++ b/solution.py
@@ -336,8 +336,8 @@
         out[rows, :LANES] = (grouped * (gate * sigmoid(gate))).astype(BF)
 
 
-def output_kernel(received, point, *refs, groups):
-    *pieces, out, w = refs
+def join_kernel(*refs, groups):
+    *pieces, w, all_gains = refs
     _, f, t = here()
     count = pieces[0].shape[0]
     split = count * LANES // 2
@@ -361,9 +361,20 @@
             parts = [spare[i * tall : (i + 1) * tall, :] for i in range(3)]
             total = parts[0] + parts[1] + parts[2]
             gains.append(jnp.concatenate([total[i : i + 1] for i in range(tall)], axis=1))
-    gain = jnp.concatenate(
+    all_gains[...] = jnp.concatenate(
         [jnp.where(t == 0, gains[0], gains[1]), jnp.where(t == 0, gains[1], gains[0])], axis=1
     )
+
+
+def output_kernel(received, point, gain, rows_in, out, w, sems, *, groups):
+    count = received.shape[0] // groups
+    wide = w.shape[1] // count
+    columns = [pl.ds(i * wide, wide) for i in range(count)]
+    copies = [
+        pltpu.make_async_copy(rows_in.at[:, c], w.at[:, c], sems.at[i]) for i, c in enumerate(columns)
+    ]
+    for copy in copies:
+        copy.start()
     half = LANES // 2
     sums, gates, states = [], [], []
     for group in range(groups):
@@ -376,11 +387,13 @@
     gate = jnp.concatenate(gates, axis=1).astype(F32)
     mean = jnp.mean(conv_sum, axis=1, keepdims=True)
     spread = jnp.mean(conv_sum * conv_sum, axis=1, keepdims=True) - mean * mean
-    scaled = (conv_sum - mean) * lax.rsqrt(spread + CHANNEL_FLOOR) * gain
+    scaled = (conv_sum - mean) * lax.rsqrt(spread + CHANNEL_FLOOR) * gain[...]
     shaped = (scaled * sigmoid(scaled)).astype(BF)
     conv_out = (dot_nn(shaped, point[...]) * (gate * sigmoid(gate))).astype(BF)
     joined = jnp.concatenate([conv_out] + states, axis=1)
-    out[...] = dot_nn(joined, w[...]).astype(BF)
+    for c, copy in zip(columns, copies):
+        copy.wait()
+        out[:, c] = dot_nn(joined, w[:, c]).astype(BF)
 
 
 def ordered_kernel(own, *refs):
@@ -516,10 +529,18 @@
     received = lax.all_to_all(
         mixed.reshape(count * halves, rows, 2 * LANES), ("sp", "tp"), 0, 0, tiled=True
     )
+    w_out, gain = call(
+        join_kernel,
+        [
+            pltpu.HBM((halves * out_rows, width), BF),
+            ((1, halves * conv_gain.shape[0]), F32),
+        ],
+        *pieces, room=20, groups=halves,
+    )
     (out,) = call(
         output_kernel, [jax.ShapeDtypeStruct((rows, width), BF)],
-        received, point_weight, *pieces, held=(1,), room=20, groups=halves,
-        scratch=[((halves * out_rows, width), BF)],
+        received, point_weight, gain, w_out, whole=(3,), room=12, groups=halves,
+        scratch=[((halves * out_rows, width), BF), pltpu.SemaphoreType.DMA((count,))],
     )
     return out.reshape(1, rows, width)
 

time: 152 us -> 140 us (0.921)
  waiting for transfers between devices: 77.1 us -> 63.5 us
  Pallas kernels: 29.4 us -> 33.9 us
  starting transfers between devices: 45.1 us -> 41.5 us
    ppermute x4, waiting for transfers between devices: 15.8 us -> 6.95 us  [across(): lax.ppermute(value, ('sp', 'tp'), [(2 * i + s, 2 * i + 1 - s) for i in ta...]
    all_to_all x1, waiting for transfers between devices: 11.8 us -> 5.43 us  [head_body(): lax.all_to_all(mixed.reshape(count * halves, rows, 2 * LANES), ('sp', 'tp...]
    all_to_all x1, starting transfers between devices: 9.03 us -> 3.58 us  [head_body(): lax.all_to_all(mixed.reshape(count * halves, rows, 2 * LANES), ('sp', 'tp...]
    ppermute x15, waiting for transfers between devices: 17.9 us -> 22.5 us  [flipped(): return lax.ppermute(value, axis, [(i, i ^ bit) for i in range(count)])]
    pallas_call x11 -> x12, Pallas kernels: 29.4 us -> 33.9 us  [call(): pl.pallas_call(functools.partial(kernel, **settings) if settings else ker...]
    ppermute x8, waiting for transfers between devices: 31.6 us -> 28.6 us  [along_line(): lax.ppermute(moved[FORWARD[i]] if i in FORWARD else value, 'sp', pairs)]
    ppermute x8, starting transfers between devices: 14.8 us -> 16.9 us  [along_line(): lax.ppermute(moved[FORWARD[i]] if i in FORWARD else value, 'sp', pairs)]
  transfers between devices with their start and end apart: 28 -> 28, of which waited for: 11 -> 13; matrix products, arithmetic and copies ran while one was open for 0% -> 0% of each run, Pallas kernels for 14% -> 20%
where the time goes in v4:
time: 140 us; the launch traced here: 139 us
  waiting for transfers between devices  63.5 us (45%)
  starting transfers between devices  41.5 us (30%)
  Pallas kernels  33.9 us (24%)
    pallas_call x12, Pallas kernels, call(): pl.pallas_call(functools.partial(kernel, **settings) if settings else ker...  33.9 us
    ppermute x8, waiting for transfers between devices, along_line(): lax.ppermute(moved[FORWARD[i]] if i in FORWARD else value, 'sp', pairs)  28.6 us
    ppermute x15, waiting for transfers between devices, flipped(): return lax.ppermute(value, axis, [(i, i ^ bit) for i in range(count)])  22.5 us
    ppermute x8, starting transfers between devices, along_line(): lax.ppermute(moved[FORWARD[i]] if i in FORWARD else value, 'sp', pairs)  16.9 us
    ppermute x15, starting transfers between devices, flipped(): return lax.ppermute(value, axis, [(i, i ^ bit) for i in range(count)])  15.8 us
    ppermute x4, waiting for transfers between devices, across(): lax.ppermute(value, ('sp', 'tp'), [(2 * i + s, 2 * i + 1 - s) for i in ta...  6.95 us
    all_to_all x1, waiting for transfers between devices, head_body(): lax.all_to_all(mixed.reshape(count * halves, rows, 2 * LANES), ('sp', 'tp...  5.43 us
    ppermute x4, starting transfers between devices, across(): lax.ppermute(value, ('sp', 'tp'), [(2 * i + s, 2 * i + 1 - s) for i in ta...  5.26 us
  transfers between devices with their start and end apart: 28, of which 13 were waited for; matrix products, arithmetic and copies ran while one was open for 0% of the time, Pallas kernels for 20%

profile of v4, /device:TPU:0, one launch (start us, length us, event | category | flops | bytes accessed | tf_op | source)
XLA Modules:
  0.0 139.4 jit_solution(2166956312913639163)
XLA Ops:
  0.0 2.0 %shard_map.191 = (bf16[128,896]{1,0:T(8,128)(2,1)S(1)}, bf16[128,896]{1,0:T(8,128)(2,1)S(1)}, bf16[128,896]{1,0:T(8,128)(2,1)S(1)}, bf16[128,896]{1,0:T(8,128)(2,1)S(1)}) custom-call(f32[1,192]{1,0:T(1,128)} %refs_0_.1, bf16[128,256]{1,0:T(8,128)(2,1)} %refs_1_.1, bf16[128,256]{1,0:T(8,128)(2,1)} %refs_2_.1, bf16[128,256]{1,0:T(8,128)(2,1)} %refs_3_.1, ...), custom_call_target="tpu_custom_call" | custom-call | tf_op jit(solution)/shard_map/pallas_call | solution.py:107
  2.0 3.1 %collective-permute-start = (bf16[128,896]{1,0:T(8,128)(2,1)S(1)}, bf16[128,896]{1,0:T(8,128)(2,1)S(1)}, u32[]{:S(2)}, u32[]{:S(2)}) collective-permute-start(bf16[128,896]{1,0:T(8,128)(2,1)S(1)} %get-tuple-element.50), channel_id=1, source_target_pairs={{0,8},{8,0},{16,24},{24,16},{1,9},{9,1},{17,25},{25,17},{2,10},{10... | collective-permute-start | bytes 688136 | tf_op jit(solution)/shard_map/ppermute | solution.py:452
  5.1 2.6 %collective-permute-start.1 = (bf16[128,896]{1,0:T(8,128)(2,1)S(1)}, bf16[128,896]{1,0:T(8,128)(2,1)S(1)}, u32[]{:S(2)}, u32[]{:S(2)}) collective-permute-start(bf16[128,896]{1,0:T(8,128)(2,1)S(1)} %get-tuple-element.51), channel_id=1, source_target_pairs={{0,16},{8,24},{16,0},{24,8},{1,17},{9,25},{17,1},{25,9},{2,18},{10... | collective-permute-start | bytes 688136 | tf_op jit(solution)/shard_map/ppermute | solution.py:452
  7.7 0.0 collective-permute-start.2
  7.7 1.7 %collective-permute-start.3 = (bf16[128,896]{1,0:T(8,128)(2,1)S(1)}, bf16[128,896]{1,0:T(8,128)(2,1)S(1)}, u32[]{:S(2)}, u32[]{:S(2)}) collective-permute-start(bf16[128,896]{1,0:T(8,128)(2,1)S(1)} %get-tuple-element.49.refs_0_), channel_id=1, source_target_pairs={{0,4},{2,6},{4,0},{6,2},{1,5},{3,7},{5,1},{7,3},{8,12},{10,14},{12... | collective-permute-start | bytes 688136 | tf_op jit(solution)/shard_map/ppermute | solution.py:452
  9.4 5.4 %collective-permute-done.refs_1_ = bf16[128,896]{1,0:T(8,128)(2,1)S(1)} collective-permute-done((bf16[128,896]{1,0:T(8,128)(2,1)S(1)}, bf16[128,896]{1,0:T(8,128)(2,1)S(1)}, u32[]{:S(2)}, u32[]{:S(2)}) %collective-permute-start) | collective-permute-done | bytes 229408 | tf_op jit(solution)/shard_map/ppermute | solution.py:452
  14.9 1.7 %collective-permute-start.4 = (bf16[128,896]{1,0:T(8,128)(2,1)S(1)}, bf16[128,896]{1,0:T(8,128)(2,1)S(1)}, u32[]{:S(2)}, u32[]{:S(2)}) collective-permute-start(bf16[128,896]{1,0:T(8,128)(2,1)S(1)} %collective-permute-done.refs_1_), channel_id=1, source_target_pairs={{0,4},{2,6},{4,0},{6,2},{1,5},{3,7},{5,1},{7,3},{8,12},{10,14},{12... | collective-permute-start | bytes 688136 | tf_op jit(solution)/shard_map/ppermute | solution.py:452
  16.6 7.7 %collective-permute-done.1.refs_2_ = bf16[128,896]{1,0:T(8,128)(2,1)S(1)} collective-permute-done((bf16[128,896]{1,0:T(8,128)(2,1)S(1)}, bf16[128,896]{1,0:T(8,128)(2,1)S(1)}, u32[]{:S(2)}, u32[]{:S(2)}) %collective-permute-start.1) | collective-permute-done | bytes 229408 | tf_op jit(solution)/shard_map/ppermute | solution.py:452
  24.3 1.5 %collective-permute-start.5 = (bf16[128,896]{1,0:T(8,128)(2,1)S(1)}, bf16[128,896]{1,0:T(8,128)(2,1)S(1)}, u32[]{:S(2)}, u32[]{:S(2)}) collective-permute-start(bf16[128,896]{1,0:T(8,128)(2,1)S(1)} %collective-permute-done.1.refs_2_), channel_id=1, source_target_pairs={{0,4},{2,6},{4,0},{6,2},{1,5},{3,7},{5,1},{7,3},{8,12},{10,14},{12... | collective-permute-start | bytes 688136 | tf_op jit(solution)/shard_map/ppermute | solution.py:452
  25.8 0.0 collective-permute-done.2.refs_3_
  25.8 0.5 collective-permute-start.6
  26.3 2.5 %shard_map.190 = (bf16[192,2048]{1,0:T(8,128)(2,1)}, bf16[96,2048]{1,0:T(8,128)(2,1)S(1)}, bf16[784,128]{1,0:T(8,128)(2,1)S(1)}) custom-call(bf16[192,2048]{1,0:T(8,128)(2,1)} %bitcast.9, f32[1,2048]{1,0:T(1,128)} %bitcast.11, bf16[256,128]{1,0:T(8,128)(2,1)} %out_conv.1, bf16[512,128]{1,0:T(8,128)(2,1)} %out_state.1, f32[1,256]{1,0:T(1,128)} %bitcast.15), custom_call_target="tpu_custom_call" | custom-call | tf_op jit(solution)/shard_map/pallas_call | solution.py:107
  28.8 4.6 %collective-permute-start.17 = (bf16[784,128]{1,0:T(8,128)(2,1)S(1)}, bf16[784,128]{1,0:T(8,128)(2,1)S(1)}, u32[]{:S(2)}, u32[]{:S(2)}) collective-permute-start(bf16[784,128]{1,0:T(8,128)(2,1)S(1)} %get-tuple-element.88.own), channel_id=1, source_target_pairs={{0,16},{8,24},{16,0},{24,8},{1,17},{9,25},{17,1},{25,9},{2,18},{10... | collective-permute-start | bytes 602120 | tf_op jit(solution)/shard_map/ppermute | solution.py:439
  33.4 0.0 collective-permute-done.3.refs_4_
  33.4 0.0 collective-permute-done.4.refs_5_
  33.4 0.0 collective-permute-done.5.refs_6_
  33.4 0.0 collective-permute-done.6.refs_7_
  33.4 0.1 shard_map.192.mine
  33.6 0.1 collective-permute-start.7
  33.7 1.5 %collective-permute-start.16 = (bf16[784,128]{1,0:T(8,128)(2,1)S(1)}, bf16[784,128]{1,0:T(8,128)(2,1)S(1)}, u32[]{:S(2)}, u32[]{:S(2)}) collective-permute-start(bf16[784,128]{1,0:T(8,128)(2,1)S(1)} %get-tuple-element.88.own), channel_id=1, source_target_pairs={{0,8},{8,0},{16,24},{24,16},{1,9},{9,1},{17,25},{25,17},{2,10},{10... | collective-permute-start | bytes 602120 | tf_op jit(solution)/shard_map/ppermute | solution.py:439
  35.2 0.7 collective-permute-start.18
  35.9 6.7 %collective-permute-done.17.refs_1_ = bf16[784,128]{1,0:T(8,128)(2,1)S(1)} collective-permute-done((bf16[784,128]{1,0:T(8,128)(2,1)S(1)}, bf16[784,128]{1,0:T(8,128)(2,1)S(1)}, u32[]{:S(2)}, u32[]{:S(2)}) %collective-permute-start.17) | collective-permute-done | bytes 200736 | tf_op jit(solution)/shard_map/ppermute | solution.py:439
  42.5 1.3 collective-permute-start.19
  43.8 0.1 collective-permute-done.16.refs_0_
  43.9 0.0 collective-permute-done.18.refs_2_
  43.9 6.2 %collective-permute-done.19.refs_3_ = bf16[784,128]{1,0:T(8,128)(2,1)S(1)} collective-permute-done((bf16[784,128]{1,0:T(8,128)(2,1)S(1)}, bf16[784,128]{1,0:T(8,128)(2,1)S(1)}, u32[]{:S(2)}, u32[]{:S(2)}) %collective-permute-start.19) | collective-permute-done | bytes 200736 | tf_op jit(solution)/shard_map/ppermute | solution.py:439
  50.1 0.1 shard_map.199.refs_0_
  50.2 2.0 %collective-permute-start.23 = (bf16[4,784,128]{2,1,0:T(8,128)(2,1)S(1)}, bf16[4,784,128]{2,1,0:T(8,128)(2,1)S(1)}, u32[]{:S(2)}, u32[]{:S(2)}) collective-permute-start(bf16[4,784,128]{2,1,0:T(8,128)(2,1)S(1)} %shard_map.199.refs_0_), channel_id=1, source_target_pairs={{0,1},{1,0},{2,3},{3,2},{4,5},{5,4},{6,7},{7,6},{8,9},{9,8},{10,11... | collective-permute-start | bytes 2408456 | tf_op jit(solution)/shard_map/ppermute | solution.py:452
  52.2 0.0 collective-permute-start.8
  52.2 6.9 %collective-permute-start.10 = (bf16[96,2048]{1,0:T(8,128)(2,1)S(1)}, bf16[96,2048]{1,0:T(8,128)(2,1)S(1)}, u32[]{:S(2)}, u32[]{:S(2)}) collective-permute-start(bf16[96,2048]{1,0:T(8,128)(2,1)S(1)} %get-tuple-element.62), channel_id=1, source_target_pairs={{0,16},{8,24},{16,0},{24,8},{1,17},{9,25},{17,1},{25,9},{2,18},{10... | collective-permute-start | bytes 1179656 | tf_op jit(solution)/shard_map/ppermute | solution.py:439
  59.0 0.7 collective-permute-start.12
  59.7 5.5 %collective-permute-done.8.refs_0_ = bf16[96,2048]{1,0:T(8,128)(2,1)S(1)} collective-permute-done((bf16[96,2048]{1,0:T(8,128)(2,1)S(1)}, bf16[96,2048]{1,0:T(8,128)(2,1)S(1)}, u32[]{:S(2)}, u32[]{:S(2)}) %collective-permute-start.8) | collective-permute-done | bytes 393248 | tf_op jit(solution)/shard_map/ppermute | solution.py:439
  65.2 0.9 collective-permute-start.9
  66.1 6.6 %collective-permute-done.10.refs_0_ = bf16[96,2048]{1,0:T(8,128)(2,1)S(1)} collective-permute-done((bf16[96,2048]{1,0:T(8,128)(2,1)S(1)}, bf16[96,2048]{1,0:T(8,128)(2,1)S(1)}, u32[]{:S(2)}, u32[]{:S(2)}) %collective-permute-start.10) | collective-permute-done | bytes 393248 | tf_op jit(solution)/shard_map/ppermute | solution.py:439
  72.8 0.0 collective-permute-start.21
  72.8 0.0 collective-permute-done.23.refs_4_
  72.8 2.0 %collective-permute-start.25 = (bf16[4,784,128]{2,1,0:T(8,128)(2,1)S(1)}, bf16[4,784,128]{2,1,0:T(8,128)(2,1)}, u32[]{:S(2)}, u32[]{:S(2)}) collective-permute-start(bf16[4,784,128]{2,1,0:T(8,128)(2,1)S(1)} %collective-permute-done.23.refs_4_), channel_id=1, source_target_pairs={{0,4},{2,6},{4,0},{6,2},{1,5},{3,7},{5,1},{7,3},{8,12},{10,14},{12... | collective-permute-start | bytes 2408456 | tf_op jit(solution)/shard_map/ppermute | solution.py:452
  74.8 0.0 collective-permute-done.12.refs_0_
  74.8 0.5 collective-permute-start.11
  75.3 2.7 %collective-permute-done.9.refs_1_ = bf16[96,2048]{1,0:T(8,128)(2,1)S(1)} collective-permute-done((bf16[96,2048]{1,0:T(8,128)(2,1)S(1)}, bf16[96,2048]{1,0:T(8,128)(2,1)S(1)}, u32[]{:S(2)}, u32[]{:S(2)}) %collective-permute-start.9) | collective-permute-done | bytes 393248 | tf_op jit(solution)/shard_map/ppermute | solution.py:445
  78.0 1.3 collective-permute-start.14
  79.3 4.2 %collective-permute-done.11.refs_1_ = bf16[96,2048]{1,0:T(8,128)(2,1)S(1)} collective-permute-done((bf16[96,2048]{1,0:T(8,128)(2,1)S(1)}, bf16[96,2048]{1,0:T(8,128)(2,1)S(1)}, u32[]{:S(2)}, u32[]{:S(2)}) %collective-permute-start.11) | collective-permute-done | bytes 393248 | tf_op jit(solution)/shard_map/ppermute | solution.py:445
  83.6 0.7 collective-permute-start.13
  84.2 3.5 %collective-permute-done.14.refs_2_ = bf16[96,2048]{1,0:T(8,128)(2,1)S(1)} collective-permute-done((bf16[96,2048]{1,0:T(8,128)(2,1)S(1)}, bf16[96,2048]{1,0:T(8,128)(2,1)S(1)}, u32[]{:S(2)}, u32[]{:S(2)}) %collective-permute-start.14) | collective-permute-done | bytes 393248 | tf_op jit(solution)/shard_map/ppermute | solution.py:439
  87.7 3.2 %collective-permute-start.15 = (bf16[96,2048]{1,0:T(8,128)(2,1)S(1)}, bf16[96,2048]{1,0:T(8,128)(2,1)S(1)}, u32[]{:S(2)}, u32[]{:S(2)}) collective-permute-start(bf16[96,2048]{1,0:T(8,128)(2,1)S(1)} %collective-permute-done.14.refs_2_), channel_id=1, source_target_pairs={{0,1},{1,0},{24,25},{25,24},{2,3},{3,2},{26,27},{27,26},{4,5},{5,4... | collective-permute-start | bytes 1179656 | tf_op jit(solution)/shard_map/ppermute | solution.py:445
  90.9 0.0 collective-permute-done.13.refs_1_
  90.9 0.1 collective-permute-start.20
  91.0 0.6 collective-permute-done.21.refs_2_
  91.6 0.0 collective-permute-start.24
  91.6 8.7 %collective-permute-done.25.refs_6_ = bf16[4,784,128]{2,1,0:T(8,128)(2,1)} collective-permute-done((bf16[4,784,128]{2,1,0:T(8,128)(2,1)S(1)}, bf16[4,784,128]{2,1,0:T(8,128)(2,1)}, u32[]{:S(2)}, u32[]{:S(2)}) %collective-permute-start.25) | collective-permute-done | bytes 802848 | tf_op jit(solution)/shard_map/ppermute | solution.py:452
  100.3 0.0 collective-permute-start.22
  100.3 0.5 collective-permute-start.26
  100.8 1.1 shard_map.193
  101.8 4.6 %shard_map.194 = (bf16[2048,896]{1,0:T(8,128)(2,1)S(1)}, bf16[192,256]{1,0:T(8,128)(2,1)S(1)}, bf16[192,128]{1,0:T(8,128)(2,1)S(1)}, f32[3,64,128]{2,1,0:T(8,128...) custom-call(bf16[192,2048]{1,0:T(8,128)(2,1)} %get-tuple-element.48., ...), custom_call_target="tpu_custom_call" | custom-call | tf_op jit(solution)/shard_map/pallas_call | solution.py:107
  106.4 3.2 %shard_map.195 = (bf16[192,256]{1,0:T(8,128)(2,1)S(1)}, bf16[192,128]{1,0:T(8,128)(2,1)S(1)}, f32[3,64,128]{2,1,0:T(8,128)S(1)}, bf16[3,128,128]{2,1,0:T(8,128)(...) custom-call(bf16[96,2048]{1,0:T(8,128)(2,1)S(1)} %collective-permute-done.8.refs_0_, ...), custom_call_target="tpu_custom_call" | custom-call | tf_op jit(solution)/shard_map/pallas_call | solution.py:107
  109.6 3.2 %shard_map.196 = (bf16[192,256]{1,0:T(8,128)(2,1)S(1)}, bf16[192,128]{1,0:T(8,128)(2,1)S(1)}, f32[3,64,128]{2,1,0:T(8,128)S(1)}, bf16[3,128,128]{2,1,0:T(8,128)(...) custom-call(bf16[96,2048]{1,0:T(8,128)(2,1)S(1)} %collective-permute-done.10.refs_0, ...), custom_call_target="tpu_custom_call" | custom-call | tf_op jit(solution)/shard_map/pallas_call | solution.py:107
  112.8 3.4 %shard_map.197 = (bf16[192,256]{1,0:T(8,128)(2,1)S(1)}, bf16[192,128]{1,0:T(8,128)(2,1)S(1)}, f32[3,64,128]{2,1,0:T(8,128)S(1)}, bf16[3,128,128]{2,1,0:T(8,128)(...) custom-call(bf16[96,2048]{1,0:T(8,128)(2,1)S(1)} %collective-permute-done.12.refs_0, ...), custom_call_target="tpu_custom_call" | custom-call | tf_op jit(solution)/shard_map/pallas_call | solution.py:107
  116.2 3.2 %shard_map.198 = bf16[768,256]{1,0:T(8,128)(2,1)} custom-call(bf16[192,256]{1,0:T(8,128)(2,1)S(1)} %get-tuple-element.55.refs_0_, bf16[192,128]{1,0:T(8,128)(2,1)S(1)} %get-tuple-element.56.refs_1_, f32[3,64,128]{2,1,0:T(8,128)S(1)} %get-tuple-element.57.refs_2_, bf16[3,128,128]{2,1,0:T(8,128)(2,1)S(1)} %get-tuple-element.58.refs_3_, ...), custom_call_target="tpu_custom_call" | custom-call | tf_op jit(solution)/shard_map/pallas_call | solution.py:107
  119.4 3.6 %all-to-all-start = ((bf16[8,96,256]{2,1,0:T(8,128)(2,1)}), bf16[8,96,256]{2,1,0:T(8,128)(2,1)S(1)}, u32[]{:S(2)}, u32[]{:S(2)}) async-start(bf16[8,96,256]{2,1,0:T(8,128)(2,1)} %bitcast.7), calls=%async_computation | async-start | bytes 786432 | tf_op jit(solution)/shard_map/all_to_all | solution.py:529
  123.0 0.0 collective-permute-done.22.refs_3_
  123.0 0.0 collective-permute-done.24.refs_5_
  123.1 6.6 %shard_map.200 = (bf16[1536,2048]{1,0:T(8,128)(2,1)}, f32[1,512]{1,0:T(1,128)S(1)}) custom-call(bf16[4,784,128]{2,1,0:T(8,128)(2,1)S(1)} %shard_map.199.refs_0_, bf16[4,784,128]{2,1,0:T(8,128)(2,1)} %collective-permute-done.20.refs_1_, bf16[4,784,128]{2,1,0:T(8,128)(2,1)S(1)} %collective-permute-done.21.refs_2_, ...), custom_call_target="tpu_custom_call" | custom-call | tf_op jit(solution)/shard_map/pallas_call | solution.py:107
  129.6 5.4 %all-to-all-done.received = bf16[8,96,256]{2,1,0:T(8,128)(2,1)S(1)} async-done(((bf16[8,96,256]{2,1,0:T(8,128)(2,1)}), bf16[8,96,256]{2,1,0:T(8,128)(2,1)S(1)}, u32[]{:S(2)}, u32[]{:S(2)}) %all-to-all-start) | async-done | bytes 393248 | tf_op jit(solution)/shard_map/all_to_all | solution.py:529
  135.1 4.1 %shard_map.201 = bf16[96,2048]{1,0:T(8,128)(2,1)} custom-call(bf16[8,96,256]{2,1,0:T(8,128)(2,1)S(1)} %all-to-all-done.received, bf16[512,512]{1,0:T(8,128)(2,1)S(1)} %copy-done, f32[1,512]{1,0:T(1,128)S(1)} %get-tuple-element.89.gain, bf16[1536,2048]{1,0:T(8,128)(2,1)} %get-tuple-element.90.rows_in), custom_call_target="tpu_custom_call" | custom-call | tf_op jit(solution)/shard_map/pallas_call | solution.py:107
  (6 shorter events, 0.0 us)
Async XLA Ops:
  2.0 12.9 %collective-permute-start = (bf16[128,896]{1,0:T(8,128)(2,1)S(1)}, bf16[128,896]{1,0:T(8,128)(2,1)S(1)}, u32[]{:S(2)}, u32[]{:S(2)}) collective-permute-start(bf16[128,896]{1,0:T(8,128)(2,1)S(1)} %get-tuple-element.50), channel_id=1, source_target_pairs={{0,8},{8,0},{16,24},{24,16},{1,9},{9,1},{17,25},{25,17},{2,10},{10... | collective-permute-start | bytes 688136 | tf_op jit(solution)/shard_map/ppermute | solution.py:452
  5.1 19.2 %collective-permute-start.1 = (bf16[128,896]{1,0:T(8,128)(2,1)S(1)}, bf16[128,896]{1,0:T(8,128)(2,1)S(1)}, u32[]{:S(2)}, u32[]{:S(2)}) collective-permute-start(bf16[128,896]{1,0:T(8,128)(2,1)S(1)} %get-tuple-element.51), channel_id=1, source_target_pairs={{0,16},{8,24},{16,0},{24,8},{1,17},{9,25},{17,1},{25,9},{2,18},{10... | collective-permute-start | bytes 688136 | tf_op jit(solution)/shard_map/ppermute | solution.py:452
  7.7 18.1 %collective-permute-start.2 = (bf16[128,896]{1,0:T(8,128)(2,1)S(1)}, bf16[128,896]{1,0:T(8,128)(2,1)S(1)}, u32[]{:S(2)}, u32[]{:S(2)}) collective-permute-start(bf16[128,896]{1,0:T(8,128)(2,1)S(1)} %get-tuple-element.52), channel_id=1, source_target_pairs={{0,24},{8,16},{16,8},{24,0},{1,25},{9,17},{17,9},{25,1},{2,26},{10... | collective-permute-start | bytes 688136 | tf_op jit(solution)/shard_map/ppermute | solution.py:452
  7.7 25.7 %collective-permute-start.3 = (bf16[128,896]{1,0:T(8,128)(2,1)S(1)}, bf16[128,896]{1,0:T(8,128)(2,1)S(1)}, u32[]{:S(2)}, u32[]{:S(2)}) collective-permute-start(bf16[128,896]{1,0:T(8,128)(2,1)S(1)} %get-tuple-element.49.refs_0_), channel_id=1, source_target_pairs={{0,4},{2,6},{4,0},{6,2},{1,5},{3,7},{5,1},{7,3},{8,12},{10,14},{12... | collective-permute-start | bytes 688136 | tf_op jit(solution)/shard_map/ppermute | solution.py:452
  14.9 18.5 %collective-permute-start.4 = (bf16[128,896]{1,0:T(8,128)(2,1)S(1)}, bf16[128,896]{1,0:T(8,128)(2,1)S(1)}, u32[]{:S(2)}, u32[]{:S(2)}) collective-permute-start(bf16[128,896]{1,0:T(8,128)(2,1)S(1)} %collective-permute-done.refs_1_), channel_id=1, source_target_pairs={{0,4},{2,6},{4,0},{6,2},{1,5},{3,7},{5,1},{7,3},{8,12},{10,14},{12... | collective-permute-start | bytes 688136 | tf_op jit(solution)/shard_map/ppermute | solution.py:452
  24.3 9.1 %collective-permute-start.5 = (bf16[128,896]{1,0:T(8,128)(2,1)S(1)}, bf16[128,896]{1,0:T(8,128)(2,1)S(1)}, u32[]{:S(2)}, u32[]{:S(2)}) collective-permute-start(bf16[128,896]{1,0:T(8,128)(2,1)S(1)} %collective-permute-done.1.refs_2_), channel_id=1, source_target_pairs={{0,4},{2,6},{4,0},{6,2},{1,5},{3,7},{5,1},{7,3},{8,12},{10,14},{12... | collective-permute-start | bytes 688136 | tf_op jit(solution)/shard_map/ppermute | solution.py:452
  25.8 7.6 %collective-permute-start.6 = (bf16[128,896]{1,0:T(8,128)(2,1)S(1)}, bf16[128,896]{1,0:T(8,128)(2,1)S(1)}, u32[]{:S(2)}, u32[]{:S(2)}) collective-permute-start(bf16[128,896]{1,0:T(8,128)(2,1)S(1)} %collective-permute-done.2.refs_3_), channel_id=1, source_target_pairs={{0,4},{2,6},{4,0},{6,2},{1,5},{3,7},{5,1},{7,3},{8,12},{10,14},{12... | collective-permute-start | bytes 688136 | tf_op jit(solution)/shard_map/ppermute | solution.py:452
  28.8 13.7 %collective-permute-start.17 = (bf16[784,128]{1,0:T(8,128)(2,1)S(1)}, bf16[784,128]{1,0:T(8,128)(2,1)S(1)}, u32[]{:S(2)}, u32[]{:S(2)}) collective-permute-start(bf16[784,128]{1,0:T(8,128)(2,1)S(1)} %get-tuple-element.88.own), channel_id=1, source_target_pairs={{0,16},{8,24},{16,0},{24,8},{1,17},{9,25},{17,1},{25,9},{2,18},{10... | collective-permute-start | bytes 602120 | tf_op jit(solution)/shard_map/ppermute | solution.py:439
  33.6 66.7 %collective-permute-start.7 = (bf16[1024,896]{1,0:T(8,128)(2,1)S(1)}, bf16[1024,896]{1,0:T(8,128)(2,1)S(1)}, u32[]{:S(2)}, u32[]{:S(2)}) collective-permute-start(bf16[1024,896]{1,0:T(8,128)(2,1)S(1)} %shard_map.192.mine), channel_id=1, source_target_pairs={{0,2},{2,0},{4,6},{6,4},{1,3},{3,1},{5,7},{7,5},{8,10},{10,8},{12,... | collective-permute-start | bytes 5505032 | tf_op jit(solution)/shard_map/ppermute | solution.py:452
  33.7 10.3 %collective-permute-start.16 = (bf16[784,128]{1,0:T(8,128)(2,1)S(1)}, bf16[784,128]{1,0:T(8,128)(2,1)S(1)}, u32[]{:S(2)}, u32[]{:S(2)}) collective-permute-start(bf16[784,128]{1,0:T(8,128)(2,1)S(1)} %get-tuple-element.88.own), channel_id=1, source_target_pairs={{0,8},{8,0},{16,24},{24,16},{1,9},{9,1},{17,25},{25,17},{2,10},{10... | collective-permute-start | bytes 602120 | tf_op jit(solution)/shard_map/ppermute | solution.py:439
  35.2 8.7 %collective-permute-start.18 = (bf16[784,128]{1,0:T(8,128)(2,1)S(1)}, bf16[784,128]{1,0:T(8,128)(2,1)S(1)}, u32[]{:S(2)}, u32[]{:S(2)}) collective-permute-start(bf16[784,128]{1,0:T(8,128)(2,1)S(1)} %get-tuple-element.88.own), channel_id=1, source_target_pairs={{8,16},{16,8},{9,17},{17,9},{10,18},{18,10},{11,19},{19,11},{12,20... | collective-permute-start | bytes 602120 | tf_op jit(solution)/shard_map/ppermute | solution.py:439
  42.5 7.6 %collective-permute-start.19 = (bf16[784,128]{1,0:T(8,128)(2,1)S(1)}, bf16[784,128]{1,0:T(8,128)(2,1)S(1)}, u32[]{:S(2)}, u32[]{:S(2)}) collective-permute-start(bf16[784,128]{1,0:T(8,128)(2,1)S(1)} %collective-permute-done.17.refs_1_), channel_id=1, source_target_pairs={{16,24},{8,0},{17,25},{9,1},{18,26},{10,2},{19,27},{11,3},{20,28},... | collective-permute-start | bytes 602120 | tf_op jit(solution)/shard_map/ppermute | solution.py:439
  50.2 22.6 %collective-permute-start.23 = (bf16[4,784,128]{2,1,0:T(8,128)(2,1)S(1)}, bf16[4,784,128]{2,1,0:T(8,128)(2,1)S(1)}, u32[]{:S(2)}, u32[]{:S(2)}) collective-permute-start(bf16[4,784,128]{2,1,0:T(8,128)(2,1)S(1)} %shard_map.199.refs_0_), channel_id=1, source_target_pairs={{0,1},{1,0},{2,3},{3,2},{4,5},{5,4},{6,7},{7,6},{8,9},{9,8},{10,11... | collective-permute-start | bytes 2408456 | tf_op jit(solution)/shard_map/ppermute | solution.py:452
  52.2 13.1 %collective-permute-start.8 = (bf16[96,2048]{1,0:T(8,128)(2,1)S(1)}, bf16[96,2048]{1,0:T(8,128)(2,1)S(1)}, u32[]{:S(2)}, u32[]{:S(2)}) collective-permute-start(bf16[96,2048]{1,0:T(8,128)(2,1)S(1)} %get-tuple-element.62), channel_id=1, source_target_pairs={{0,8},{8,0},{16,24},{24,16},{1,9},{9,1},{17,25},{25,17},{2,10},{10... | collective-permute-start | bytes 1179656 | tf_op jit(solution)/shard_map/ppermute | solution.py:439
  52.2 20.6 %collective-permute-start.10 = (bf16[96,2048]{1,0:T(8,128)(2,1)S(1)}, bf16[96,2048]{1,0:T(8,128)(2,1)S(1)}, u32[]{:S(2)}, u32[]{:S(2)}) collective-permute-start(bf16[96,2048]{1,0:T(8,128)(2,1)S(1)} %get-tuple-element.62), channel_id=1, source_target_pairs={{0,16},{8,24},{16,0},{24,8},{1,17},{9,25},{17,1},{25,9},{2,18},{10... | collective-permute-start | bytes 1179656 | tf_op jit(solution)/shard_map/ppermute | solution.py:439
  59.0 15.8 %collective-permute-start.12 = (bf16[96,2048]{1,0:T(8,128)(2,1)S(1)}, bf16[96,2048]{1,0:T(8,128)(2,1)S(1)}, u32[]{:S(2)}, u32[]{:S(2)}) collective-permute-start(bf16[96,2048]{1,0:T(8,128)(2,1)S(1)} %get-tuple-element.62), channel_id=1, source_target_pairs={{8,16},{16,8},{9,17},{17,9},{10,18},{18,10},{11,19},{19,11},{12,20... | collective-permute-start | bytes 1179656 | tf_op jit(solution)/shard_map/ppermute | solution.py:439
  65.2 12.8 %collective-permute-start.9 = (bf16[96,2048]{1,0:T(8,128)(2,1)S(1)}, bf16[96,2048]{1,0:T(8,128)(2,1)S(1)}, u32[]{:S(2)}, u32[]{:S(2)}) collective-permute-start(bf16[96,2048]{1,0:T(8,128)(2,1)S(1)} %collective-permute-done.8.refs_0_), channel_id=1, source_target_pairs={{0,1},{1,0},{8,9},{9,8},{16,17},{17,16},{24,25},{25,24},{2,3},{3,2... | collective-permute-start | bytes 1179656 | tf_op jit(solution)/shard_map/ppermute | solution.py:445
  72.8 18.8 %collective-permute-start.21 = (bf16[4,784,128]{2,1,0:T(8,128)(2,1)S(1)}, bf16[4,784,128]{2,1,0:T(8,128)(2,1)S(1)}, u32[]{:S(2)}, u32[]{:S(2)}) collective-permute-start(bf16[4,784,128]{2,1,0:T(8,128)(2,1)S(1)} %shard_map.199.refs_0_), channel_id=1, source_target_pairs={{0,4},{2,6},{4,0},{6,2},{1,5},{3,7},{5,1},{7,3},{8,12},{10,14},{12... | collective-permute-start | bytes 2408456 | tf_op jit(solution)/shard_map/ppermute | solution.py:452
  72.8 27.5 %collective-permute-start.25 = (bf16[4,784,128]{2,1,0:T(8,128)(2,1)S(1)}, bf16[4,784,128]{2,1,0:T(8,128)(2,1)}, u32[]{:S(2)}, u32[]{:S(2)}) collective-permute-start(bf16[4,784,128]{2,1,0:T(8,128)(2,1)S(1)} %collective-permute-done.23.refs_4_), channel_id=1, source_target_pairs={{0,4},{2,6},{4,0},{6,2},{1,5},{3,7},{5,1},{7,3},{8,12},{10,14},{12... | collective-permute-start | bytes 2408456 | tf_op jit(solution)/shard_map/ppermute | solution.py:452
  74.8 8.7 %collective-permute-start.11 = (bf16[96,2048]{1,0:T(8,128)(2,1)S(1)}, bf16[96,2048]{1,0:T(8,128)(2,1)S(1)}, u32[]{:S(2)}, u32[]{:S(2)}) collective-permute-start(bf16[96,2048]{1,0:T(8,128)(2,1)S(1)} %collective-permute-done.10.refs_0_), channel_id=1, source_target_pairs={{0,1},{1,0},{8,9},{9,8},{16,17},{17,16},{24,25},{25,24},{2,3},{3,2... | collective-permute-start | bytes 1179656 | tf_op jit(solution)/shard_map/ppermute | solution.py:445
  78.0 9.7 %collective-permute-start.14 = (bf16[96,2048]{1,0:T(8,128)(2,1)S(1)}, bf16[96,2048]{1,0:T(8,128)(2,1)S(1)}, u32[]{:S(2)}, u32[]{:S(2)}) collective-permute-start(bf16[96,2048]{1,0:T(8,128)(2,1)S(1)} %collective-permute-done.10.refs_0_), channel_id=1, source_target_pairs={{16,24},{8,0},{17,25},{9,1},{18,26},{10,2},{19,27},{11,3},{20,28},... | collective-permute-start | bytes 1179656 | tf_op jit(solution)/shard_map/ppermute | solution.py:439
  83.6 7.3 %collective-permute-start.13 = (bf16[96,2048]{1,0:T(8,128)(2,1)S(1)}, bf16[96,2048]{1,0:T(8,128)(2,1)S(1)}, u32[]{:S(2)}, u32[]{:S(2)}) collective-permute-start(bf16[96,2048]{1,0:T(8,128)(2,1)S(1)} %collective-permute-done.12.refs_0_), channel_id=1, source_target_pairs={{8,9},{9,8},{16,17},{17,16},{10,11},{11,10},{18,19},{19,18},{12,13... | collective-permute-start | bytes 1179656 | tf_op jit(solution)/shard_map/ppermute | solution.py:445
  87.7 25.1 %collective-permute-start.15 = (bf16[96,2048]{1,0:T(8,128)(2,1)S(1)}, bf16[96,2048]{1,0:T(8,128)(2,1)S(1)}, u32[]{:S(2)}, u32[]{:S(2)}) collective-permute-start(bf16[96,2048]{1,0:T(8,128)(2,1)S(1)} %collective-permute-done.14.refs_2_), channel_id=1, source_target_pairs={{0,1},{1,0},{24,25},{25,24},{2,3},{3,2},{26,27},{27,26},{4,5},{5,4... | collective-permute-start | bytes 1179656 | tf_op jit(solution)/shard_map/ppermute | solution.py:445
  90.9 32.2 %collective-permute-start.20 = (bf16[4,784,128]{2,1,0:T(8,128)(2,1)S(1)}, bf16[4,784,128]{2,1,0:T(8,128)(2,1)}, u32[]{:S(2)}, u32[]{:S(2)}) collective-permute-start(bf16[4,784,128]{2,1,0:T(8,128)(2,1)S(1)} %shard_map.199.refs_0_), channel_id=1, source_target_pairs={{0,2},{2,0},{4,6},{6,4},{1,3},{3,1},{5,7},{7,5},{8,10},{10,8},{12,... | collective-permute-start | bytes 2408456 | tf_op jit(solution)/shard_map/ppermute | solution.py:452
  91.6 31.5 %collective-permute-start.24 = (bf16[4,784,128]{2,1,0:T(8,128)(2,1)S(1)}, bf16[4,784,128]{2,1,0:T(8,128)(2,1)}, u32[]{:S(2)}, u32[]{:S(2)}) collective-permute-start(bf16[4,784,128]{2,1,0:T(8,128)(2,1)S(1)} %collective-permute-done.23.refs_4_), channel_id=1, source_target_pairs={{0,2},{2,0},{4,6},{6,4},{1,3},{3,1},{5,7},{7,5},{8,10},{10,8},{12,... | collective-permute-start | bytes 2408456 | tf_op jit(solution)/shard_map/ppermute | solution.py:452
  100.3 22.8 %collective-permute-start.22 = (bf16[4,784,128]{2,1,0:T(8,128)(2,1)S(1)}, bf16[4,784,128]{2,1,0:T(8,128)(2,1)}, u32[]{:S(2)}, u32[]{:S(2)}) collective-permute-start(bf16[4,784,128]{2,1,0:T(8,128)(2,1)S(1)} %collective-permute-done.21.refs_2_), channel_id=1, source_target_pairs={{0,2},{2,0},{4,6},{6,4},{1,3},{3,1},{5,7},{7,5},{8,10},{10,8},{12,... | collective-permute-start | bytes 2408456 | tf_op jit(solution)/shard_map/ppermute | solution.py:452
  100.3 22.8 %collective-permute-start.26 = (bf16[4,784,128]{2,1,0:T(8,128)(2,1)}, bf16[4,784,128]{2,1,0:T(8,128)(2,1)}, u32[]{:S(2)}, u32[]{:S(2)}) collective-permute-start(bf16[4,784,128]{2,1,0:T(8,128)(2,1)} %collective-permute-done.25.refs_6_), channel_id=1, source_target_pairs={{0,2},{2,0},{4,6},{6,4},{1,3},{3,1},{5,7},{7,5},{8,10},{10,8},{12,... | collective-permute-start | bytes 2408456 | tf_op jit(solution)/shard_map/ppermute | solution.py:452
  119.4 15.6 %copy-start = (bf16[512,512]{1,0:T(8,128)(2,1)S(1)}, bf16[512,512]{1,0:T(8,128)(2,1)}, u32[]{:S(2)}) copy-start(bf16[512,512]{1,0:T(8,128)(2,1)} %point.1) | copy-start | bytes 1572868
  119.4 15.6 %all-to-all-start = ((bf16[8,96,256]{2,1,0:T(8,128)(2,1)}), bf16[8,96,256]{2,1,0:T(8,128)(2,1)S(1)}, u32[]{:S(2)}, u32[]{:S(2)}) async-start(bf16[8,96,256]{2,1,0:T(8,128)(2,1)} %bitcast.7), calls=%async_computation | async-start | bytes 786432 | tf_op jit(solution)/shard_map/all_to_all | solution.py:529

commit v5 on v3

--- a/solution.py
+++ b/solution.py
@@ -72,23 +72,26 @@
         out[:, start + half :] = spare
 
 
-def norm_kernel(tokens, gain, out_conv, out_state, conv_gain, normed, part, rows_out):
+def rows_kernel(out_conv, out_state, conv_gain, rows_out):
+    split, wide = out_conv.shape[0], out_state.shape[0]
+    rows_out[:split, :] = out_conv[...]
+    rows_out[split : split + wide, :] = out_state[...]
+    gains = jnp.concatenate(
+        [conv_gain[:, i * LANES : (i + 1) * LANES] for i in range(split // LANES)], axis=0
+    )
+    spare = jnp.concatenate(
+        list(three_terms(gains)) + [jnp.zeros((SPARE - 3 * gains.shape[0], LANES), F32)],
+        axis=0,
+    )
+    rows_out[split + wide :, :] = spare.astype(BF)
+
+
+def norm_kernel(tokens, gain, normed, part):
     count = part.shape[0]
     floats = tokens[...].astype(F32)
     inverse = lax.rsqrt(jnp.mean(floats * floats, axis=1, keepdims=True) + NORM_FLOOR)
     normed[...] = (floats * inverse * gain[...]).astype(BF)
     part[...] = normed[pl.ds(pl.multiple_of(here()[2] * count, 16), count), :]
-    split, wide = out_conv.shape[0], out_state.shape[0]
-    rows_out[:split, :] = out_conv[...]
-    rows_out[split : split + wide, :] = out_state[...]
-    gains = jnp.concatenate(
-        [conv_gain[:, i * LANES : (i + 1) * LANES] for i in range(split // LANES)], axis=0
-    )
-    spare = jnp.concatenate(
-        list(three_terms(gains)) + [jnp.zeros((SPARE - 3 * gains.shape[0], LANES), F32)],
-        axis=0,
-    )
-    rows_out[split + wide :, :] = spare.astype(BF)
 
 
 def assemble_kernel(*refs):
@@ -272,7 +275,7 @@
 
 def final_kernel(*refs, count, width):
     slots = [refs[7 * i : 7 * (i + 1)] for i in range(count)]
-    start, rows_in, tap, out, conv, gates, local, lead, step, added, kept, conv_rows, y = refs[
+    start, rows_in, tap, *outs, out, conv, gates, local, lead, step, added, kept, conv_rows, y = refs[
         7 * count :
     ]
     z = here()[0]
@@ -334,12 +337,19 @@
         gate = gates[block].astype(F32)
         grouped = centered * lax.rsqrt(variance + GROUP_FLOOR) * gain_row
         out[rows, :LANES] = (grouped * (gate * sigmoid(gate))).astype(BF)
-
-
-def output_kernel(received, point, *refs, groups):
-    *pieces, out, w = refs
-    _, f, t = here()
+    size = outs[0].shape[0]
+    for at, target in enumerate(outs):
+        row = ((z * lax.axis_size("tp") + here()[2]) ^ at) * size
+        target[...] = out[pl.ds(pl.multiple_of(row, 32), size), :]
+
+
+def output_kernel(point, *refs, groups):
+    *operands, out, w, received = refs
+    parts_in, pieces = operands[: received.shape[0]], operands[received.shape[0] :]
+    z, f, t = here()
     count = pieces[0].shape[0]
+    for at, part in enumerate(parts_in):
+        received[(z * groups + t) ^ at] = part[...]
     split = count * LANES // 2
     wide = count * LANES
     gains = []
@@ -457,11 +467,13 @@
     )
     taken = [slices[0]] + [flipped(slices[k], "sp", k) for k in range(1, count)]
     out_rows = output_conv.shape[0] + output_state.shape[0]
-    normed, half, rows_out = call(
-        norm_kernel,
-        [pltpu.HBM((length, width), BF), ((part, width), BF), ((out_rows + SPARE, output_conv.shape[1]), BF)],
-        tokens.reshape(length, width), norm_gain.reshape(1, width), output_conv,
-        output_state, conv_gain.reshape(1, -1), held=range(5),
+    (rows_out,) = call(
+        rows_kernel, [((out_rows + SPARE, output_conv.shape[1]), BF)],
+        output_conv, output_state, conv_gain.reshape(1, -1), held=range(3),
+    )
+    normed, half = call(
+        norm_kernel, [pltpu.HBM((length, width), BF), ((part, width), BF)],
+        tokens.reshape(length, width), norm_gain.reshape(1, width), held=range(2),
     )
     line_out = along_line(rows_out)
     near = along_line(half)
@@ -508,18 +520,21 @@
             step=step, conditions=tuple(holds for _, holds in choices),
         )
     mixed = call(
-        final_kernel, [((total, 2 * LANES), BF)], *slots, begin, gains, tap,
+        final_kernel, [((rows, 2 * LANES), BF)] * (count * halves), *slots, begin, gains, tap,
         count=count, width=kernel,
-        scratch=[((count,) + a, b) for a, b in terms]
+        scratch=[((total, 2 * LANES), BF)]
+        + [((count,) + a, b) for a, b in terms]
         + [((total // 2 + 32, LANES), F32), ((total, LANES), F32)],
-    )[0]
-    received = lax.all_to_all(
-        mixed.reshape(count * halves, rows, 2 * LANES), ("sp", "tp"), 0, 0, tiled=True
-    )
+    )
+    received = [mixed[0]]
+    for i in range(1, count * halves):
+        received.append(
+            lax.ppermute(mixed[i], ("sp", "tp"), [(d, d ^ i) for d in range(count * halves)])
+        )
     (out,) = call(
         output_kernel, [jax.ShapeDtypeStruct((rows, width), BF)],
-        received, point_weight, *pieces, held=(1,), room=20, groups=halves,
-        scratch=[((halves * out_rows, width), BF)],
+        point_weight, *received, *pieces, room=20, groups=halves,
+        scratch=[((halves * out_rows, width), BF), ((count * halves, rows, 2 * LANES), BF)],
     )
     return out.reshape(1, rows, width)
 

time: 152 us -> 170 us (1.12)
  starting transfers between devices: 45.1 us -> 68.5 us
  waiting for transfers between devices: 77.1 us -> 73.2 us
  Pallas kernels: 29.4 us -> 27.3 us
    ppermute x8, starting transfers between devices: 14.8 us -> 32 us  [along_line(): lax.ppermute(moved[FORWARD[i]] if i in FORWARD else value, 'sp', pairs)]
    ppermute x0 -> x7, starting transfers between devices: none -> 16.6 us  [head_body(): lax.ppermute(mixed[i], ('sp', 'tp'), [(d, d ^ i) for d in range(count * h...]
    all_to_all x1 -> x0, waiting for transfers between devices: 11.8 us -> none  [head_body(): lax.all_to_all(mixed.reshape(count * halves, rows, 2 * LANES), ('sp', 'tp...]
    all_to_all x1 -> x0, starting transfers between devices: 9.03 us -> none  [head_body(): lax.all_to_all(mixed.reshape(count * halves, rows, 2 * LANES), ('sp', 'tp...]
    ppermute x0 -> x7, waiting for transfers between devices: none -> 4.15 us  [head_body(): lax.ppermute(mixed[i], ('sp', 'tp'), [(d, d ^ i) for d in range(count * h...]
    ppermute x15, waiting for transfers between devices: 17.9 us -> 21.5 us  [flipped(): return lax.ppermute(value, axis, [(i, i ^ bit) for i in range(count)])]
    ppermute x15, starting transfers between devices: 15.9 us -> 13.7 us  [flipped(): return lax.ppermute(value, axis, [(i, i ^ bit) for i in range(count)])]
    pallas_call x11 -> x12, Pallas kernels: 29.4 us -> 27.3 us  [call(): pl.pallas_call(functools.partial(kernel, **settings) if settings else ker...]
  transfers between devices with their start and end apart: 28 -> 34, of which waited for: 11 -> 14; matrix products, arithmetic and copies ran while one was open for 0% -> 0% of each run, Pallas kernels for 14% -> 13%
where the time goes in v5:
time: 170 us; the launch traced here: 169 us
  waiting for transfers between devices  73.2 us (43%)
  starting transfers between devices  68.5 us (40%)
  Pallas kernels  27.3 us (16%)
    ppermute x8, starting transfers between devices, along_line(): lax.ppermute(moved[FORWARD[i]] if i in FORWARD else value, 'sp', pairs)  32 us
    ppermute x8, waiting for transfers between devices, along_line(): lax.ppermute(moved[FORWARD[i]] if i in FORWARD else value, 'sp', pairs)  31.3 us
    pallas_call x12, Pallas kernels, call(): pl.pallas_call(functools.partial(kernel, **settings) if settings else ker...  27.3 us
    ppermute x15, waiting for transfers between devices, flipped(): return lax.ppermute(value, axis, [(i, i ^ bit) for i in range(count)])  21.5 us
    ppermute x7, starting transfers between devices, head_body(): lax.ppermute(mixed[i], ('sp', 'tp'), [(d, d ^ i) for d in range(count * h...  16.6 us
    ppermute x4, waiting for transfers between devices, across(): lax.ppermute(value, ('sp', 'tp'), [(2 * i + s, 2 * i + 1 - s) for i in ta...  16.3 us
    ppermute x15, starting transfers between devices, flipped(): return lax.ppermute(value, axis, [(i, i ^ bit) for i in range(count)])  13.7 us
    ppermute x4, starting transfers between devices, across(): lax.ppermute(value, ('sp', 'tp'), [(2 * i + s, 2 * i + 1 - s) for i in ta...  6.11 us
  transfers between devices with their start and end apart: 34, of which 14 were waited for; matrix products, arithmetic and copies ran while one was open for 0% of the time, Pallas kernels for 13%

profile of v5, /device:TPU:0, one launch (start us, length us, event | category | flops | bytes accessed | tf_op | source)
XLA Modules:
  0.0 169.2 jit_solution(13650183594615882235)
XLA Ops:
  0.0 0.9 shard_map.199.own
  0.9 4.1 %collective-permute-start.24 = (bf16[784,128]{1,0:T(8,128)(2,1)S(1)}, bf16[784,128]{1,0:T(8,128)(2,1)S(1)}, u32[]{:S(2)}, u32[]{:S(2)}) collective-permute-start(bf16[784,128]{1,0:T(8,128)(2,1)S(1)} %shard_map.199.own), channel_id=1, source_target_pairs={{0,16},{8,24},{16,0},{24,8},{1,17},{9,25},{17,1},{25,9},{2,18},{10... | collective-permute-start | bytes 602120 | tf_op jit(solution)/shard_map/ppermute | solution.py:436
  5.1 1.6 collective-permute-start.23
  6.6 2.0 %shard_map.191 = (bf16[128,896]{1,0:T(8,128)(2,1)S(1)}, bf16[128,896]{1,0:T(8,128)(2,1)S(1)}, bf16[128,896]{1,0:T(8,128)(2,1)S(1)}, bf16[128,896]{1,0:T(8,128)(2,1)S(1)}) custom-call(f32[1,192]{1,0:T(1,128)} %refs_0_.1, bf16[128,256]{1,0:T(8,128)(2,1)} %refs_1_.1, bf16[128,256]{1,0:T(8,128)(2,1)} %refs_2_.1, bf16[128,256]{1,0:T(8,128)(2,1)} %refs_3_.1, ...), custom_call_target="tpu_custom_call" | custom-call | tf_op jit(solution)/shard_map/pallas_call | solution.py:110
  8.6 0.5 collective-permute-start
  9.1 0.1 collective-permute-start.1
  9.2 3.9 %collective-permute-start.2 = (bf16[128,896]{1,0:T(8,128)(2,1)S(1)}, bf16[128,896]{1,0:T(8,128)(2,1)S(1)}, u32[]{:S(2)}, u32[]{:S(2)}) collective-permute-start(bf16[128,896]{1,0:T(8,128)(2,1)S(1)} %get-tuple-element.57), channel_id=1, source_target_pairs={{0,24},{8,16},{16,8},{24,0},{1,25},{9,17},{17,9},{25,1},{2,26},{10... | collective-permute-start | bytes 688136 | tf_op jit(solution)/shard_map/ppermute | solution.py:449
  13.1 2.2 %collective-permute-done.24.refs_1_ = bf16[784,128]{1,0:T(8,128)(2,1)S(1)} collective-permute-done((bf16[784,128]{1,0:T(8,128)(2,1)S(1)}, bf16[784,128]{1,0:T(8,128)(2,1)S(1)}, u32[]{:S(2)}, u32[]{:S(2)}) %collective-permute-start.24) | collective-permute-done | bytes 200736 | tf_op jit(solution)/shard_map/ppermute | solution.py:436
  15.3 0.7 collective-permute-start.25
  16.0 4.6 %collective-permute-done.23.refs_0_ = bf16[784,128]{1,0:T(8,128)(2,1)S(1)} collective-permute-done((bf16[784,128]{1,0:T(8,128)(2,1)S(1)}, bf16[784,128]{1,0:T(8,128)(2,1)S(1)}, u32[]{:S(2)}, u32[]{:S(2)}) %collective-permute-start.23) | collective-permute-done | bytes 200736 | tf_op jit(solution)/shard_map/ppermute | solution.py:436
  20.6 1.3 collective-permute-start.26
  21.9 1.4 collective-permute-start.3
  23.3 7.2 %collective-permute-done.refs_1_ = bf16[128,896]{1,0:T(8,128)(2,1)S(1)} collective-permute-done((bf16[128,896]{1,0:T(8,128)(2,1)S(1)}, bf16[128,896]{1,0:T(8,128)(2,1)S(1)}, u32[]{:S(2)}, u32[]{:S(2)}) %collective-permute-start) | collective-permute-done | bytes 229408 | tf_op jit(solution)/shard_map/ppermute | solution.py:449
  30.5 1.6 collective-permute-start.4
  32.1 0.0 collective-permute-done.1.refs_2_
  32.1 0.5 collective-permute-start.5
  32.6 1.6 collective-permute-start.6
  34.1 0.0 collective-permute-done.26.refs_3_
  34.1 0.1 shard_map.200.refs_8_
  34.2 1.6 collective-permute-start.30
  35.8 2.0 %collective-permute-done.4.refs_5_ = bf16[128,896]{1,0:T(8,128)(2,1)S(1)} collective-permute-done((bf16[128,896]{1,0:T(8,128)(2,1)S(1)}, bf16[128,896]{1,0:T(8,128)(2,1)S(1)}, u32[]{:S(2)}, u32[]{:S(2)}) %collective-permute-start.4) | collective-permute-done | bytes 229408 | tf_op jit(solution)/shard_map/ppermute | solution.py:449
  37.8 2.5 %collective-permute-done.5.refs_6_ = bf16[128,896]{1,0:T(8,128)(2,1)S(1)} collective-permute-done((bf16[128,896]{1,0:T(8,128)(2,1)S(1)}, bf16[128,896]{1,0:T(8,128)(2,1)S(1)}, u32[]{:S(2)}, u32[]{:S(2)}) %collective-permute-start.5) | collective-permute-done | bytes 229408 | tf_op jit(solution)/shard_map/ppermute | solution.py:449
  40.3 2.5 %collective-permute-done.6.refs_7_ = bf16[128,896]{1,0:T(8,128)(2,1)S(1)} collective-permute-done((bf16[128,896]{1,0:T(8,128)(2,1)S(1)}, bf16[128,896]{1,0:T(8,128)(2,1)S(1)}, u32[]{:S(2)}, u32[]{:S(2)}) %collective-permute-start.6) | collective-permute-done | bytes 229408 | tf_op jit(solution)/shard_map/ppermute | solution.py:449
  42.7 0.1 shard_map.192.mine
  42.9 0.1 collective-permute-start.7
  42.9 2.4 %shard_map.190 = (bf16[192,2048]{1,0:T(8,128)(2,1)}, bf16[96,2048]{1,0:T(8,128)(2,1)S(1)}) custom-call(bf16[192,2048]{1,0:T(8,128)(2,1)} %bitcast.8, f32[1,2048]{1,0:T(1,128)} %bitcast.10), custom_call_target="tpu_custom_call" | custom-call | tf_op jit(solution)/shard_map/pallas_call | solution.py:110
  45.3 20.5 %collective-permute-start.10 = (bf16[96,2048]{1,0:T(8,128)(2,1)S(1)}, bf16[96,2048]{1,0:T(8,128)(2,1)S(1)}, u32[]{:S(2)}, u32[]{:S(2)}) collective-permute-start(bf16[96,2048]{1,0:T(8,128)(2,1)S(1)} %get-tuple-element.67), channel_id=1, source_target_pairs={{0,16},{8,24},{16,0},{24,8},{1,17},{9,25},{17,1},{25,9},{2,18},{10... | collective-permute-start | bytes 1179656 | tf_op jit(solution)/shard_map/ppermute | solution.py:436
  65.9 0.7 collective-permute-start.12
  66.5 1.9 %collective-permute-start.8 = (bf16[96,2048]{1,0:T(8,128)(2,1)S(1)}, bf16[96,2048]{1,0:T(8,128)(2,1)S(1)}, u32[]{:S(2)}, u32[]{:S(2)}) collective-permute-start(bf16[96,2048]{1,0:T(8,128)(2,1)S(1)} %get-tuple-element.67), channel_id=1, source_target_pairs={{0,8},{8,0},{16,24},{24,16},{1,9},{9,1},{17,25},{25,17},{2,10},{10... | collective-permute-start | bytes 1179656 | tf_op jit(solution)/shard_map/ppermute | solution.py:436
  68.4 15.9 %collective-permute-done.10.refs_0_ = bf16[96,2048]{1,0:T(8,128)(2,1)S(1)} collective-permute-done((bf16[96,2048]{1,0:T(8,128)(2,1)S(1)}, bf16[96,2048]{1,0:T(8,128)(2,1)S(1)}, u32[]{:S(2)}, u32[]{:S(2)}) %collective-permute-start.10) | collective-permute-done | bytes 393248 | tf_op jit(solution)/shard_map/ppermute | solution.py:436
  84.3 1.3 collective-permute-start.14
  85.6 0.0 collective-permute-done.12.refs_0_
  85.6 0.7 collective-permute-start.13
  86.3 1.6 collective-permute-start.28
  87.9 0.0 collective-permute-done.30.refs_12_
  87.9 0.5 collective-permute-start.32
  88.4 8.6 %collective-permute-done.14.refs_2_ = bf16[96,2048]{1,0:T(8,128)(2,1)S(1)} collective-permute-done((bf16[96,2048]{1,0:T(8,128)(2,1)S(1)}, bf16[96,2048]{1,0:T(8,128)(2,1)S(1)}, u32[]{:S(2)}, u32[]{:S(2)}) %collective-permute-start.14) | collective-permute-done | bytes 393248 | tf_op jit(solution)/shard_map/ppermute | solution.py:436
  96.9 1.5 collective-permute-start.11
  98.4 0.0 collective-permute-done.13.refs_1_
  98.4 0.5 collective-permute-start.9
  99.0 10.0 %collective-permute-done.11.refs_1_ = bf16[96,2048]{1,0:T(8,128)(2,1)S(1)} collective-permute-done((bf16[96,2048]{1,0:T(8,128)(2,1)S(1)}, bf16[96,2048]{1,0:T(8,128)(2,1)S(1)}, u32[]{:S(2)}, u32[]{:S(2)}) %collective-permute-start.11) | collective-permute-done | bytes 393248 | tf_op jit(solution)/shard_map/ppermute | solution.py:442
  108.9 0.0 collective-permute-start.27
  108.9 6.3 %collective-permute-done.9.refs_1_ = bf16[96,2048]{1,0:T(8,128)(2,1)S(1)} collective-permute-done((bf16[96,2048]{1,0:T(8,128)(2,1)S(1)}, bf16[96,2048]{1,0:T(8,128)(2,1)S(1)}, u32[]{:S(2)}, u32[]{:S(2)}) %collective-permute-start.9) | collective-permute-done | bytes 393248 | tf_op jit(solution)/shard_map/ppermute | solution.py:442
  115.3 0.5 collective-permute-start.29
  115.8 7.3 %collective-permute-done.32.refs_14_ = bf16[4,784,128]{2,1,0:T(8,128)(2,1)S(1)} collective-permute-done((bf16[4,784,128]{2,1,0:T(8,128)(2,1)S(1)}, bf16[4,784,128]{2,1,0:T(8,128)(2,1)S(1)}, u32[]{:S(2)}, u32[]{:S(2)}) %collective-permute-start.32) | collective-permute-done | bytes 802848 | tf_op jit(solution)/shard_map/ppermute | solution.py:449
  123.1 3.4 %collective-permute-start.15 = (bf16[96,2048]{1,0:T(8,128)(2,1)S(1)}, bf16[96,2048]{1,0:T(8,128)(2,1)S(1)}, u32[]{:S(2)}, u32[]{:S(2)}) collective-permute-start(bf16[96,2048]{1,0:T(8,128)(2,1)S(1)} %collective-permute-done.14.refs_2_), channel_id=1, source_target_pairs={{0,1},{1,0},{24,25},{25,24},{2,3},{3,2},{26,27},{27,26},{4,5},{5,4... | collective-permute-start | bytes 1179656 | tf_op jit(solution)/shard_map/ppermute | solution.py:442
  126.5 1.1 shard_map.193
  127.6 4.6 %shard_map.194 = (bf16[2048,896]{1,0:T(8,128)(2,1)S(1)}, bf16[192,256]{1,0:T(8,128)(2,1)S(1)}, bf16[192,128]{1,0:T(8,128)(2,1)S(1)}, f32[3,64,128]{2,1,0:T(8,128...) custom-call(bf16[192,2048]{1,0:T(8,128)(2,1)} %get-tuple-element.53., ...), custom_call_target="tpu_custom_call" | custom-call | tf_op jit(solution)/shard_map/pallas_call | solution.py:110
  132.2 3.2 %shard_map.196 = (bf16[192,256]{1,0:T(8,128)(2,1)S(1)}, bf16[192,128]{1,0:T(8,128)(2,1)S(1)}, f32[3,64,128]{2,1,0:T(8,128)S(1)}, bf16[3,128,128]{2,1,0:T(8,128)(...) custom-call(bf16[96,2048]{1,0:T(8,128)(2,1)S(1)} %collective-permute-done.10.refs_0, ...), custom_call_target="tpu_custom_call" | custom-call | tf_op jit(solution)/shard_map/pallas_call | solution.py:110
  135.4 3.2 %shard_map.195 = (bf16[192,256]{1,0:T(8,128)(2,1)S(1)}, bf16[192,128]{1,0:T(8,128)(2,1)S(1)}, f32[3,64,128]{2,1,0:T(8,128)S(1)}, bf16[3,128,128]{2,1,0:T(8,128)(...) custom-call(bf16[96,2048]{1,0:T(8,128)(2,1)S(1)} %collective-permute-done.8.refs_0_, ...), custom_call_target="tpu_custom_call" | custom-call | tf_op jit(solution)/shard_map/pallas_call | solution.py:110
  138.6 3.4 %shard_map.197 = (bf16[192,256]{1,0:T(8,128)(2,1)S(1)}, bf16[192,128]{1,0:T(8,128)(2,1)S(1)}, f32[3,64,128]{2,1,0:T(8,128)S(1)}, bf16[3,128,128]{2,1,0:T(8,128)(...) custom-call(bf16[96,2048]{1,0:T(8,128)(2,1)S(1)} %collective-permute-done.12.refs_0, ...), custom_call_target="tpu_custom_call" | custom-call | tf_op jit(solution)/shard_map/pallas_call | solution.py:110
  142.0 0.0 copy-start
  142.0 2.5 %shard_map.198 = (bf16[96,256]{1,0:T(8,128)(2,1)S(1)}, bf16[96,256]{1,0:T(8,128)(2,1)S(1)}, bf16[96,256]{1,0:T(8,128)(2,1)S(1)}, bf16[96,256]{1,0:T(8,128)(2,1)S...) custom-call(bf16[192,256]{1,0:T(8,128)(2,1)S(1)} %get-tuple-element., ...), custom_call_target="tpu_custom_call" | custom-call | tf_op jit(solution)/shard_map/pallas_call | solution.py:110
  144.5 0.6 collective-permute-start.16
  145.0 7.4 %collective-permute-start.17 = (bf16[96,256]{1,0:T(8,128)(2,1)S(1)}, bf16[96,256]{1,0:T(8,128)(2,1)S(1)}, u32[]{:S(2)}, u32[]{:S(2)}) collective-permute-start(bf16[96,256]{1,0:T(8,128)(2,1)S(1)} %get-tuple-element.95), channel_id=1, source_target_pairs={{0,8},{1,9},{8,0},{9,1},{16,24},{17,25},{24,16},{25,17},{2,10},{3,... | collective-permute-start | bytes 147464 | tf_op jit(solution)/shard_map/ppermute | solution.py:532
  152.4 1.0 collective-permute-start.18
  153.5 0.9 collective-permute-start.19
  154.4 2.0 %collective-permute-start.20 = (bf16[96,256]{1,0:T(8,128)(2,1)S(1)}, bf16[96,256]{1,0:T(8,128)(2,1)S(1)}, u32[]{:S(2)}, u32[]{:S(2)}) collective-permute-start(bf16[96,256]{1,0:T(8,128)(2,1)S(1)} %get-tuple-element.98), channel_id=1, source_target_pairs={{0,17},{1,16},{8,25},{9,24},{16,1},{17,0},{24,9},{25,8},{2,19},{3,... | collective-permute-start | bytes 147464 | tf_op jit(solution)/shard_map/ppermute | solution.py:532
  156.4 2.0 %collective-permute-start.21 = (bf16[96,256]{1,0:T(8,128)(2,1)S(1)}, bf16[96,256]{1,0:T(8,128)(2,1)S(1)}, u32[]{:S(2)}, u32[]{:S(2)}) collective-permute-start(bf16[96,256]{1,0:T(8,128)(2,1)S(1)} %get-tuple-element.99), channel_id=1, source_target_pairs={{0,24},{1,25},{8,16},{9,17},{16,8},{17,9},{24,0},{25,1},{2,26},{3,... | collective-permute-start | bytes 147464 | tf_op jit(solution)/shard_map/ppermute | solution.py:532
  158.4 2.7 %collective-permute-start.22 = (bf16[96,256]{1,0:T(8,128)(2,1)S(1)}, bf16[96,256]{1,0:T(8,128)(2,1)S(1)}, u32[]{:S(2)}, u32[]{:S(2)}) collective-permute-start(bf16[96,256]{1,0:T(8,128)(2,1)S(1)} %get-tuple-element.100), channel_id=1, source_target_pairs={{0,25},{1,24},{8,17},{9,16},{16,9},{17,8},{24,1},{25,0},{2,27},{3,... | collective-permute-start | bytes 147464 | tf_op jit(solution)/shard_map/ppermute | solution.py:532
  161.1 0.2 collective-permute-done.19.refs_4_
  161.3 1.2 collective-permute-done.20.refs_5_
  162.5 2.7 %collective-permute-done.22.refs_7_ = bf16[96,256]{1,0:T(8,128)(2,1)S(1)} collective-permute-done((bf16[96,256]{1,0:T(8,128)(2,1)S(1)}, bf16[96,256]{1,0:T(8,128)(2,1)S(1)}, u32[]{:S(2)}, u32[]{:S(2)}) %collective-permute-start.22) | collective-permute-done | bytes 49184 | tf_op jit(solution)/shard_map/ppermute | solution.py:532
  165.3 3.9 %shard_map.201 = bf16[96,2048]{1,0:T(8,128)(2,1)} custom-call(bf16[512,512]{1,0:T(8,128)(2,1)S(1)} %copy-done, bf16[96,256]{1,0:T(8,128)(2,1)S(1)} %get-tuple-element.93.refs_0_, bf16[96,256]{1,0:T(8,128)(2,1)S(1)} %collective-permute-done.16.refs_1_, bf16[96,256]{1,0:T(8,128)(2,1)S(1)} %collective-permute-done.17.refs_2_, ...), custom_call_target="tpu_custom_call" | custom-call | tf_op jit(solution)/shard_map/pallas_call | solution.py:110
  (18 shorter events, 0.0 us)
Async XLA Ops:
  0.9 14.4 %collective-permute-start.24 = (bf16[784,128]{1,0:T(8,128)(2,1)S(1)}, bf16[784,128]{1,0:T(8,128)(2,1)S(1)}, u32[]{:S(2)}, u32[]{:S(2)}) collective-permute-start(bf16[784,128]{1,0:T(8,128)(2,1)S(1)} %shard_map.199.own), channel_id=1, source_target_pairs={{0,16},{8,24},{16,0},{24,8},{1,17},{9,25},{17,1},{25,9},{2,18},{10... | collective-permute-start | bytes 602120 | tf_op jit(solution)/shard_map/ppermute | solution.py:436
  5.1 15.5 %collective-permute-start.23 = (bf16[784,128]{1,0:T(8,128)(2,1)S(1)}, bf16[784,128]{1,0:T(8,128)(2,1)S(1)}, u32[]{:S(2)}, u32[]{:S(2)}) collective-permute-start(bf16[784,128]{1,0:T(8,128)(2,1)S(1)} %shard_map.199.own), channel_id=1, source_target_pairs={{0,8},{8,0},{16,24},{24,16},{1,9},{9,1},{17,25},{25,17},{2,10},{10... | collective-permute-start | bytes 602120 | tf_op jit(solution)/shard_map/ppermute | solution.py:436
  8.6 21.9 %collective-permute-start = (bf16[128,896]{1,0:T(8,128)(2,1)S(1)}, bf16[128,896]{1,0:T(8,128)(2,1)S(1)}, u32[]{:S(2)}, u32[]{:S(2)}) collective-permute-start(bf16[128,896]{1,0:T(8,128)(2,1)S(1)} %get-tuple-element.55), channel_id=1, source_target_pairs={{0,8},{8,0},{16,24},{24,16},{1,9},{9,1},{17,25},{25,17},{2,10},{10... | collective-permute-start | bytes 688136 | tf_op jit(solution)/shard_map/ppermute | solution.py:449
  9.1 23.0 %collective-permute-start.1 = (bf16[128,896]{1,0:T(8,128)(2,1)S(1)}, bf16[128,896]{1,0:T(8,128)(2,1)S(1)}, u32[]{:S(2)}, u32[]{:S(2)}) collective-permute-start(bf16[128,896]{1,0:T(8,128)(2,1)S(1)} %get-tuple-element.56), channel_id=1, source_target_pairs={{0,16},{8,24},{16,0},{24,8},{1,17},{9,25},{17,1},{25,9},{2,18},{10... | collective-permute-start | bytes 688136 | tf_op jit(solution)/shard_map/ppermute | solution.py:449
  9.2 23.4 %collective-permute-start.2 = (bf16[128,896]{1,0:T(8,128)(2,1)S(1)}, bf16[128,896]{1,0:T(8,128)(2,1)S(1)}, u32[]{:S(2)}, u32[]{:S(2)}) collective-permute-start(bf16[128,896]{1,0:T(8,128)(2,1)S(1)} %get-tuple-element.57), channel_id=1, source_target_pairs={{0,24},{8,16},{16,8},{24,0},{1,25},{9,17},{17,9},{25,1},{2,26},{10... | collective-permute-start | bytes 688136 | tf_op jit(solution)/shard_map/ppermute | solution.py:449
  15.3 6.6 %collective-permute-start.25 = (bf16[784,128]{1,0:T(8,128)(2,1)S(1)}, bf16[784,128]{1,0:T(8,128)(2,1)S(1)}, u32[]{:S(2)}, u32[]{:S(2)}) collective-permute-start(bf16[784,128]{1,0:T(8,128)(2,1)S(1)} %shard_map.199.own), channel_id=1, source_target_pairs={{8,16},{16,8},{9,17},{17,9},{10,18},{18,10},{11,19},{19,11},{12,20... | collective-permute-start | bytes 602120 | tf_op jit(solution)/shard_map/ppermute | solution.py:436
  20.6 13.6 %collective-permute-start.26 = (bf16[784,128]{1,0:T(8,128)(2,1)S(1)}, bf16[784,128]{1,0:T(8,128)(2,1)S(1)}, u32[]{:S(2)}, u32[]{:S(2)}) collective-permute-start(bf16[784,128]{1,0:T(8,128)(2,1)S(1)} %collective-permute-done.24.refs_1_), channel_id=1, source_target_pairs={{16,24},{8,0},{17,25},{9,1},{18,26},{10,2},{19,27},{11,3},{20,28},... | collective-permute-start | bytes 602120 | tf_op jit(solution)/shard_map/ppermute | solution.py:436
  21.9 13.9 %collective-permute-start.3 = (bf16[128,896]{1,0:T(8,128)(2,1)S(1)}, bf16[128,896]{1,0:T(8,128)(2,1)S(1)}, u32[]{:S(2)}, u32[]{:S(2)}) collective-permute-start(bf16[128,896]{1,0:T(8,128)(2,1)S(1)} %get-tuple-element.54.refs_0_), channel_id=1, source_target_pairs={{0,4},{2,6},{4,0},{6,2},{1,5},{3,7},{5,1},{7,3},{8,12},{10,14},{12... | collective-permute-start | bytes 688136 | tf_op jit(solution)/shard_map/ppermute | solution.py:449
  30.5 7.3 %collective-permute-start.4 = (bf16[128,896]{1,0:T(8,128)(2,1)S(1)}, bf16[128,896]{1,0:T(8,128)(2,1)S(1)}, u32[]{:S(2)}, u32[]{:S(2)}) collective-permute-start(bf16[128,896]{1,0:T(8,128)(2,1)S(1)} %collective-permute-done.refs_1_), channel_id=1, source_target_pairs={{0,4},{2,6},{4,0},{6,2},{1,5},{3,7},{5,1},{7,3},{8,12},{10,14},{12... | collective-permute-start | bytes 688136 | tf_op jit(solution)/shard_map/ppermute | solution.py:449
  32.1 8.2 %collective-permute-start.5 = (bf16[128,896]{1,0:T(8,128)(2,1)S(1)}, bf16[128,896]{1,0:T(8,128)(2,1)S(1)}, u32[]{:S(2)}, u32[]{:S(2)}) collective-permute-start(bf16[128,896]{1,0:T(8,128)(2,1)S(1)} %collective-permute-done.1.refs_2_), channel_id=1, source_target_pairs={{0,4},{2,6},{4,0},{6,2},{1,5},{3,7},{5,1},{7,3},{8,12},{10,14},{12... | collective-permute-start | bytes 688136 | tf_op jit(solution)/shard_map/ppermute | solution.py:449
  32.6 10.2 %collective-permute-start.6 = (bf16[128,896]{1,0:T(8,128)(2,1)S(1)}, bf16[128,896]{1,0:T(8,128)(2,1)S(1)}, u32[]{:S(2)}, u32[]{:S(2)}) collective-permute-start(bf16[128,896]{1,0:T(8,128)(2,1)S(1)} %collective-permute-done.2.refs_3_), channel_id=1, source_target_pairs={{0,4},{2,6},{4,0},{6,2},{1,5},{3,7},{5,1},{7,3},{8,12},{10,14},{12... | collective-permute-start | bytes 688136 | tf_op jit(solution)/shard_map/ppermute | solution.py:449
  34.2 53.7 %collective-permute-start.30 = (bf16[4,784,128]{2,1,0:T(8,128)(2,1)S(1)}, bf16[4,784,128]{2,1,0:T(8,128)(2,1)S(1)}, u32[]{:S(2)}, u32[]{:S(2)}) collective-permute-start(bf16[4,784,128]{2,1,0:T(8,128)(2,1)S(1)} %shard_map.200.refs_8_), channel_id=1, source_target_pairs={{0,1},{1,0},{2,3},{3,2},{4,5},{5,4},{6,7},{7,6},{8,9},{9,8},{10,11... | collective-permute-start | bytes 2408456 | tf_op jit(solution)/shard_map/ppermute | solution.py:449
  42.9 80.3 %collective-permute-start.7 = (bf16[1024,896]{1,0:T(8,128)(2,1)S(1)}, bf16[1024,896]{1,0:T(8,128)(2,1)S(1)}, u32[]{:S(2)}, u32[]{:S(2)}) collective-permute-start(bf16[1024,896]{1,0:T(8,128)(2,1)S(1)} %shard_map.192.mine), channel_id=1, source_target_pairs={{0,2},{2,0},{4,6},{6,4},{1,3},{3,1},{5,7},{7,5},{8,10},{10,8},{12,... | collective-permute-start | bytes 5505032 | tf_op jit(solution)/shard_map/ppermute | solution.py:449
  45.3 39.0 %collective-permute-start.10 = (bf16[96,2048]{1,0:T(8,128)(2,1)S(1)}, bf16[96,2048]{1,0:T(8,128)(2,1)S(1)}, u32[]{:S(2)}, u32[]{:S(2)}) collective-permute-start(bf16[96,2048]{1,0:T(8,128)(2,1)S(1)} %get-tuple-element.67), channel_id=1, source_target_pairs={{0,16},{8,24},{16,0},{24,8},{1,17},{9,25},{17,1},{25,9},{2,18},{10... | collective-permute-start | bytes 1179656 | tf_op jit(solution)/shard_map/ppermute | solution.py:436
  65.9 19.7 %collective-permute-start.12 = (bf16[96,2048]{1,0:T(8,128)(2,1)S(1)}, bf16[96,2048]{1,0:T(8,128)(2,1)S(1)}, u32[]{:S(2)}, u32[]{:S(2)}) collective-permute-start(bf16[96,2048]{1,0:T(8,128)(2,1)S(1)} %get-tuple-element.67), channel_id=1, source_target_pairs={{8,16},{16,8},{9,17},{17,9},{10,18},{18,10},{11,19},{19,11},{12,20... | collective-permute-start | bytes 1179656 | tf_op jit(solution)/shard_map/ppermute | solution.py:436
  66.5 19.7 %collective-permute-start.8 = (bf16[96,2048]{1,0:T(8,128)(2,1)S(1)}, bf16[96,2048]{1,0:T(8,128)(2,1)S(1)}, u32[]{:S(2)}, u32[]{:S(2)}) collective-permute-start(bf16[96,2048]{1,0:T(8,128)(2,1)S(1)} %get-tuple-element.67), channel_id=1, source_target_pairs={{0,8},{8,0},{16,24},{24,16},{1,9},{9,1},{17,25},{25,17},{2,10},{10... | collective-permute-start | bytes 1179656 | tf_op jit(solution)/shard_map/ppermute | solution.py:436
  84.3 12.6 %collective-permute-start.14 = (bf16[96,2048]{1,0:T(8,128)(2,1)S(1)}, bf16[96,2048]{1,0:T(8,128)(2,1)S(1)}, u32[]{:S(2)}, u32[]{:S(2)}) collective-permute-start(bf16[96,2048]{1,0:T(8,128)(2,1)S(1)} %collective-permute-done.10.refs_0_), channel_id=1, source_target_pairs={{16,24},{8,0},{17,25},{9,1},{18,26},{10,2},{19,27},{11,3},{20,28},... | collective-permute-start | bytes 1179656 | tf_op jit(solution)/shard_map/ppermute | solution.py:436
  85.6 12.9 %collective-permute-start.13 = (bf16[96,2048]{1,0:T(8,128)(2,1)S(1)}, bf16[96,2048]{1,0:T(8,128)(2,1)S(1)}, u32[]{:S(2)}, u32[]{:S(2)}) collective-permute-start(bf16[96,2048]{1,0:T(8,128)(2,1)S(1)} %collective-permute-done.12.refs_0_), channel_id=1, source_target_pairs={{8,9},{9,8},{16,17},{17,16},{10,11},{11,10},{18,19},{19,18},{12,13... | collective-permute-start | bytes 1179656 | tf_op jit(solution)/shard_map/ppermute | solution.py:442
  86.3 29.0 %collective-permute-start.28 = (bf16[4,784,128]{2,1,0:T(8,128)(2,1)S(1)}, bf16[4,784,128]{2,1,0:T(8,128)(2,1)S(1)}, u32[]{:S(2)}, u32[]{:S(2)}) collective-permute-start(bf16[4,784,128]{2,1,0:T(8,128)(2,1)S(1)} %shard_map.200.refs_8_), channel_id=1, source_target_pairs={{0,4},{2,6},{4,0},{6,2},{1,5},{3,7},{5,1},{7,3},{8,12},{10,14},{12... | collective-permute-start | bytes 2408456 | tf_op jit(solution)/shard_map/ppermute | solution.py:449
  87.9 35.2 %collective-permute-start.32 = (bf16[4,784,128]{2,1,0:T(8,128)(2,1)S(1)}, bf16[4,784,128]{2,1,0:T(8,128)(2,1)S(1)}, u32[]{:S(2)}, u32[]{:S(2)}) collective-permute-start(bf16[4,784,128]{2,1,0:T(8,128)(2,1)S(1)} %collective-permute-done.30.refs_12_), channel_id=1, source_target_pairs={{0,4},{2,6},{4,0},{6,2},{1,5},{3,7},{5,1},{7,3},{8,12},{10,14},{12... | collective-permute-start | bytes 2408456 | tf_op jit(solution)/shard_map/ppermute | solution.py:449
  96.9 12.0 %collective-permute-start.11 = (bf16[96,2048]{1,0:T(8,128)(2,1)S(1)}, bf16[96,2048]{1,0:T(8,128)(2,1)S(1)}, u32[]{:S(2)}, u32[]{:S(2)}) collective-permute-start(bf16[96,2048]{1,0:T(8,128)(2,1)S(1)} %collective-permute-done.10.refs_0_), channel_id=1, source_target_pairs={{0,1},{1,0},{8,9},{9,8},{16,17},{17,16},{24,25},{25,24},{2,3},{3,2... | collective-permute-start | bytes 1179656 | tf_op jit(solution)/shard_map/ppermute | solution.py:442
  98.4 16.8 %collective-permute-start.9 = (bf16[96,2048]{1,0:T(8,128)(2,1)S(1)}, bf16[96,2048]{1,0:T(8,128)(2,1)S(1)}, u32[]{:S(2)}, u32[]{:S(2)}) collective-permute-start(bf16[96,2048]{1,0:T(8,128)(2,1)S(1)} %collective-permute-done.8.refs_0_), channel_id=1, source_target_pairs={{0,1},{1,0},{8,9},{9,8},{16,17},{17,16},{24,25},{25,24},{2,3},{3,2... | collective-permute-start | bytes 1179656 | tf_op jit(solution)/shard_map/ppermute | solution.py:442
  108.9 36.1 %collective-permute-start.27 = (bf16[4,784,128]{2,1,0:T(8,128)(2,1)S(1)}, bf16[4,784,128]{2,1,0:T(8,128)(2,1)S(1)}, u32[]{:S(2)}, u32[]{:S(2)}) collective-permute-start(bf16[4,784,128]{2,1,0:T(8,128)(2,1)S(1)} %shard_map.200.refs_8_), channel_id=1, source_target_pairs={{0,2},{2,0},{4,6},{6,4},{1,3},{3,1},{5,7},{7,5},{8,10},{10,8},{12,... | collective-permute-start | bytes 2408456 | tf_op jit(solution)/shard_map/ppermute | solution.py:449
  115.3 37.2 %collective-permute-start.31 = (bf16[4,784,128]{2,1,0:T(8,128)(2,1)S(1)}, bf16[4,784,128]{2,1,0:T(8,128)(2,1)S(1)}, u32[]{:S(2)}, u32[]{:S(2)}) collective-permute-start(bf16[4,784,128]{2,1,0:T(8,128)(2,1)S(1)} %collective-permute-done.30.refs_12_), channel_id=1, source_target_pairs={{0,2},{2,0},{4,6},{6,4},{1,3},{3,1},{5,7},{7,5},{8,10},{10,8},{12,... | collective-permute-start | bytes 2408456 | tf_op jit(solution)/shard_map/ppermute | solution.py:449
  115.3 38.2 %collective-permute-start.29 = (bf16[4,784,128]{2,1,0:T(8,128)(2,1)S(1)}, bf16[4,784,128]{2,1,0:T(8,128)(2,1)S(1)}, u32[]{:S(2)}, u32[]{:S(2)}) collective-permute-start(bf16[4,784,128]{2,1,0:T(8,128)(2,1)S(1)} %collective-permute-done.28.refs_10_), channel_id=1, source_target_pairs={{0,2},{2,0},{4,6},{6,4},{1,3},{3,1},{5,7},{7,5},{8,10},{10,8},{12,... | collective-permute-start | bytes 2408456 | tf_op jit(solution)/shard_map/ppermute | solution.py:449
  123.1 42.2 %collective-permute-start.33 = (bf16[4,784,128]{2,1,0:T(8,128)(2,1)S(1)}, bf16[4,784,128]{2,1,0:T(8,128)(2,1)S(1)}, u32[]{:S(2)}, u32[]{:S(2)}) collective-permute-start(bf16[4,784,128]{2,1,0:T(8,128)(2,1)S(1)} %collective-permute-done.32.refs_14_), channel_id=1, source_target_pairs={{0,2},{2,0},{4,6},{6,4},{1,3},{3,1},{5,7},{7,5},{8,10},{10,8},{12,... | collective-permute-start | bytes 2408456 | tf_op jit(solution)/shard_map/ppermute | solution.py:449
  123.1 15.4 %collective-permute-start.15 = (bf16[96,2048]{1,0:T(8,128)(2,1)S(1)}, bf16[96,2048]{1,0:T(8,128)(2,1)S(1)}, u32[]{:S(2)}, u32[]{:S(2)}) collective-permute-start(bf16[96,2048]{1,0:T(8,128)(2,1)S(1)} %collective-permute-done.14.refs_2_), channel_id=1, source_target_pairs={{0,1},{1,0},{24,25},{25,24},{2,3},{3,2},{26,27},{27,26},{4,5},{5,4... | collective-permute-start | bytes 1179656 | tf_op jit(solution)/shard_map/ppermute | solution.py:442
  142.0 23.3 %copy-start = (bf16[512,512]{1,0:T(8,128)(2,1)S(1)}, bf16[512,512]{1,0:T(8,128)(2,1)}, u32[]{:S(2)}) copy-start(bf16[512,512]{1,0:T(8,128)(2,1)} %point.1) | copy-start | bytes 1572868
  144.5 9.9 %collective-permute-start.16 = (bf16[96,256]{1,0:T(8,128)(2,1)S(1)}, bf16[96,256]{1,0:T(8,128)(2,1)S(1)}, u32[]{:S(2)}, u32[]{:S(2)}) collective-permute-start(bf16[96,256]{1,0:T(8,128)(2,1)S(1)} %get-tuple-element.94), channel_id=1, source_target_pairs={{0,1},{1,0},{8,9},{9,8},{16,17},{17,16},{24,25},{25,24},{2,3},{3,2... | collective-permute-start | bytes 147464 | tf_op jit(solution)/shard_map/ppermute | solution.py:532
  145.0 11.4 %collective-permute-start.17 = (bf16[96,256]{1,0:T(8,128)(2,1)S(1)}, bf16[96,256]{1,0:T(8,128)(2,1)S(1)}, u32[]{:S(2)}, u32[]{:S(2)}) collective-permute-start(bf16[96,256]{1,0:T(8,128)(2,1)S(1)} %get-tuple-element.95), channel_id=1, source_target_pairs={{0,8},{1,9},{8,0},{9,1},{16,24},{17,25},{24,16},{25,17},{2,10},{3,... | collective-permute-start | bytes 147464 | tf_op jit(solution)/shard_map/ppermute | solution.py:532
  152.4 5.9 %collective-permute-start.18 = (bf16[96,256]{1,0:T(8,128)(2,1)S(1)}, bf16[96,256]{1,0:T(8,128)(2,1)S(1)}, u32[]{:S(2)}, u32[]{:S(2)}) collective-permute-start(bf16[96,256]{1,0:T(8,128)(2,1)S(1)} %get-tuple-element.96), channel_id=1, source_target_pairs={{0,9},{1,8},{8,1},{9,0},{16,25},{17,24},{24,17},{25,16},{2,11},{3,... | collective-permute-start | bytes 147464 | tf_op jit(solution)/shard_map/ppermute | solution.py:532
  153.5 7.9 %collective-permute-start.19 = (bf16[96,256]{1,0:T(8,128)(2,1)S(1)}, bf16[96,256]{1,0:T(8,128)(2,1)S(1)}, u32[]{:S(2)}, u32[]{:S(2)}) collective-permute-start(bf16[96,256]{1,0:T(8,128)(2,1)S(1)} %get-tuple-element.97), channel_id=1, source_target_pairs={{0,16},{1,17},{8,24},{9,25},{16,0},{17,1},{24,8},{25,9},{2,18},{3,... | collective-permute-start | bytes 147464 | tf_op jit(solution)/shard_map/ppermute | solution.py:532
  154.4 8.1 %collective-permute-start.20 = (bf16[96,256]{1,0:T(8,128)(2,1)S(1)}, bf16[96,256]{1,0:T(8,128)(2,1)S(1)}, u32[]{:S(2)}, u32[]{:S(2)}) collective-permute-start(bf16[96,256]{1,0:T(8,128)(2,1)S(1)} %get-tuple-element.98), channel_id=1, source_target_pairs={{0,17},{1,16},{8,25},{9,24},{16,1},{17,0},{24,9},{25,8},{2,19},{3,... | collective-permute-start | bytes 147464 | tf_op jit(solution)/shard_map/ppermute | solution.py:532
  156.4 6.1 %collective-permute-start.21 = (bf16[96,256]{1,0:T(8,128)(2,1)S(1)}, bf16[96,256]{1,0:T(8,128)(2,1)S(1)}, u32[]{:S(2)}, u32[]{:S(2)}) collective-permute-start(bf16[96,256]{1,0:T(8,128)(2,1)S(1)} %get-tuple-element.99), channel_id=1, source_target_pairs={{0,24},{1,25},{8,16},{9,17},{16,8},{17,9},{24,0},{25,1},{2,26},{3,... | collective-permute-start | bytes 147464 | tf_op jit(solution)/shard_map/ppermute | solution.py:532
  158.4 6.9 %collective-permute-start.22 = (bf16[96,256]{1,0:T(8,128)(2,1)S(1)}, bf16[96,256]{1,0:T(8,128)(2,1)S(1)}, u32[]{:S(2)}, u32[]{:S(2)}) collective-permute-start(bf16[96,256]{1,0:T(8,128)(2,1)S(1)} %get-tuple-element.100), channel_id=1, source_target_pairs={{0,25},{1,24},{8,17},{9,16},{16,9},{17,8},{24,1},{25,0},{2,27},{3,... | collective-permute-start | bytes 147464 | tf_op jit(solution)/shard_map/ppermute | solution.py:532
